TPU v7x, 32 devices: a whole 2x2x4 slice. The times are simulated.
32 devices in a mesh: ep: 16 (over z, y, x), tp: 2 (over core).
Axes of the slice: x: 2, y: 2, z: 4, core: 2. Of those that a mesh axis runs over, the one named last changes fastest.
Arguments:
- tokens: bfloat16 [4096, 2048], P(('ep', 'tp')), may hold values from -6 to 6
- norm_gain: float32 [2048], replicated, may hold values from 0.25 to 4
- routes: int32 [4096, 2], P(('ep', 'tp')), may hold values from 0 to 15, all different within a row; in each aligned block of 128 rows (0 to 127, 128 to 255, ...) at most 22 rows name the same one
- route_weights: float32 [4096, 2], P(('ep', 'tp')), may hold values from 0.1 to 1
- w_gate: bfloat16 [16, 2048, 1024], P('ep', None, 'tp'), may hold values from -0.125 to 0.125
- w_up: bfloat16 [16, 2048, 1024], P('ep', None, 'tp'), may hold values from -0.125 to 0.125
- w_down: bfloat16 [16, 1024, 2048], P('ep', 'tp'), may hold values from -0.1875 to 0.1875
- dense_in: bfloat16 [2048, 256], P('ep'), may hold values from -0.125 to 0.125
- dense_out: bfloat16 [2048, 256], P('ep'), may hold values from -0.375 to 0.375
- dense_gate: float32 [2048], replicated, may hold values from -6 to 6
Outputs:
- mixed: bfloat16 [4096, 2048], P(('ep', 'tp'))
Inputs may be any that keep to these rules, and one draw needn't show every extreme that they name: `routes`: each row names 2 different experts. Among the 128 rows of one device no expert is named more than 22 times; every draw has a device and an expert with exactly 22.
All inputs are finite; a program needn't handle non-finite values.
Results may differ from a plain program's by a relative error of at most 0.0074.
Values may be sent and summed in bfloat16 or wider, within the bound.
No kernel may reach another device: no remote copies, remote signals or barrier semaphores. Data moves between devices by JAX's collectives and lax.ppermute only.
A program may use at most 128 MiB of HBM per device.

v0:
```python
import jax
import jax.numpy as jnp
from jax import lax
from jax.sharding import PartitionSpec as P

CLAMP_LIMIT = 7.0
SLOPE_ALPHA = 1.702
NORM_EPS = 1e-06


def rms_normed(tokens, norm_gain):
    widened = tokens.astype(jnp.float32)
    inv_scale = lax.rsqrt(jnp.mean(widened * widened, axis=1, keepdims=True) + NORM_EPS)
    return (widened * inv_scale * norm_gain).astype(jnp.bfloat16)


def clamped_unit(gate_pre, up_pre):
    gate_clip = jnp.minimum(gate_pre, CLAMP_LIMIT)
    up_clip = jnp.clip(up_pre, -CLAMP_LIMIT, CLAMP_LIMIT)
    return ((up_clip + 1.0) * gate_clip * jax.nn.sigmoid(SLOPE_ALPHA * gate_clip)).astype(
        jnp.bfloat16
    )


def rounded_term(hidden_rows, down_rows):
    partial_value = jnp.dot(hidden_rows, down_rows, preferred_element_type=jnp.float32).astype(
        jnp.bfloat16
    )
    return lax.optimization_barrier(partial_value).astype(jnp.float32)


def shards(
    tokens, norm_gain, routes, route_weights, w_gate, w_up, w_down, dense_in, dense_out, dense_gate
):
    tok_rows, model_width = tokens.shape
    top_count = routes.shape[1]
    sources = lax.axis_size("ep")
    experts = sources * w_gate.shape[0]
    core_count = lax.axis_size("tp")
    capacity = (4 * tok_rows * top_count + 3 * experts - 1) // (3 * experts)
    entries = tok_rows * top_count
    normed = rms_normed(tokens, norm_gain)
    flat_routes = routes.reshape(entries)
    onehot = flat_routes[:, None] == lax.broadcasted_iota(jnp.int32, (1, experts), 1)
    earlier_mask = (
        lax.broadcasted_iota(jnp.int32, (entries, entries), 0)
        > lax.broadcasted_iota(jnp.int32, (entries, entries), 1)
    ).astype(jnp.bfloat16)
    counted = jnp.dot(earlier_mask, onehot.astype(jnp.bfloat16), preferred_element_type=jnp.float32)
    slot_index = jnp.sum(jnp.where(onehot, counted, 0.0), axis=1).astype(jnp.int32)
    position = flat_routes * capacity + slot_index
    places = position[None, :] == lax.broadcasted_iota(jnp.int32, (experts * capacity, 1), 0)
    filled = jnp.any(places, axis=1)
    source_entry = jnp.sum(
        jnp.where(places, lax.broadcasted_iota(jnp.int32, (1, entries), 1), 0), axis=1
    )
    buffer = jnp.where(
        filled[:, None], normed[source_entry // top_count], jnp.zeros((), jnp.bfloat16)
    )
    buffer = buffer.reshape(experts, capacity, model_width)
    gate_w = w_gate[0]
    up_w = w_up[0]
    down_w = w_down[0]
    gate_w, up_w, down_w = (
        lax.all_gather(gate_w, "tp", axis=1, tiled=True),
        lax.all_gather(up_w, "tp", axis=1, tiled=True),
        lax.all_gather(down_w, "tp", axis=0, tiled=True),
    )
    received = lax.all_to_all(buffer, "ep", split_axis=0, concat_axis=0, tiled=True)
    slot_count = received.shape[1]
    flat_rows = received.reshape(sources * slot_count, model_width)
    hidden = clamped_unit(
        jnp.dot(flat_rows, gate_w, preferred_element_type=jnp.float32),
        jnp.dot(flat_rows, up_w, preferred_element_type=jnp.float32),
    )
    half_width = hidden.shape[1] // core_count
    summed = rounded_term(hidden[:, :half_width], down_w[:half_width])
    summed = summed + rounded_term(
        hidden[:, half_width : half_width + half_width],
        down_w[half_width : half_width + half_width],
    )
    expert_out = summed.astype(jnp.bfloat16).reshape(sources, slot_count, model_width)
    returned = lax.all_to_all(expert_out, "ep", split_axis=0, concat_axis=0, tiled=True)
    flat_returned = returned.reshape(experts * capacity, model_width)
    picked = flat_returned[position].astype(jnp.float32).reshape(tok_rows, top_count, model_width)
    weighted = jnp.sum(picked * route_weights[:, :, None], axis=1)
    whole_in, whole_out = (
        lax.all_gather(dense_in, "ep", axis=0, tiled=True),
        lax.all_gather(dense_out, "ep", axis=0, tiled=True),
    )
    dense_hidden = jax.nn.silu(
        jnp.dot(normed, whole_in, preferred_element_type=jnp.float32)
    ).astype(jnp.bfloat16)
    branch = lax.dot_general(
        dense_hidden, whole_out, (((1,), (1,)), ((), ())), preferred_element_type=jnp.float32
    )
    return (weighted + jax.nn.sigmoid(dense_gate) * branch).astype(jnp.bfloat16)


def solution(mesh):
    placed = (
        P(("ep", "tp"), None),
        P(),
        P(("ep", "tp"), None),
        P(("ep", "tp"), None),
        P("ep", None, "tp"),
        P("ep", None, "tp"),
        P("ep", "tp", None),
        P("ep", None),
        P("ep", None),
        P(),
    )
    return jax.shard_map(
        shards, mesh=mesh, in_specs=placed, out_specs=P(("ep", "tp"), None), check_vma=False
    )
```

profile of v0, /device:TPU:0, one launch (start us, length us, event | category | flops | bytes accessed | tf_op | source)
XLA Modules:
  0.0 191.8 jit_solution(7920561846483275655)
XLA Ops:
  6.5 0.7 all-gather.15.cloned.1.call-update
  7.3 0.7 all-gather.13.cloned.1.call-update
  8.1 0.7 all-gather.17.cloned.1.call-update
  9.0 0.2 fusion.14
  9.5 0.2 fusion.15
  9.7 0.2 fusion.17
  9.9 2.5 %gather_fusion = bf16[352,2048]{1,0:T(8,128)(2,1)S(1)} fusion(bf16[128,2048]{1,0:T(8,128)(2,1)S(1)} %fusion.17, s32[1024]{0:T(1024)S(1)} %pad_clamp_fusion.1), kind=kCustom, calls=%fused_computation | custom fusion | bytes 2884992 | tf_op jit(solution)/shard_map/gather | solution.py:58
  12.3 0.4 gather.9
  12.8 0.2 fusion.20
  13.0 1.4 broadcast_select_fusion
  14.4 8.3 %all-to-all-start = ((bf16[16,22,2048]{2,1,0:T(8,128)(2,1)}), bf16[16,22,2048]{2,1,0:T(8,128)(2,1)S(1)}, u32[]{:S(2)}, u32[]{:S(2)}) async-start(bf16[16,22,2048]{2,1,0:T(8,128)(2,1)} %broadcast_select_fusion), calls=%async_computation | async-start | bytes 3145728 | tf_op jit(solution)/shard_map/all_to_all | solution.py:69
  22.8 0.5 all-gather.11.cloned.1.call-update
  23.3 33.5 %all-to-all-done = bf16[16,22,2048]{2,1,0:T(8,128)(2,1)S(1)} async-done(((bf16[16,22,2048]{2,1,0:T(8,128)(2,1)}), bf16[16,22,2048]{2,1,0:T(8,128)(2,1)S(1)}, u32[]{:S(2)}, u32[]{:S(2)}) %all-to-all-start) | async-done | bytes 1441824 | tf_op jit(solution)/shard_map/all_to_all | solution.py:69
  56.8 0.4 reshape.136
  57.3 5.0 %fusion.9 = f32[352,1024]{1,0:T(8,128)} fusion(bf16[352,2048]{1,0:T(8,128)(2,1)S(1)} %reshape.136, bf16[1,2048,1024]{2,1,0:T(8,128)(2,1)} %all-gather.15.cloned.1.call-done), kind=kOutput, calls=%fused_computation.17 | convolution fusion | flops 1476755456 | bytes 7077888 | tf_op jit(solution)/shard_map/dot_general | solution.py:73
  62.3 4.5 %multiply_convert_fusion = bf16[352,1024]{1,0:T(8,128)(2,1)S(1)} fusion(f32[352,1024]{1,0:T(8,128)} %fusion.9, bf16[352,2048]{1,0:T(8,128)(2,1)S(1)} %reshape.136, bf16[1,2048,1024]{2,1,0:T(8,128)(2,1)} %all-gather.13.cloned.1.call-done), kind=kOutput, calls=%fused_computation.18 | convolution fusion | flops 1479639040 | bytes 7798784 | tf_op jit(solution)/shard_map/dot_general | solution.py:74
  66.8 2.7 %convolution_convert_fusion.1 = bf16[352,2048]{1,0:T(8,128)(2,1)S(1)} fusion(bf16[1,1024,2048]{2,1,0:T(8,128)(2,1)} %all-gather.17.cloned.1.call-done, bf16[352,1024]{1,0:T(8,128)(2,1)S(1)} %multiply_convert_fusion), kind=kOutput, calls=%fused_computation.8 | convolution fusion | flops 738918400 | bytes 3899392 | tf_op jit(solution)/shard_map/dot_general | solution.py:26
  69.5 0.2 copy-done.6
  69.6 0.9 convolution_convert_fusion
  70.6 0.5 add_convert_fusion
  71.1 1.4 reshape.137
  72.5 7.9 %all-to-all-start.1 = ((bf16[16,22,2048]{2,1,0:T(8,128)(2,1)}), bf16[16,22,2048]{2,1,0:T(8,128)(2,1)S(1)}, u32[]{:S(2)}, u32[]{:S(2)}) async-start(bf16[16,22,2048]{2,1,0:T(8,128)(2,1)} %reshape.137), calls=%async_computation.1 | async-start | bytes 3145728 | tf_op jit(solution)/shard_map/all_to_all | solution.py:83
  80.4 0.2 all-gather.9.cloned.1.call-start
  80.6 0.4 all-gather.9.cloned.1.call-update
  81.3 0.7 copy.17
  82.0 38.2 %all-to-all-done.1 = bf16[16,22,2048]{2,1,0:T(8,128)(2,1)S(1)} async-done(((bf16[16,22,2048]{2,1,0:T(8,128)(2,1)}), bf16[16,22,2048]{2,1,0:T(8,128)(2,1)S(1)}, u32[]{:S(2)}, u32[]{:S(2)}) %all-to-all-start.1) | async-done | bytes 1441824 | tf_op jit(solution)/shard_map/all_to_all | solution.py:83
  120.2 0.4 reshape.138
  120.6 2.3 %gather_fusion.1 = bf16[256,2048]{1,0:T(8,128)(2,1)} fusion(bf16[352,2048]{1,0:T(8,128)(2,1)S(1)} %reshape.138, s32[1024]{0:T(1024)S(1)} %pad_clamp_fusion), kind=kCustom, calls=%fused_computation.1 | custom fusion | bytes 2098176 | tf_op jit(solution)/shard_map/gather | solution.py:85
  123.0 2.4 %reshape.139 = f32[128,2,2048]{2,1,0:T(2,128)S(1)} reshape(bf16[256,2048]{1,0:T(8,128)(2,1)} %gather_fusion.1) | data formatting | bytes 3145728 | tf_op jit(solution)/shard_map/convert_element_type | solution.py:85
  125.4 4.1 %multiply_reduce_fusion = f32[128,2048]{1,0:T(8,128)} fusion(f32[128,2,2048]{2,1,0:T(2,128)S(1)} %reshape.139, f32[128,2]{1,0:T(8,128)S(1)} %copy-done.1), kind=kLoop, calls=%fused_computation.14 | loop fusion | flops 786432 | bytes 3146752 | tf_op jit(solution)/shard_map/reduce_sum | solution.py:86
  129.4 52.3 %all-gather.9.cloned.1.call-done = bf16[2048,256]{1,0:T(8,128)(2,1)} async-done(((bf16[128,256]{1,0:T(8,128)(2,1)}), bf16[2048,256]{1,0:T(8,128)(2,1)}) %all-gather.9.cloned.1.call-update) | async-done | bytes 1048592 | tf_op jit(solution)/shard_map/all_gather | solution.py:88
  181.7 3.6 %fusion.5 = bf16[128,2048]{1,0:T(8,128)(2,1)} fusion(f32[128,2048]{1,0:T(8,128)} %multiply_reduce_fusion, bf16[2048,256]{1,0:T(8,128)(2,1)} %all-gather.11.cloned.1.call-done, f32[2048]{0:T(1024)S(1)} %add_divide_fusion, bf16[128,2048]{1,0:T(8,128)(2,1)S(1)} %fusion.17, bf16[2048,256]{1,0:T(8,128)(2,1)} %all-gather.9.cloned.1.call-done), kind=kOutput, calls=%fused_computation.11 | convolution fusion | flops 269385728 | bytes 4202496 | tf_op jit(solution)/shard_map/dot_general | solution.py:94
  (36 shorter events, 1.0 us)
Async XLA Ops:
  6.5 50.8 %all-gather.15.cloned.1.call-start = ((), (), s32[]{:S(2)}) async-start(), calls=%async_computation.5 | async-start | bytes 6291456 | tf_op jit(solution)/shard_map/all_gather | solution.py:65
  7.3 55.0 %all-gather.13.cloned.1.call-start = ((), (), s32[]{:S(2)}) async-start(), calls=%async_computation.4 | async-start | bytes 6291456 | tf_op jit(solution)/shard_map/all_gather | solution.py:66
  8.0 0.8 copy-start.4
  8.0 1.4 copy-start
  8.0 1.6 copy-start.2
  8.0 58.8 %all-gather.17.cloned.1.call-start = ((), (), s32[]{:S(2)}) async-start(), calls=%async_computation.6 | async-start | bytes 6291456 | tf_op jit(solution)/shard_map/all_gather | solution.py:67
  14.4 42.4 %all-to-all-start = ((bf16[16,22,2048]{2,1,0:T(8,128)(2,1)}), bf16[16,22,2048]{2,1,0:T(8,128)(2,1)S(1)}, u32[]{:S(2)}, u32[]{:S(2)}) async-start(bf16[16,22,2048]{2,1,0:T(8,128)(2,1)} %broadcast_select_fusion), calls=%async_computation | async-start | bytes 3145728 | tf_op jit(solution)/shard_map/all_to_all | solution.py:69
  22.7 106.7 %all-gather.11.cloned.1.call-start = ((), (), s32[]{:S(2)}) async-start(), calls=%async_computation.3 | async-start | bytes 1114112 | tf_op jit(solution)/shard_map/all_gather | solution.py:89
  66.8 2.8 %copy-start.6 = (bf16[1,1024,2048]{2,1,0:T(8,128)(2,1)S(1)}, bf16[1,1024,2048]{2,1,0:T(8,128)(2,1)}, u32[]{:S(2)}) copy-start(bf16[1,1024,2048]{2,1,0:T(8,128)(2,1)} %all-gather.17.cloned.1.call-done) | copy-start | bytes 12582916
  72.5 8.8 %copy-start.5 = (f32[128,2]{0,1:T(2,128)S(1)}, f32[128,2]{0,1:T(2,128)}, u32[]{:S(2)}) copy-start(f32[128,2]{0,1:T(2,128)} %param.13) | copy-start | bytes 3076
  72.5 9.5 %copy-start.3 = (f32[2048]{0:T(1024)S(1)}, f32[2048]{0:T(1024)}, u32[]{:S(2)}) copy-start(f32[2048]{0:T(1024)} %param.19) | copy-start | bytes 24580
  72.5 47.7 %all-to-all-start.1 = ((bf16[16,22,2048]{2,1,0:T(8,128)(2,1)}), bf16[16,22,2048]{2,1,0:T(8,128)(2,1)S(1)}, u32[]{:S(2)}, u32[]{:S(2)}) async-start(bf16[16,22,2048]{2,1,0:T(8,128)(2,1)} %reshape.137), calls=%async_computation.1 | async-start | bytes 3145728 | tf_op jit(solution)/shard_map/all_to_all | solution.py:83
  80.4 101.3 %all-gather.9.cloned.1.call-start = ((), (), s32[]{:S(2)}) async-start(), calls=%async_computation.2 | async-start | bytes 1114112 | tf_op jit(solution)/shard_map/all_gather | solution.py:88
  123.0 2.4 %copy-start.1 = (f32[128,2]{1,0:T(8,128)S(1)}, f32[128,2]{1,0:T(8,128)}, u32[]{:S(2)}) copy-start(f32[128,2]{1,0:T(8,128)} %copy.17) | copy-start | bytes 3076
Sparse Core Ops, SparseCore 0:
  8.9 16.3 all-gather.14
  26.8 14.8 all-gather.12
  43.3 14.8 all-gather.16
  60.8 63.4 all-gather.10
  126.8 54.8 all-gather.8
where the time goes:
time: 192 us
  waiting for transfers between devices  127 us (66%)
  matrix products  16.8 us (9%)
  starting transfers between devices  16.6 us (9%)
  between operations  13.4 us (7%)
  local copies, waits for them, and re-layouts  11.4 us (6%)
  other arithmetic  6.7 us (3%)
    all_gather x1, waiting for transfers between devices, shards(): lax.all_gather(dense_in, 'ep', axis=0, tiled=True)  52.3 us
    all_to_all x1, waiting for transfers between devices, shards(): lax.all_to_all(expert_out, 'ep', split_axis=0, concat_axis=0, tiled=True)  38.2 us
    all_to_all x1, waiting for transfers between devices, shards(): lax.all_to_all(buffer, 'ep', split_axis=0, concat_axis=0, tiled=True)  33.5 us
    all_to_all x1, starting transfers between devices, shards(): lax.all_to_all(buffer, 'ep', split_axis=0, concat_axis=0, tiled=True)  8.34 us
    all_to_all x1, starting transfers between devices, shards(): lax.all_to_all(expert_out, 'ep', split_axis=0, concat_axis=0, tiled=True)  7.9 us
    dot_general x1, matrix products, shards(): jnp.dot(flat_rows, gate_w, preferred_element_type=jnp.float32)  5 us
    dot_general x1, matrix products, shards(): jnp.dot(flat_rows, up_w, preferred_element_type=jnp.float32)  4.48 us
    reduce_sum x1, other arithmetic, shards(): weighted = jnp.sum(picked * route_weights[:, :, None], axis=1)  4.05 us
  transfers between devices with their start and end apart: 7, of which 3 were waited for; matrix products, arithmetic and copies ran while one was open for 16% of the time, Pallas kernels for 0%

commit v1 on v0

--- a/solution.py
+++ b/solution.py
@@ -1,11 +1,23 @@
+import math
+
 import jax
 import jax.numpy as jnp
 from jax import lax
+from jax.experimental import pallas as pl
+from jax.experimental.pallas import tpu as pltpu
 from jax.sharding import PartitionSpec as P
+
 
 CLAMP_LIMIT = 7.0
 SLOPE_ALPHA = 1.702
 NORM_EPS = 1e-06
+VMEM = pl.BlockSpec(memory_space=pltpu.VMEM)
+HBM = pl.BlockSpec(memory_space=pltpu.HBM)
+LIMIT = 40 * 1024 * 1024
+
+
+def capacity_of(tok_rows, top_count, experts):
+    return (4 * tok_rows * top_count + 3 * experts - 1) // (3 * experts)
 
 
 def rms_normed(tokens, norm_gain):
@@ -22,6 +34,382 @@
     )
 
 
+def position():
+    return lax.axis_index("ep").astype(jnp.int32), lax.axis_index("tp").astype(jnp.int32)
+
+
+def row_split(capacity, width):
+    pieces = 8 // math.gcd(capacity, 8)
+    return pieces if width % (128 * pieces) == 0 else 1
+
+
+def position():
+    return lax.axis_index("ep").astype(jnp.int32), lax.axis_index("tp").astype(jnp.int32)
+
+
+def row_split(capacity, width):
+    pieces = 8 // math.gcd(capacity, 8)
+    return pieces if width % (128 * pieces) == 0 else 1
+
+
+def position():
+    return lax.axis_index("ep").astype(jnp.int32), lax.axis_index("tp").astype(jnp.int32)
+
+
+def row_split(capacity, width):
+    pieces = 8 // math.gcd(capacity, 8)
+    return pieces if width % (128 * pieces) == 0 else 1
+
+
+def expert_column(plan):
+    me, core = position()
+    block = lax.broadcasted_iota(jnp.int32, (len(plan), 1), 0)
+    column = jnp.zeros((len(plan), 1), jnp.int32)
+    for m, (first, second) in enumerate(plan):
+        column = jnp.where(block == m, jnp.where(core == 0, first, second), column)
+    return jnp.bitwise_xor(column, me)
+
+
+def choice_masks(routes, expert):
+    return [routes[c : c + 1, :] == expert for c in range(routes.shape[0])]
+
+
+def slot_ranks(routes, expert):
+    tokens = routes.shape[1]
+    chosen = sum(jnp.where(mask, 1.0, 0.0) for mask in choice_masks(routes, expert))
+    earlier = lax.broadcasted_iota(jnp.int32, (tokens, tokens), 0) < lax.broadcasted_iota(
+        jnp.int32, (tokens, tokens), 1
+    )
+    counted = jnp.dot(
+        chosen.astype(jnp.bfloat16),
+        jnp.where(earlier, 1.0, 0.0).astype(jnp.bfloat16),
+        preferred_element_type=jnp.float32,
+    )
+    return jnp.where(chosen > 0.0, counted, -1.0)
+
+
+def block_rows(capacity, pieces):
+    row = lax.broadcasted_iota(jnp.int32, (capacity * pieces, 1), 0)
+    piece = sum((row >= h * capacity).astype(jnp.int32) for h in range(1, pieces)) + 0 * row
+    return piece, (row - piece * capacity).astype(jnp.float32)
+
+
+def load_kernel(tok_ref, gain_ref, route_ref, rate_ref, in_ref, out_ref, held_ref, norm_ref,
+                gain_v, route_v, rate_v, tok_v, sems):
+    _, core = position()
+    pairs = ((tok_ref, tok_v), (gain_ref, gain_v), (route_ref, route_v), (rate_ref, rate_v))
+    copies = [pltpu.make_async_copy(a, b, sems.at[i]) for i, (a, b) in enumerate(pairs)]
+    for copy in copies:
+        copy.start()
+    last = sems.at[len(pairs)]
+
+    @pl.when(core == 0)
+    def _():
+        pltpu.make_async_copy(in_ref, held_ref, last).start()
+
+    @pl.when(core != 0)
+    def _():
+        pltpu.make_async_copy(out_ref, held_ref, last).start()
+
+    for copy in copies:
+        copy.wait()
+    norm_ref[...] = rms_normed(tok_v[...], gain_v[...])
+    pltpu.make_async_copy(in_ref, held_ref, last).wait()
+
+
+def pack_kernel(capacity, plan, own_ref, tok2_ref, gain_ref, route_ref, route2_ref,
+                norm_ref, *send_refs):
+    half = own_ref.shape[0]
+    rows, part = send_refs[0].shape
+    pieces = rows // capacity
+    norm_ref[:half, :] = own_ref[...]
+    norm_ref[half:, :] = rms_normed(tok2_ref[...], gain_ref[...])
+    routes = jnp.concatenate([route_ref[...], route2_ref[...]], axis=1)
+    ranks = slot_ranks(routes, expert_column(plan))
+    piece, slot = block_rows(capacity, pieces)
+    packed = None
+    for h in range(pieces):
+        select = jnp.concatenate(
+            [
+                jnp.where((ranks[m : m + 1, :] == slot) & (piece == h), 1.0, 0.0)
+                for m in range(len(send_refs))
+            ],
+            axis=0,
+        ).astype(jnp.bfloat16)
+        term = jnp.dot(
+            select, norm_ref[:, h * part : (h + 1) * part], preferred_element_type=jnp.float32
+        )
+        packed = term if packed is None else packed + term
+    packed = packed.astype(jnp.bfloat16)
+    for m, send_ref in enumerate(send_refs):
+        send_ref[...] = packed[m * rows : (m + 1) * rows, :]
+
+
+def whole_rows(block, capacity, padded):
+    rows = block.shape[0]
+    pieces = rows // capacity
+    if pieces == 1:
+        return block
+    wide = block.astype(jnp.float32)
+    parts = [wide[:padded]] + [
+        pltpu.roll(wide, rows - h * capacity, 0)[:padded] for h in range(1, pieces)
+    ]
+    return jnp.concatenate(parts, axis=1).astype(jnp.bfloat16)
+
+
+def split_rows(values, capacity, pieces):
+    if pieces == 1:
+        return values
+    rows, part = capacity * pieces, values.shape[1] // pieces
+    piece, _ = block_rows(capacity, pieces)
+    filler = jnp.zeros((rows - values.shape[0], part), values.dtype)
+    block = None
+    for h in range(pieces):
+        each = jnp.concatenate([values[:, h * part : (h + 1) * part], filler], axis=0)
+        block = each if h == 0 else jnp.where(piece == h, pltpu.roll(each, h * capacity, 0), block)
+    return block
+
+
+def expert_kernel(count, capacity, *refs):
+    row_refs, refs = refs[:count], refs[count:]
+    (gate0, up0, down0, gate1, up1, down1), out_refs = refs[:6], refs[6:]
+    pieces = row_refs[0].shape[0] // capacity
+    padded = -(-capacity // 8) * 8
+    flat = jnp.concatenate([whole_rows(r[...], capacity, padded) for r in row_refs], axis=0)
+    total = None
+    for gate_ref, up_ref, down_ref in ((gate0, up0, down0), (gate1, up1, down1)):
+        hidden = clamped_unit(
+            jnp.dot(flat, gate_ref[...], preferred_element_type=jnp.float32),
+            jnp.dot(flat, up_ref[...], preferred_element_type=jnp.float32),
+        )
+        part = jnp.dot(hidden, down_ref[...], preferred_element_type=jnp.float32)
+        part = part.astype(jnp.bfloat16).astype(jnp.float32)
+        total = part if total is None else total + part
+    for k in range(count):
+        values = total[k * padded : (k + 1) * padded, :]
+        out_refs[k][...] = split_rows(values, capacity, pieces).astype(jnp.bfloat16)
+
+
+def weigh_kernel(capacity, pieces, plan, early, route_ref, route2_ref, rate_ref, rate2_ref,
+                 *out_refs):
+    routes = jnp.concatenate([route_ref[...], route2_ref[...]], axis=1)
+    weights = jnp.concatenate([rate_ref[...], rate2_ref[...]], axis=1)
+    expert = expert_column(plan)
+    ranks = slot_ranks(routes, expert)
+    scale = sum(
+        jnp.where(mask, weights[c : c + 1, :], 0.0)
+        for c, mask in enumerate(choice_masks(routes, expert))
+    )
+    piece, slot = block_rows(capacity, pieces)
+    tokens = routes.shape[1]
+    tables = [
+        jnp.where(ranks[m : m + 1, :] == slot, scale[m : m + 1, :], 0.0) for m in range(len(plan))
+    ]
+    for group, (high_ref, low_ref) in zip(
+        (tables[:early], tables[early:]), (out_refs[:2], out_refs[2:])
+    ):
+        for h in range(pieces):
+            table = jnp.concatenate([jnp.where(piece == h, t, 0.0) for t in group], axis=0).T
+            high = table.astype(jnp.bfloat16)
+            high_ref[h * tokens : (h + 1) * tokens, :] = high
+            low_ref[h * tokens : (h + 1) * tokens, :] = (
+                table - high.astype(jnp.float32)
+            ).astype(jnp.bfloat16)
+
+
+def join_kernel(*refs):
+    at = 0
+    for ref in refs[:-1]:
+        refs[-1][at : at + ref.shape[0], :] = ref[...]
+        at += ref.shape[0]
+
+
+def shards_of(order, refs):
+    place = 0
+    shard = sum(r.shape[0] for r in refs) // len(order)
+    for ref in refs:
+        for at in range(0, ref.shape[0], shard):
+            yield shard, order[place], ref, at
+            place += 1
+
+
+def hidden_kernel(order, norm_ref, *refs):
+    held_refs, out_ref = refs[:-1], refs[-1]
+    me, core = position()
+
+    @pl.when(core == 0)
+    def _():
+        total = None
+        for shard, offset, ref, at in shards_of(order, held_refs):
+            source = pl.multiple_of(jnp.bitwise_xor(me, offset) * shard, shard)
+            part = jnp.dot(
+                norm_ref[:, pl.ds(source, shard)],
+                ref[at : at + shard, :],
+                preferred_element_type=jnp.float32,
+            )
+            total = part if total is None else total + part
+        out_ref[...] = (total / (1.0 + jnp.exp(-total))).astype(jnp.bfloat16)
+
+    @pl.when(core != 0)
+    def _():
+        out_ref[...] = jnp.zeros_like(out_ref)
+
+
+def gather_into(out_ref, start_ref, row_refs, high_ref, low_ref):
+    flat = jnp.concatenate([r[...] for r in row_refs], axis=0)
+    tokens, part = out_ref.shape[0], flat.shape[1]
+    for h in range(out_ref.shape[1] // part):
+        at = slice(h * tokens, (h + 1) * tokens)
+        value = jnp.dot(high_ref[at, :], flat, preferred_element_type=jnp.float32)
+        value = value + jnp.dot(low_ref[at, :], flat, preferred_element_type=jnp.float32)
+        lanes = slice(h * part, (h + 1) * part)
+        out_ref[:, lanes] = value if start_ref is None else value + start_ref[:, lanes]
+
+
+def early_kernel(order, held_count, high_ref, low_ref, hid_ref, dgate_ref, *refs):
+    held_refs, row_refs, out_ref = refs[:held_count], refs[held_count:-1], refs[-1]
+    me, core = position()
+    gather_into(out_ref, None, row_refs, high_ref, low_ref)
+
+    @pl.when(core != 0)
+    def _():
+        half = hid_ref.shape[0] // 2
+        hid = jnp.concatenate([hid_ref[half:, :], hid_ref[:half, :]], axis=0)
+        for shard, offset, ref, at in shards_of(order, held_refs):
+            lanes = pl.ds(pl.multiple_of(jnp.bitwise_xor(me, offset) * shard, shard), shard)
+            branch = lax.dot_general(
+                hid,
+                ref[at : at + shard, :],
+                (((1,), (1,)), ((), ())),
+                preferred_element_type=jnp.float32,
+            )
+            out_ref[:, lanes] += jax.nn.sigmoid(dgate_ref[:, lanes]) * branch
+
+
+def late_kernel(early_ref, high_ref, low_ref, *refs):
+    row_refs, own_ref, other_ref, sum_ref = refs[:-3], refs[-3], refs[-2], refs[-1]
+    half = own_ref.shape[0]
+    gather_into(sum_ref, early_ref, row_refs, high_ref, low_ref)
+    own_ref[...] = sum_ref[:half, :]
+    other_ref[...] = sum_ref[half:, :].astype(jnp.bfloat16)
+
+
+def call(kernel, outs, ins, scratch=(), spec=VMEM):
+    return pl.pallas_call(
+        kernel,
+        out_shape=outs,
+        in_specs=[spec for _ in ins],
+        out_specs=jax.tree.map(lambda _: VMEM, outs),
+        scratch_shapes=list(scratch),
+        compiler_params=pltpu.CompilerParams(vmem_limit_bytes=LIMIT),
+    )(*ins)
+
+
+def swapped(value, offsets):
+    size = lax.axis_size("ep")
+    pairs = [(2 * i + c, 2 * (i ^ offsets[c]) + c) for i in range(size) for c in range(2)]
+    return lax.ppermute(value, ("ep", "tp"), pairs)
+
+
+def partners(value):
+    return lax.ppermute(value, "tp", [(0, 1), (1, 0)])
+
+
+def plan_of(sources):
+    half = sources // 2
+    far = [(k, k + 1) for k in range(half, sources, 2)]
+    near = [(k, k + 1) for k in range(0, half, 2)]
+    cut = len(far) // 2
+    return far[:cut] + near[1:] + near[:1] + far[cut:], cut, len(near)
+
+
+def bits_of(sources):
+    return [1 << b for b in range(sources.bit_length() - 2, 1, -1)]
+
+
+def direct_shards(
+    tokens, norm_gain, routes, route_weights, w_gate, w_up, w_down, dense_in, dense_out, dense_gate
+):
+    tok_rows, width = tokens.shape
+    sources = lax.axis_size("ep")
+    capacity = 2 * capacity_of(tok_rows, routes.shape[1], sources)
+    pieces = row_split(capacity, width)
+    bf16, f32 = jnp.bfloat16, jnp.float32
+    shape = jax.ShapeDtypeStruct
+    plan, cut, near = plan_of(sources)
+    blocks = len(plan)
+    early = cut + near
+    groups = (range(cut, early), range(cut), range(early, blocks))
+
+    gain = norm_gain.reshape(1, width)
+    routes, rates = routes.T, route_weights.T
+    tokens2 = partners(tokens)
+    routes2 = partners(routes)
+    rates2 = partners(rates)
+    own = (w_gate[0], w_up[0], w_down[0])
+    other = tuple(partners(w) for w in own)
+
+    inputs = (tokens, gain, routes, rates)
+    held, norm_own, gain, routes, rates = call(
+        load_kernel,
+        tuple(shape(v.shape, v.dtype) for v in (dense_in,) + inputs),
+        inputs + (dense_in, dense_out),
+        scratch=(pltpu.VMEM(tokens.shape, bf16), pltpu.SemaphoreType.DMA((5,))),
+        spec=HBM,
+    )
+    block = shape((capacity * pieces, width // pieces), bf16)
+    normed, *sends = call(
+        lambda *r: pack_kernel(capacity, plan, *r),
+        (shape((2 * tok_rows, width), bf16),) + (block,) * blocks,
+        (norm_own, tokens2, gain, routes, routes2),
+    )
+    got = [swapped(sends[m], plan[m]) for m in range(blocks)]
+
+    order = [0]
+    for bit in bits_of(sources):
+        more = swapped(held, (bit, bit))
+        held = call(join_kernel, shape((2 * held.shape[0], held.shape[1]), bf16), (held, more))
+        order = order + [k ^ bit for k in order]
+    helds = (held,) + tuple(swapped(held, (k, k)) for k in (1, 2, 3))
+    order = [k ^ j for j in range(4) for k in order]
+
+    columns = (early * block.shape[0], (blocks - early) * block.shape[0])
+    high0, low0, high1, low1 = call(
+        lambda *r: weigh_kernel(capacity, pieces, plan, early, *r),
+        tuple(shape((2 * tok_rows * pieces, n), bf16) for n in columns for _ in range(2)),
+        (routes, routes2, rates, rates2),
+    )
+    dense_hidden = call(
+        lambda *r: hidden_kernel(order, *r),
+        shape((2 * tok_rows, dense_in.shape[1]), bf16),
+        (normed,) + helds,
+    )
+    dense_hidden = partners(dense_hidden)
+    back = {}
+    for group in groups:
+        outs = call(
+            lambda *r, c=len(group): expert_kernel(c, capacity, *r),
+            (block,) * len(group),
+            tuple(got[m] for m in group) + own + other,
+        )
+        for m, value in zip(group, outs):
+            back[m] = swapped(value, plan[m])
+    sum0 = call(
+        lambda *r: early_kernel(order, len(helds), *r),
+        shape((2 * tok_rows, width), f32),
+        (high0, low0, dense_hidden, dense_gate.reshape(1, width))
+        + helds
+        + tuple(back[m] for m in range(early)),
+    )
+    total, share = call(
+        late_kernel,
+        (shape((tok_rows, width), f32), shape((tok_rows, width), bf16)),
+        (sum0, high1, low1) + tuple(back[m] for m in range(early, blocks)),
+        scratch=(pltpu.VMEM((2 * tok_rows, width), f32),),
+    )
+    return (total + partners(share).astype(f32)).astype(bf16)
+
+
 def rounded_term(hidden_rows, down_rows):
     partial_value = jnp.dot(hidden_rows, down_rows, preferred_element_type=jnp.float32).astype(
         jnp.bfloat16
@@ -29,7 +417,7 @@
     return lax.optimization_barrier(partial_value).astype(jnp.float32)
 
 
-def shards(
+def general_shards(
     tokens, norm_gain, routes, route_weights, w_gate, w_up, w_down, dense_in, dense_out, dense_gate
 ):
     tok_rows, model_width = tokens.shape
@@ -37,7 +425,7 @@
     sources = lax.axis_size("ep")
     experts = sources * w_gate.shape[0]
     core_count = lax.axis_size("tp")
-    capacity = (4 * tok_rows * top_count + 3 * experts - 1) // (3 * experts)
+    capacity = capacity_of(tok_rows, top_count, experts)
     entries = tok_rows * top_count
     normed = rms_normed(tokens, norm_gain)
     flat_routes = routes.reshape(entries)
@@ -58,13 +446,10 @@
         filled[:, None], normed[source_entry // top_count], jnp.zeros((), jnp.bfloat16)
     )
     buffer = buffer.reshape(experts, capacity, model_width)
-    gate_w = w_gate[0]
-    up_w = w_up[0]
-    down_w = w_down[0]
     gate_w, up_w, down_w = (
-        lax.all_gather(gate_w, "tp", axis=1, tiled=True),
-        lax.all_gather(up_w, "tp", axis=1, tiled=True),
-        lax.all_gather(down_w, "tp", axis=0, tiled=True),
+        lax.all_gather(w_gate[0], "tp", axis=1, tiled=True),
+        lax.all_gather(w_up[0], "tp", axis=1, tiled=True),
+        lax.all_gather(w_down[0], "tp", axis=0, tiled=True),
     )
     received = lax.all_to_all(buffer, "ep", split_axis=0, concat_axis=0, tiled=True)
     slot_count = received.shape[1]
@@ -110,6 +495,28 @@
         P("ep", None),
         P(),
     )
-    return jax.shard_map(
-        shards, mesh=mesh, in_specs=placed, out_specs=P(("ep", "tp"), None), check_vma=False
-    )
+    sources = mesh.shape["ep"]
+
+    def is_direct(tokens, routes, w_gate, dense_in):
+        capacity = capacity_of(tokens.shape[0] // mesh.size, routes.shape[1], sources)
+        return (
+            sources >= 8
+            and sources & (sources - 1) == 0
+            and mesh.shape["tp"] == 2
+            and w_gate.shape[0] == sources
+            and capacity >= 8
+            and dense_in.shape[0] % (128 * sources) == 0
+        )
+
+    def mapped(shards):
+        return jax.shard_map(
+            shards, mesh=mesh, in_specs=placed, out_specs=P(("ep", "tp"), None), check_vma=False
+        )
+
+    def step(*arrays):
+        tokens, routes, w_gate, dense_in = arrays[0], arrays[2], arrays[4], arrays[7]
+        if is_direct(tokens, routes, w_gate, dense_in):
+            return mapped(direct_shards)(*arrays)
+        return mapped(general_shards)(*arrays)
+
+    return step

time: 192 us -> 124 us (0.65)
  the two profiles are of different devices: /device:TPU:0 before, /device:TPU:9 now
where the time goes in v1:
time: 124 us
  waiting for transfers between devices  61.9 us (50%)
  starting transfers between devices  41 us (33%)
  Pallas kernels  14 us (11%)
  local copies, waits for them, and re-layouts  5.71 us (5%)
    ppermute x21, waiting for transfers between devices, swapped(): return lax.ppermute(value, ('ep', 'tp'), pairs)  59 us
    ppermute x21, starting transfers between devices, swapped(): return lax.ppermute(value, ('ep', 'tp'), pairs)  36.3 us
    pallas_call x11, Pallas kernels, call(): pl.pallas_call(kernel, out_shape=outs, in_specs=[spec for _ in ins], out_...  14 us
    unnamed x20, local copies, waits for them, and re-layouts  5.71 us
    ppermute x8, starting transfers between devices, partners(): return lax.ppermute(value, 'tp', [(0, 1), (1, 0)])  4.7 us
    ppermute x8, waiting for transfers between devices, partners(): return lax.ppermute(value, 'tp', [(0, 1), (1, 0)])  2.92 us
  transfers between devices with their start and end apart: 29, of which 13 were waited for; matrix products, arithmetic and copies ran while one was open for 0% of the time, Pallas kernels for 11%

profile of v1, /device:TPU:9, one launch (start us, length us, event | category | flops | bytes accessed | tf_op | source)
XLA Modules:
  0.0 123.8 jit_solution(12902844248244921694)
XLA Ops:
  6.5 2.4 %collective-permute-start.3 = (bf16[128,256]{1,0:T(8,128)(2,1)S(1)}, bf16[128,256]{1,0:T(8,128)(2,1)S(1)}, u32[]{:S(2)}, u32[]{:S(2)}) collective-permute-start(bf16[128,256]{1,0:T(8,128)(2,1)S(1)} %get-tuple-element.40.refs_0_), channel_id=1, source_target_pairs={{0,16},{1,17},{2,18},{3,19},{4,20},{5,21},{6,22},{7,23},{8,24},{9,... | collective-permute-start | bytes 196616 | tf_op jit(solution)/shard_map/ppermute | solution.py:311
  8.8 3.2 %collective-permute-done.3.refs_1_ = bf16[128,256]{1,0:T(8,128)(2,1)S(1)} collective-permute-done((bf16[128,256]{1,0:T(8,128)(2,1)S(1)}, bf16[128,256]{1,0:T(8,128)(2,1)S(1)}, u32[]{:S(2)}, u32[]{:S(2)}) %collective-permute-start.3) | collective-permute-done | bytes 65568 | tf_op jit(solution)/shard_map/ppermute | solution.py:311
  13.8 2.8 %collective-permute-done.4.refs_1_ = bf16[256,256]{1,0:T(8,128)(2,1)S(1)} collective-permute-done((bf16[256,256]{1,0:T(8,128)(2,1)S(1)}, bf16[256,256]{1,0:T(8,128)(2,1)S(1)}, u32[]{:S(2)}, u32[]{:S(2)}) %collective-permute-start.4) | collective-permute-done | bytes 131104 | tf_op jit(solution)/shard_map/ppermute | solution.py:311
  16.7 1.3 %collective-permute-start = (s32[2,128]{1,0:T(2,128)}, s32[2,128]{1,0:T(2,128)S(1)}, u32[]{:S(2)}, u32[]{:S(2)}) collective-permute-start(s32[2,128]{1,0:T(2,128)} %bitcast.1.route_ref), channel_id=1, source_target_pairs={{0,1},{1,0},{2,3},{3,2},{4,5},{5,4},{6,7},{7,6},{8,9},{9,8},{10,11... | collective-permute-start | bytes 3080 | tf_op jit(solution)/shard_map/ppermute | solution.py:315
  19.0 2.2 %collective-permute-start.7 = (bf16[512,256]{1,0:T(8,128)(2,1)S(1)}, bf16[512,256]{1,0:T(8,128)(2,1)S(1)}, u32[]{:S(2)}, u32[]{:S(2)}) collective-permute-start(bf16[512,256]{1,0:T(8,128)(2,1)S(1)} %shard_map.104.r_1_.r_4_), channel_id=1, source_target_pairs={{0,6},{1,7},{2,4},{3,5},{4,2},{5,3},{6,0},{7,1},{8,14},{9,15},{10,... | collective-permute-start | bytes 786440 | tf_op jit(solution)/shard_map/ppermute | solution.py:311
  21.2 6.3 %collective-permute-done.7.r_4_.r_7_ = bf16[512,256]{1,0:T(8,128)(2,1)S(1)} collective-permute-done((bf16[512,256]{1,0:T(8,128)(2,1)S(1)}, bf16[512,256]{1,0:T(8,128)(2,1)S(1)}, u32[]{:S(2)}, u32[]{:S(2)}) %collective-permute-start.7) | collective-permute-done | bytes 262176 | tf_op jit(solution)/shard_map/ppermute | solution.py:311
  27.4 1.2 %collective-permute-start.6 = (bf16[512,256]{1,0:T(8,128)(2,1)S(1)}, bf16[512,256]{1,0:T(8,128)(2,1)S(1)}, u32[]{:S(2)}, u32[]{:S(2)}) collective-permute-start(bf16[512,256]{1,0:T(8,128)(2,1)S(1)} %shard_map.104.r_1_.r_4_), channel_id=1, source_target_pairs={{0,4},{1,5},{2,6},{3,7},{4,0},{5,1},{6,2},{7,3},{8,12},{9,13},{10,... | collective-permute-start | bytes 786440 | tf_op jit(solution)/shard_map/ppermute | solution.py:311
  28.7 1.2 collective-permute-start.5
  31.0 3.0 %collective-permute-done.6.r_3_.r_6_ = bf16[512,256]{1,0:T(8,128)(2,1)S(1)} collective-permute-done((bf16[512,256]{1,0:T(8,128)(2,1)S(1)}, bf16[512,256]{1,0:T(8,128)(2,1)S(1)}, u32[]{:S(2)}, u32[]{:S(2)}) %collective-permute-start.6) | collective-permute-done | bytes 262176 | tf_op jit(solution)/shard_map/ppermute | solution.py:311
  34.1 4.0 %collective-permute-start.9 = (bf16[88,1024]{1,0:T(8,128)(2,1)S(1)}, bf16[88,1024]{1,0:T(8,128)(2,1)S(1)}, u32[]{:S(2)}, u32[]{:S(2)}) collective-permute-start(bf16[88,1024]{1,0:T(8,128)(2,1)S(1)} %get-tuple-element.41), channel_id=1, source_target_pairs={{0,16},{1,19},{2,18},{3,17},{4,20},{5,23},{6,22},{7,21},{8,24},{9,... | collective-permute-start | bytes 540680 | tf_op jit(solution)/shard_map/ppermute | solution.py:311
  39.1 10.8 %collective-permute-done.9.r_0_ = bf16[88,1024]{1,0:T(8,128)(2,1)S(1)} collective-permute-done((bf16[88,1024]{1,0:T(8,128)(2,1)S(1)}, bf16[88,1024]{1,0:T(8,128)(2,1)S(1)}, u32[]{:S(2)}, u32[]{:S(2)}) %collective-permute-start.9) | collective-permute-done | bytes 180256 | tf_op jit(solution)/shard_map/ppermute | solution.py:311
  49.8 1.2 collective-permute-start.16
  51.0 2.6 %collective-permute-done.10.r_1_ = bf16[88,1024]{1,0:T(8,128)(2,1)S(1)} collective-permute-done((bf16[88,1024]{1,0:T(8,128)(2,1)S(1)}, bf16[88,1024]{1,0:T(8,128)(2,1)S(1)}, u32[]{:S(2)}, u32[]{:S(2)}) %collective-permute-start.10) | collective-permute-done | bytes 180256 | tf_op jit(solution)/shard_map/ppermute | solution.py:311
  53.7 3.1 %collective-permute-start.17 = (bf16[88,1024]{1,0:T(8,128)(2,1)S(1)}, bf16[88,1024]{1,0:T(8,128)(2,1)S(1)}, u32[]{:S(2)}, u32[]{:S(2)}) collective-permute-start(bf16[88,1024]{1,0:T(8,128)(2,1)S(1)} %get-tuple-element.46), channel_id=1, source_target_pairs={{0,8},{1,11},{2,10},{3,9},{4,12},{5,15},{6,14},{7,13},{8,0},{9,3},... | collective-permute-start | bytes 540680 | tf_op jit(solution)/shard_map/ppermute | solution.py:311
  56.8 1.3 %collective-permute-start.18 = (bf16[88,1024]{1,0:T(8,128)(2,1)S(1)}, bf16[88,1024]{1,0:T(8,128)(2,1)S(1)}, u32[]{:S(2)}, u32[]{:S(2)}) collective-permute-start(bf16[88,1024]{1,0:T(8,128)(2,1)S(1)} %get-tuple-element.47), channel_id=1, source_target_pairs={{0,12},{1,15},{2,14},{3,13},{4,8},{5,11},{6,10},{7,9},{8,4},{9,7},... | collective-permute-start | bytes 540680 | tf_op jit(solution)/shard_map/ppermute | solution.py:311
  58.1 2.2 %collective-permute-start.19 = (bf16[88,1024]{1,0:T(8,128)(2,1)S(1)}, bf16[88,1024]{1,0:T(8,128)(2,1)S(1)}, u32[]{:S(2)}, u32[]{:S(2)}) collective-permute-start(bf16[88,1024]{1,0:T(8,128)(2,1)S(1)} %get-tuple-element.48), channel_id=1, source_target_pairs={{0,0},{1,3},{2,2},{3,1},{4,4},{5,7},{6,6},{7,5},{8,8},{9,11},{10,1... | collective-permute-start | bytes 540680 | tf_op jit(solution)/shard_map/ppermute | solution.py:311
  61.6 1.6 %copy-done.2 = bf16[1,512,2048]{2,1,0:T(8,128)(2,1)S(1)} copy-done((bf16[1,512,2048]{2,1,0:T(8,128)(2,1)S(1)}, bf16[1,512,2048]{2,1,0:T(8,128)(2,1)}, u32[]{:S(2)}) %copy-start.2) | copy-done | bytes 2097176
  63.2 2.4 %shard_map.106 = (bf16[88,1024]{1,0:T(8,128)(2,1)S(1)}, bf16[88,1024]{1,0:T(8,128)(2,1)S(1)}) custom-call(bf16[88,1024]{1,0:T(8,128)(2,1)S(1)} %collective-permute-done.9.r_0_, bf16[88,1024]{1,0:T(8,128)(2,1)S(1)} %collective-permute-done.10.r_1_, bf16[2048,512]{1,0:T(8,128)(2,1)S(1)} %bitcast.8, bf16[2048,512]{1,0:T(8,128)(2,1)S(1)} %bitcast.12, ...), custom_call_target="tpu_custom_call" | custom-call | tf_op jit(solution)/shard_map/pallas_call | solution.py:298
  65.6 3.1 %collective-permute-start.24 = (bf16[88,1024]{1,0:T(8,128)(2,1)S(1)}, bf16[88,1024]{1,0:T(8,128)(2,1)S(1)}, u32[]{:S(2)}, u32[]{:S(2)}) collective-permute-start(bf16[88,1024]{1,0:T(8,128)(2,1)S(1)} %get-tuple-element.55), channel_id=1, source_target_pairs={{0,24},{1,27},{2,26},{3,25},{4,28},{5,31},{6,30},{7,29},{8,16},{9,... | collective-permute-start | bytes 540680 | tf_op jit(solution)/shard_map/ppermute | solution.py:311
  69.7 3.7 %collective-permute-start.14 = (bf16[88,1024]{1,0:T(8,128)(2,1)S(1)}, bf16[88,1024]{1,0:T(8,128)(2,1)S(1)}, u32[]{:S(2)}, u32[]{:S(2)}) collective-permute-start(bf16[88,1024]{1,0:T(8,128)(2,1)S(1)} %get-tuple-element.43), channel_id=1, source_target_pairs={{0,16},{1,19},{2,18},{3,17},{4,20},{5,23},{6,22},{7,21},{8,24},{9,... | collective-permute-start | bytes 540680 | tf_op jit(solution)/shard_map/ppermute | solution.py:311
  73.4 2.9 %shard_map.107 = (bf16[88,1024]{1,0:T(8,128)(2,1)S(1)}, bf16[88,1024]{1,0:T(8,128)(2,1)S(1)}, bf16[88,1024]{1,0:T(8,128)(2,1)S(1)}, bf16[88,1024]{1,0:T(8,128)(2,1)S(1)}) custom-call(bf16[88,1024]{1,0:T(8,128)(2,1)S(1)} %collective-permute-done.16.r_0_, bf16[88,1024]{1,0:T(8,128)(2,1)S(1)} %collective-permute-done.17.r_1_, ...), custom_call_target="tpu_custom_call" | custom-call | tf_op jit(solution)/shard_map/pallas_call | solution.py:298
  76.4 1.6 %collective-permute-start.20 = (bf16[88,1024]{1,0:T(8,128)(2,1)S(1)}, bf16[88,1024]{1,0:T(8,128)(2,1)S(1)}, u32[]{:S(2)}, u32[]{:S(2)}) collective-permute-start(bf16[88,1024]{1,0:T(8,128)(2,1)S(1)} %get-tuple-element.49), channel_id=1, source_target_pairs={{0,4},{1,7},{2,6},{3,5},{4,0},{5,3},{6,2},{7,1},{8,12},{9,15},{10,... | collective-permute-start | bytes 540680 | tf_op jit(solution)/shard_map/ppermute | solution.py:311
  78.1 10.5 %collective-permute-done.24.r_0_ = bf16[88,1024]{1,0:T(8,128)(2,1)S(1)} collective-permute-done((bf16[88,1024]{1,0:T(8,128)(2,1)S(1)}, bf16[88,1024]{1,0:T(8,128)(2,1)S(1)}, u32[]{:S(2)}, u32[]{:S(2)}) %collective-permute-start.24) | collective-permute-done | bytes 180256 | tf_op jit(solution)/shard_map/ppermute | solution.py:311
  88.6 5.1 %collective-permute-done.25.r_1_ = bf16[88,1024]{1,0:T(8,128)(2,1)S(1)} collective-permute-done((bf16[88,1024]{1,0:T(8,128)(2,1)S(1)}, bf16[88,1024]{1,0:T(8,128)(2,1)S(1)}, u32[]{:S(2)}, u32[]{:S(2)}) %collective-permute-start.25) | collective-permute-done | bytes 180256 | tf_op jit(solution)/shard_map/ppermute | solution.py:311
  93.7 2.2 %collective-permute-done.14.r_8_ = bf16[88,1024]{1,0:T(8,128)(2,1)S(1)} collective-permute-done((bf16[88,1024]{1,0:T(8,128)(2,1)S(1)}, bf16[88,1024]{1,0:T(8,128)(2,1)S(1)}, u32[]{:S(2)}, u32[]{:S(2)}) %collective-permute-start.14) | collective-permute-done | bytes 180256 | tf_op jit(solution)/shard_map/ppermute | solution.py:311
  95.9 2.7 %collective-permute-start.23 = (bf16[88,1024]{1,0:T(8,128)(2,1)S(1)}, bf16[88,1024]{1,0:T(8,128)(2,1)S(1)}, u32[]{:S(2)}, u32[]{:S(2)}) collective-permute-start(bf16[88,1024]{1,0:T(8,128)(2,1)S(1)} %get-tuple-element.52), channel_id=1, source_target_pairs={{0,0},{1,3},{2,2},{3,1},{4,4},{5,7},{6,6},{7,5},{8,8},{9,11},{10,1... | collective-permute-start | bytes 540680 | tf_op jit(solution)/shard_map/ppermute | solution.py:311
  98.6 2.4 %shard_map.109 = (bf16[88,1024]{1,0:T(8,128)(2,1)S(1)}, bf16[88,1024]{1,0:T(8,128)(2,1)S(1)}) custom-call(bf16[88,1024]{1,0:T(8,128)(2,1)S(1)} %collective-permute-done.24.r_0_, bf16[88,1024]{1,0:T(8,128)(2,1)S(1)} %collective-permute-done.25.r_1_, bf16[2048,512]{1,0:T(8,128)(2,1)S(1)} %bitcast.10, bf16[2048,512]{1,0:T(8,128)(2,1)S(1)} %bitcast.14, ...), custom_call_target="tpu_custom_call" | custom-call | tf_op jit(solution)/shard_map/pallas_call | solution.py:298
  101.2 3.1 %collective-permute-start.27 = (bf16[88,1024]{1,0:T(8,128)(2,1)S(1)}, bf16[88,1024]{1,0:T(8,128)(2,1)S(1)}, u32[]{:S(2)}, u32[]{:S(2)}) collective-permute-start(bf16[88,1024]{1,0:T(8,128)(2,1)S(1)} %get-tuple-element.58), channel_id=1, source_target_pairs={{0,28},{1,31},{2,30},{3,29},{4,24},{5,27},{6,26},{7,25},{8,20},{9,... | collective-permute-start | bytes 540680 | tf_op jit(solution)/shard_map/ppermute | solution.py:311
  105.1 2.7 %shard_map.108.early_ref = f32[256,2048]{1,0:T(8,128)S(1)} custom-call(bf16[512,528]{1,0:T(8,128)(2,1)S(1)} %get-tuple-element.35.r_0_, bf16[512,528]{1,0:T(8,128)(2,1)S(1)} %get-tuple-element.36.r_1_, bf16[256,256]{1,0:T(8,128)(2,1)S(1)} %collective-permute-done.8.r_2_, f32[1,2048]{1,0:T(1,128)S(1)} %bitcast.19, bf16[512,256]{1,0:T(8,128)(2,1)S(1)} %shard_map.104.r_1_.r_4_, ...), custom_call_target="tpu_custom_call" | custom-call | tf_op jit(solution)/shard_map/pallas_call | solution.py:298
  107.8 8.4 %collective-permute-done.26.refs_0_ = bf16[88,1024]{1,0:T(8,128)(2,1)S(1)} collective-permute-done((bf16[88,1024]{1,0:T(8,128)(2,1)S(1)}, bf16[88,1024]{1,0:T(8,128)(2,1)S(1)}, u32[]{:S(2)}, u32[]{:S(2)}) %collective-permute-start.26) | collective-permute-done | bytes 180256 | tf_op jit(solution)/shard_map/ppermute | solution.py:311
  116.3 4.0 %collective-permute-done.27.refs_1_ = bf16[88,1024]{1,0:T(8,128)(2,1)S(1)} collective-permute-done((bf16[88,1024]{1,0:T(8,128)(2,1)S(1)}, bf16[88,1024]{1,0:T(8,128)(2,1)S(1)}, u32[]{:S(2)}, u32[]{:S(2)}) %collective-permute-start.27) | collective-permute-done | bytes 180256 | tf_op jit(solution)/shard_map/ppermute | solution.py:311
  121.1 1.9 %collective-permute-done.28 = bf16[128,2048]{1,0:T(8,128)(2,1)S(1)} collective-permute-done((bf16[128,2048]{1,0:T(8,128)(2,1)S(1)}, bf16[128,2048]{1,0:T(8,128)(2,1)S(1)}, u32[]{:S(2)}, u32[]{:S(2)}) %collective-permute-start.28) | collective-permute-done | bytes 524320 | tf_op jit(solution)/shard_map/ppermute | solution.py:315
  (58 shorter events, 16.4 us)
Async XLA Ops:
  0.0 58.1 %collective-permute-start.11 = (bf16[2048,512]{1,0:T(8,128)(2,1)}, bf16[2048,512]{1,0:T(8,128)(2,1)S(1)}, u32[]{:S(2)}, u32[]{:S(2)}) collective-permute-start(bf16[2048,512]{1,0:T(8,128)(2,1)} %bitcast.7), channel_id=1, source_target_pairs={{0,1},{1,0},{2,3},{3,2},{4,5},{5,4},{6,7},{7,6},{8,9},{9,8},{10,11... | collective-permute-start | bytes 6291464 | tf_op jit(solution)/shard_map/ppermute | solution.py:315
  0.7 59.6 %collective-permute-start.12 = (bf16[2048,512]{1,0:T(8,128)(2,1)}, bf16[2048,512]{1,0:T(8,128)(2,1)S(1)}, u32[]{:S(2)}, u32[]{:S(2)}) collective-permute-start(bf16[2048,512]{1,0:T(8,128)(2,1)} %bitcast.11), channel_id=1, source_target_pairs={{0,1},{1,0},{2,3},{3,2},{4,5},{5,4},{6,7},{7,6},{8,9},{9,8},{10,11... | collective-permute-start | bytes 6291464 | tf_op jit(solution)/shard_map/ppermute | solution.py:315
  0.7 60.8 %collective-permute-start.13 = (bf16[512,2048]{1,0:T(8,128)(2,1)}, bf16[512,2048]{1,0:T(8,128)(2,1)S(1)}, u32[]{:S(2)}, u32[]{:S(2)}) collective-permute-start(bf16[512,2048]{1,0:T(8,128)(2,1)} %bitcast.15), channel_id=1, source_target_pairs={{0,1},{1,0},{2,3},{3,2},{4,5},{5,4},{6,7},{7,6},{8,9},{9,8},{10,11... | collective-permute-start | bytes 6291464 | tf_op jit(solution)/shard_map/ppermute | solution.py:315
  5.3 56.3 %copy-start.1 = (bf16[1,2048,512]{2,1,0:T(8,128)(2,1)S(1)}, bf16[1,2048,512]{2,1,0:T(8,128)(2,1)}, u32[]{:S(2)}) copy-start(bf16[1,2048,512]{2,1,0:T(8,128)(2,1)} %param.15) | copy-start | bytes 6291460
  6.4 55.1 %copy-start.9 = (f32[128,2]{0,1:T(2,128)S(1)}, f32[128,2]{0,1:T(2,128)}, u32[]{:S(2)}) copy-start(f32[128,2]{0,1:T(2,128)} %param.13) | copy-start | bytes 3076
  6.4 55.2 %copy-start = (bf16[1,2048,512]{2,1,0:T(8,128)(2,1)S(1)}, bf16[1,2048,512]{2,1,0:T(8,128)(2,1)}, u32[]{:S(2)}) copy-start(bf16[1,2048,512]{2,1,0:T(8,128)(2,1)} %param.14) | copy-start | bytes 6291460
  6.5 5.5 %collective-permute-start.3 = (bf16[128,256]{1,0:T(8,128)(2,1)S(1)}, bf16[128,256]{1,0:T(8,128)(2,1)S(1)}, u32[]{:S(2)}, u32[]{:S(2)}) collective-permute-start(bf16[128,256]{1,0:T(8,128)(2,1)S(1)} %get-tuple-element.40.refs_0_), channel_id=1, source_target_pairs={{0,16},{1,17},{2,18},{3,19},{4,20},{5,21},{6,22},{7,23},{8,24},{9,... | collective-permute-start | bytes 196616 | tf_op jit(solution)/shard_map/ppermute | solution.py:311
  12.0 4.7 %collective-permute-start.4 = (bf16[256,256]{1,0:T(8,128)(2,1)S(1)}, bf16[256,256]{1,0:T(8,128)(2,1)S(1)}, u32[]{:S(2)}, u32[]{:S(2)}) collective-permute-start(bf16[256,256]{1,0:T(8,128)(2,1)S(1)} %shard_map.103.refs_0_), channel_id=1, source_target_pairs={{0,8},{1,9},{2,10},{3,11},{4,12},{5,13},{6,14},{7,15},{8,0},{9,1},... | collective-permute-start | bytes 393224 | tf_op jit(solution)/shard_map/ppermute | solution.py:311
  12.9 15.7 %collective-permute-start.2 = (bf16[128,2048]{1,0:T(8,128)(2,1)}, bf16[128,2048]{1,0:T(8,128)(2,1)S(1)}, u32[]{:S(2)}, u32[]{:S(2)}) collective-permute-start(bf16[128,2048]{1,0:T(8,128)(2,1)} %tok_ref.1), channel_id=1, source_target_pairs={{0,1},{1,0},{2,3},{3,2},{4,5},{5,4},{6,7},{7,6},{8,9},{9,8},{10,11... | collective-permute-start | bytes 1572872 | tf_op jit(solution)/shard_map/ppermute | solution.py:315
  16.7 2.4 %collective-permute-start = (s32[2,128]{1,0:T(2,128)}, s32[2,128]{1,0:T(2,128)S(1)}, u32[]{:S(2)}, u32[]{:S(2)}) collective-permute-start(s32[2,128]{1,0:T(2,128)} %bitcast.1.route_ref), channel_id=1, source_target_pairs={{0,1},{1,0},{2,3},{3,2},{4,5},{5,4},{6,7},{7,6},{8,9},{9,8},{10,11... | collective-permute-start | bytes 3080 | tf_op jit(solution)/shard_map/ppermute | solution.py:315
  19.0 8.4 %collective-permute-start.7 = (bf16[512,256]{1,0:T(8,128)(2,1)S(1)}, bf16[512,256]{1,0:T(8,128)(2,1)S(1)}, u32[]{:S(2)}, u32[]{:S(2)}) collective-permute-start(bf16[512,256]{1,0:T(8,128)(2,1)S(1)} %shard_map.104.r_1_.r_4_), channel_id=1, source_target_pairs={{0,6},{1,7},{2,4},{3,5},{4,2},{5,3},{6,0},{7,1},{8,14},{9,15},{10,... | collective-permute-start | bytes 786440 | tf_op jit(solution)/shard_map/ppermute | solution.py:311
  27.4 6.7 %collective-permute-start.6 = (bf16[512,256]{1,0:T(8,128)(2,1)S(1)}, bf16[512,256]{1,0:T(8,128)(2,1)S(1)}, u32[]{:S(2)}, u32[]{:S(2)}) collective-permute-start(bf16[512,256]{1,0:T(8,128)(2,1)S(1)} %shard_map.104.r_1_.r_4_), channel_id=1, source_target_pairs={{0,4},{1,5},{2,6},{3,7},{4,0},{5,1},{6,2},{7,3},{8,12},{9,13},{10,... | collective-permute-start | bytes 786440 | tf_op jit(solution)/shard_map/ppermute | solution.py:311
  28.7 9.5 %collective-permute-start.5 = (bf16[512,256]{1,0:T(8,128)(2,1)S(1)}, bf16[512,256]{1,0:T(8,128)(2,1)S(1)}, u32[]{:S(2)}, u32[]{:S(2)}) collective-permute-start(bf16[512,256]{1,0:T(8,128)(2,1)S(1)} %shard_map.104.r_1_.r_4_), channel_id=1, source_target_pairs={{0,2},{1,3},{2,0},{3,1},{4,6},{5,7},{6,4},{7,5},{8,10},{9,11},{10,... | collective-permute-start | bytes 786440 | tf_op jit(solution)/shard_map/ppermute | solution.py:311
  34.1 15.7 %collective-permute-start.9 = (bf16[88,1024]{1,0:T(8,128)(2,1)S(1)}, bf16[88,1024]{1,0:T(8,128)(2,1)S(1)}, u32[]{:S(2)}, u32[]{:S(2)}) collective-permute-start(bf16[88,1024]{1,0:T(8,128)(2,1)S(1)} %get-tuple-element.41), channel_id=1, source_target_pairs={{0,16},{1,19},{2,18},{3,17},{4,20},{5,23},{6,22},{7,21},{8,24},{9,... | collective-permute-start | bytes 540680 | tf_op jit(solution)/shard_map/ppermute | solution.py:311
  38.1 15.6 %collective-permute-start.10 = (bf16[88,1024]{1,0:T(8,128)(2,1)S(1)}, bf16[88,1024]{1,0:T(8,128)(2,1)S(1)}, u32[]{:S(2)}, u32[]{:S(2)}) collective-permute-start(bf16[88,1024]{1,0:T(8,128)(2,1)S(1)} %get-tuple-element.42), channel_id=1, source_target_pairs={{0,20},{1,23},{2,22},{3,21},{4,16},{5,19},{6,18},{7,17},{8,28},{9,... | collective-permute-start | bytes 540680 | tf_op jit(solution)/shard_map/ppermute | solution.py:311
  49.8 7.0 %collective-permute-start.16 = (bf16[88,1024]{1,0:T(8,128)(2,1)S(1)}, bf16[88,1024]{1,0:T(8,128)(2,1)S(1)}, u32[]{:S(2)}, u32[]{:S(2)}) collective-permute-start(bf16[88,1024]{1,0:T(8,128)(2,1)S(1)} %get-tuple-element.45), channel_id=1, source_target_pairs={{0,4},{1,7},{2,6},{3,5},{4,0},{5,3},{6,2},{7,1},{8,12},{9,15},{10,... | collective-permute-start | bytes 540680 | tf_op jit(solution)/shard_map/ppermute | solution.py:311
  53.7 11.9 %collective-permute-start.17 = (bf16[88,1024]{1,0:T(8,128)(2,1)S(1)}, bf16[88,1024]{1,0:T(8,128)(2,1)S(1)}, u32[]{:S(2)}, u32[]{:S(2)}) collective-permute-start(bf16[88,1024]{1,0:T(8,128)(2,1)S(1)} %get-tuple-element.46), channel_id=1, source_target_pairs={{0,8},{1,11},{2,10},{3,9},{4,12},{5,15},{6,14},{7,13},{8,0},{9,3},... | collective-permute-start | bytes 540680 | tf_op jit(solution)/shard_map/ppermute | solution.py:311
  56.8 11.9 %collective-permute-start.18 = (bf16[88,1024]{1,0:T(8,128)(2,1)S(1)}, bf16[88,1024]{1,0:T(8,128)(2,1)S(1)}, u32[]{:S(2)}, u32[]{:S(2)}) collective-permute-start(bf16[88,1024]{1,0:T(8,128)(2,1)S(1)} %get-tuple-element.47), channel_id=1, source_target_pairs={{0,12},{1,15},{2,14},{3,13},{4,8},{5,11},{6,10},{7,9},{8,4},{9,7},... | collective-permute-start | bytes 540680 | tf_op jit(solution)/shard_map/ppermute | solution.py:311
  58.1 11.6 %collective-permute-start.19 = (bf16[88,1024]{1,0:T(8,128)(2,1)S(1)}, bf16[88,1024]{1,0:T(8,128)(2,1)S(1)}, u32[]{:S(2)}, u32[]{:S(2)}) collective-permute-start(bf16[88,1024]{1,0:T(8,128)(2,1)S(1)} %get-tuple-element.48), channel_id=1, source_target_pairs={{0,0},{1,3},{2,2},{3,1},{4,4},{5,7},{6,6},{7,5},{8,8},{9,11},{10,1... | collective-permute-start | bytes 540680 | tf_op jit(solution)/shard_map/ppermute | solution.py:311
  60.3 16.1 %collective-permute-start.8 = (bf16[256,256]{1,0:T(8,128)(2,1)S(1)}, bf16[256,256]{1,0:T(8,128)(2,1)S(1)}, u32[]{:S(2)}, u32[]{:S(2)}) collective-permute-start(bf16[256,256]{1,0:T(8,128)(2,1)S(1)} %shard_map.105), channel_id=1, source_target_pairs={{0,1},{1,0},{2,3},{3,2},{4,5},{5,4},{6,7},{7,6},{8,9},{9,8},{10,11... | collective-permute-start | bytes 393224 | tf_op jit(solution)/shard_map/ppermute | solution.py:315
  61.5 14.8 %collective-permute-start.1 = (f32[2,128]{1,0:T(2,128)S(1)}, f32[2,128]{1,0:T(2,128)S(1)}, u32[]{:S(2)}, u32[]{:S(2)}) collective-permute-start(f32[2,128]{1,0:T(2,128)S(1)} %bitcast.22), channel_id=1, source_target_pairs={{0,1},{1,0},{2,3},{3,2},{4,5},{5,4},{6,7},{7,6},{8,9},{9,8},{10,11... | collective-permute-start | bytes 3080 | tf_op jit(solution)/shard_map/ppermute | solution.py:315
  65.6 23.0 %collective-permute-start.24 = (bf16[88,1024]{1,0:T(8,128)(2,1)S(1)}, bf16[88,1024]{1,0:T(8,128)(2,1)S(1)}, u32[]{:S(2)}, u32[]{:S(2)}) collective-permute-start(bf16[88,1024]{1,0:T(8,128)(2,1)S(1)} %get-tuple-element.55), channel_id=1, source_target_pairs={{0,24},{1,27},{2,26},{3,25},{4,28},{5,31},{6,30},{7,29},{8,16},{9,... | collective-permute-start | bytes 540680 | tf_op jit(solution)/shard_map/ppermute | solution.py:311
  68.7 25.0 %collective-permute-start.25 = (bf16[88,1024]{1,0:T(8,128)(2,1)S(1)}, bf16[88,1024]{1,0:T(8,128)(2,1)S(1)}, u32[]{:S(2)}, u32[]{:S(2)}) collective-permute-start(bf16[88,1024]{1,0:T(8,128)(2,1)S(1)} %get-tuple-element.56), channel_id=1, source_target_pairs={{0,28},{1,31},{2,30},{3,29},{4,24},{5,27},{6,26},{7,25},{8,20},{9,... | collective-permute-start | bytes 540680 | tf_op jit(solution)/shard_map/ppermute | solution.py:311
  69.7 26.1 %collective-permute-start.14 = (bf16[88,1024]{1,0:T(8,128)(2,1)S(1)}, bf16[88,1024]{1,0:T(8,128)(2,1)S(1)}, u32[]{:S(2)}, u32[]{:S(2)}) collective-permute-start(bf16[88,1024]{1,0:T(8,128)(2,1)S(1)} %get-tuple-element.43), channel_id=1, source_target_pairs={{0,16},{1,19},{2,18},{3,17},{4,20},{5,23},{6,22},{7,21},{8,24},{9,... | collective-permute-start | bytes 540680 | tf_op jit(solution)/shard_map/ppermute | solution.py:311
  76.3 24.7 %collective-permute-start.15 = (bf16[88,1024]{1,0:T(8,128)(2,1)S(1)}, bf16[88,1024]{1,0:T(8,128)(2,1)S(1)}, u32[]{:S(2)}, u32[]{:S(2)}) collective-permute-start(bf16[88,1024]{1,0:T(8,128)(2,1)S(1)} %get-tuple-element.44), channel_id=1, source_target_pairs={{0,20},{1,23},{2,22},{3,21},{4,16},{5,19},{6,18},{7,17},{8,28},{9,... | collective-permute-start | bytes 540680 | tf_op jit(solution)/shard_map/ppermute | solution.py:311
  76.4 24.8 %collective-permute-start.20 = (bf16[88,1024]{1,0:T(8,128)(2,1)S(1)}, bf16[88,1024]{1,0:T(8,128)(2,1)S(1)}, u32[]{:S(2)}, u32[]{:S(2)}) collective-permute-start(bf16[88,1024]{1,0:T(8,128)(2,1)S(1)} %get-tuple-element.49), channel_id=1, source_target_pairs={{0,4},{1,7},{2,6},{3,5},{4,0},{5,3},{6,2},{7,1},{8,12},{9,15},{10,... | collective-permute-start | bytes 540680 | tf_op jit(solution)/shard_map/ppermute | solution.py:311
  88.6 16.5 %collective-permute-start.21 = (bf16[88,1024]{1,0:T(8,128)(2,1)S(1)}, bf16[88,1024]{1,0:T(8,128)(2,1)S(1)}, u32[]{:S(2)}, u32[]{:S(2)}) collective-permute-start(bf16[88,1024]{1,0:T(8,128)(2,1)S(1)} %get-tuple-element.50), channel_id=1, source_target_pairs={{0,8},{1,11},{2,10},{3,9},{4,12},{5,15},{6,14},{7,13},{8,0},{9,3},... | collective-permute-start | bytes 540680 | tf_op jit(solution)/shard_map/ppermute | solution.py:311
  93.7 11.4 %collective-permute-start.22 = (bf16[88,1024]{1,0:T(8,128)(2,1)S(1)}, bf16[88,1024]{1,0:T(8,128)(2,1)S(1)}, u32[]{:S(2)}, u32[]{:S(2)}) collective-permute-start(bf16[88,1024]{1,0:T(8,128)(2,1)S(1)} %get-tuple-element.51), channel_id=1, source_target_pairs={{0,12},{1,15},{2,14},{3,13},{4,8},{5,11},{6,10},{7,9},{8,4},{9,7},... | collective-permute-start | bytes 540680 | tf_op jit(solution)/shard_map/ppermute | solution.py:311
  95.9 9.2 %collective-permute-start.23 = (bf16[88,1024]{1,0:T(8,128)(2,1)S(1)}, bf16[88,1024]{1,0:T(8,128)(2,1)S(1)}, u32[]{:S(2)}, u32[]{:S(2)}) collective-permute-start(bf16[88,1024]{1,0:T(8,128)(2,1)S(1)} %get-tuple-element.52), channel_id=1, source_target_pairs={{0,0},{1,3},{2,2},{3,1},{4,4},{5,7},{6,6},{7,5},{8,8},{9,11},{10,1... | collective-permute-start | bytes 540680 | tf_op jit(solution)/shard_map/ppermute | solution.py:311
  101.0 15.3 %collective-permute-start.26 = (bf16[88,1024]{1,0:T(8,128)(2,1)S(1)}, bf16[88,1024]{1,0:T(8,128)(2,1)S(1)}, u32[]{:S(2)}, u32[]{:S(2)}) collective-permute-start(bf16[88,1024]{1,0:T(8,128)(2,1)S(1)} %get-tuple-element.57), channel_id=1, source_target_pairs={{0,24},{1,27},{2,26},{3,25},{4,28},{5,31},{6,30},{7,29},{8,16},{9,... | collective-permute-start | bytes 540680 | tf_op jit(solution)/shard_map/ppermute | solution.py:311
  101.2 19.0 %collective-permute-start.27 = (bf16[88,1024]{1,0:T(8,128)(2,1)S(1)}, bf16[88,1024]{1,0:T(8,128)(2,1)S(1)}, u32[]{:S(2)}, u32[]{:S(2)}) collective-permute-start(bf16[88,1024]{1,0:T(8,128)(2,1)S(1)} %get-tuple-element.58), channel_id=1, source_target_pairs={{0,28},{1,31},{2,30},{3,29},{4,24},{5,27},{6,26},{7,25},{8,20},{9,... | collective-permute-start | bytes 540680 | tf_op jit(solution)/shard_map/ppermute | solution.py:311
  121.0 2.0 %collective-permute-start.28 = (bf16[128,2048]{1,0:T(8,128)(2,1)S(1)}, bf16[128,2048]{1,0:T(8,128)(2,1)S(1)}, u32[]{:S(2)}, u32[]{:S(2)}) collective-permute-start(bf16[128,2048]{1,0:T(8,128)(2,1)S(1)} %get-tuple-element.60), channel_id=1, source_target_pairs={{0,1},{1,0},{2,3},{3,2},{4,5},{5,4},{6,7},{7,6},{8,9},{9,8},{10,11... | collective-permute-start | bytes 1572872 | tf_op jit(solution)/shard_map/ppermute | solution.py:315
  (7 other events, 14.9 us)

commit v2 on v1

--- a/solution.py
+++ b/solution.py
@@ -32,15 +32,6 @@
     return ((up_clip + 1.0) * gate_clip * jax.nn.sigmoid(SLOPE_ALPHA * gate_clip)).astype(
         jnp.bfloat16
     )
-
-
-def position():
-    return lax.axis_index("ep").astype(jnp.int32), lax.axis_index("tp").astype(jnp.int32)
-
-
-def row_split(capacity, width):
-    pieces = 8 // math.gcd(capacity, 8)
-    return pieces if width % (128 * pieces) == 0 else 1
 
 
 def position():
@@ -217,6 +208,18 @@
             ).astype(jnp.bfloat16)
 
 
+def fetch_kernel(*refs):
+    count = len(refs) // 2
+    sems = refs[-1]
+    copies = [
+        pltpu.make_async_copy(refs[i].at[0], refs[count + i], sems.at[i]) for i in range(count)
+    ]
+    for copy in copies:
+        copy.start()
+    for copy in copies:
+        copy.wait()
+
+
 def join_kernel(*refs):
     at = 0
     for ref in refs[:-1]:
@@ -295,6 +298,8 @@
 
 
 def call(kernel, outs, ins, scratch=(), spec=VMEM):
+    if spec is HBM:
+        ins = tuple(pltpu.with_memory_space_constraint(v, pltpu.HBM) for v in ins)
     return pl.pallas_call(
         kernel,
         out_shape=outs,
@@ -346,8 +351,15 @@
     tokens2 = partners(tokens)
     routes2 = partners(routes)
     rates2 = partners(rates)
-    own = (w_gate[0], w_up[0], w_down[0])
-    other = tuple(partners(w) for w in own)
+    own = (w_gate, w_up, w_down)
+    other = tuple(partners(w[0]) for w in own)
+    own = call(
+        fetch_kernel,
+        tuple(shape(w.shape[1:], w.dtype) for w in own),
+        own,
+        scratch=(pltpu.SemaphoreType.DMA((3,)),),
+        spec=HBM,
+    )
 
     inputs = (tokens, gain, routes, rates)
     held, norm_own, gain, routes, rates = call(

time: 124 us -> 121 us (0.976)
  local copies, waits for them, and re-layouts: 5.71 us -> 0.01 us
  Pallas kernels: 14 us -> 17.1 us
    unnamed x20 -> x4, local copies, waits for them, and re-layouts: 5.71 us -> 0.01 us
    pallas_call x11 -> x12, Pallas kernels: 14 us -> 17.1 us  [call(): pl.pallas_call(kernel, out_shape=outs, in_specs=[spec for _ in ins], out_...]
  transfers between devices with their start and end apart: 29 -> 29, of which waited for: 13 -> 13; matrix products, arithmetic and copies ran while one was open for 0% -> 0% of each run, Pallas kernels for 11% -> 14%
where the time goes in v2:
time: 121 us
  waiting for transfers between devices  61.9 us (51%)
  starting transfers between devices  41 us (34%)
  Pallas kernels  17.1 us (14%)
    ppermute x21, waiting for transfers between devices, swapped(): return lax.ppermute(value, ('ep', 'tp'), pairs)  59 us
    ppermute x21, starting transfers between devices, swapped(): return lax.ppermute(value, ('ep', 'tp'), pairs)  36.3 us
    pallas_call x12, Pallas kernels, call(): pl.pallas_call(kernel, out_shape=outs, in_specs=[spec for _ in ins], out_...  17.1 us
    ppermute x8, starting transfers between devices, partners(): return lax.ppermute(value, 'tp', [(0, 1), (1, 0)])  4.69 us
    ppermute x8, waiting for transfers between devices, partners(): return lax.ppermute(value, 'tp', [(0, 1), (1, 0)])  2.92 us
  transfers between devices with their start and end apart: 29, of which 13 were waited for; matrix products, arithmetic and copies ran while one was open for 0% of the time, Pallas kernels for 14%

profile of v2, /device:TPU:9, one launch (start us, length us, event | category | flops | bytes accessed | tf_op | source)
XLA Modules:
  0.0 121.2 jit_solution(7820245204892450678)
XLA Ops:
  1.2 1.3 %shard_map.100 = (bf16[128,256]{1,0:T(8,128)(2,1)S(1)}, bf16[128,2048]{1,0:T(8,128)(2,1)S(1)}, f32[1,2048]{1,0:T(1,128)S(1)}, s32[2,128]{1,0:T(2,128)S(1)}, f32[2,128]{1,0:T(2,128)S(1)}) custom-call(bf16[128,2048]{1,0:T(8,128)(2,1)} %tok_ref.1, f32[1,2048]{1,0:T(1,128)} %bitcast.11, s32[2,128]{1,0:T(2,128)} %bitcast.12, f32[2,128]{1,0:T(2,128)} %bitcast.14, ...), custom_call_target="tpu_custom_call" | custom-call | tf_op jit(solution)/shard_map/pallas_call | solution.py:303
  2.5 2.4 %collective-permute-start.3 = (bf16[128,256]{1,0:T(8,128)(2,1)S(1)}, bf16[128,256]{1,0:T(8,128)(2,1)S(1)}, u32[]{:S(2)}, u32[]{:S(2)}) collective-permute-start(bf16[128,256]{1,0:T(8,128)(2,1)S(1)} %get-tuple-element.43.refs_0_), channel_id=1, source_target_pairs={{0,16},{1,17},{2,18},{3,19},{4,20},{5,21},{6,22},{7,23},{8,24},{9,... | collective-permute-start | bytes 196616 | tf_op jit(solution)/shard_map/ppermute | solution.py:316
  4.9 3.2 %collective-permute-done.3.refs_1_ = bf16[128,256]{1,0:T(8,128)(2,1)S(1)} collective-permute-done((bf16[128,256]{1,0:T(8,128)(2,1)S(1)}, bf16[128,256]{1,0:T(8,128)(2,1)S(1)}, u32[]{:S(2)}, u32[]{:S(2)}) %collective-permute-start.3) | collective-permute-done | bytes 65568 | tf_op jit(solution)/shard_map/ppermute | solution.py:316
  9.9 2.8 %collective-permute-done.4.refs_1_ = bf16[256,256]{1,0:T(8,128)(2,1)S(1)} collective-permute-done((bf16[256,256]{1,0:T(8,128)(2,1)S(1)}, bf16[256,256]{1,0:T(8,128)(2,1)S(1)}, u32[]{:S(2)}, u32[]{:S(2)}) %collective-permute-start.4) | collective-permute-done | bytes 131104 | tf_op jit(solution)/shard_map/ppermute | solution.py:316
  12.7 1.3 %collective-permute-start = (s32[2,128]{1,0:T(2,128)}, s32[2,128]{1,0:T(2,128)S(1)}, u32[]{:S(2)}, u32[]{:S(2)}) collective-permute-start(s32[2,128]{1,0:T(2,128)} %bitcast.13), channel_id=1, source_target_pairs={{0,1},{1,0},{2,3},{3,2},{4,5},{5,4},{6,7},{7,6},{8,9},{9,8},{10,11... | collective-permute-start | bytes 3080 | tf_op jit(solution)/shard_map/ppermute | solution.py:320
  15.1 2.2 %collective-permute-start.7 = (bf16[512,256]{1,0:T(8,128)(2,1)S(1)}, bf16[512,256]{1,0:T(8,128)(2,1)S(1)}, u32[]{:S(2)}, u32[]{:S(2)}) collective-permute-start(bf16[512,256]{1,0:T(8,128)(2,1)S(1)} %shard_map.104.r_1_.r_4_), channel_id=1, source_target_pairs={{0,6},{1,7},{2,4},{3,5},{4,2},{5,3},{6,0},{7,1},{8,14},{9,15},{10,... | collective-permute-start | bytes 786440 | tf_op jit(solution)/shard_map/ppermute | solution.py:316
  17.2 6.3 %collective-permute-done.7.r_4_.r_7_ = bf16[512,256]{1,0:T(8,128)(2,1)S(1)} collective-permute-done((bf16[512,256]{1,0:T(8,128)(2,1)S(1)}, bf16[512,256]{1,0:T(8,128)(2,1)S(1)}, u32[]{:S(2)}, u32[]{:S(2)}) %collective-permute-start.7) | collective-permute-done | bytes 262176 | tf_op jit(solution)/shard_map/ppermute | solution.py:316
  23.5 1.2 %collective-permute-start.6 = (bf16[512,256]{1,0:T(8,128)(2,1)S(1)}, bf16[512,256]{1,0:T(8,128)(2,1)S(1)}, u32[]{:S(2)}, u32[]{:S(2)}) collective-permute-start(bf16[512,256]{1,0:T(8,128)(2,1)S(1)} %shard_map.104.r_1_.r_4_), channel_id=1, source_target_pairs={{0,4},{1,5},{2,6},{3,7},{4,0},{5,1},{6,2},{7,3},{8,12},{9,13},{10,... | collective-permute-start | bytes 786440 | tf_op jit(solution)/shard_map/ppermute | solution.py:316
  24.7 1.2 collective-permute-start.5
  27.1 3.0 %collective-permute-done.6.r_3_.r_6_ = bf16[512,256]{1,0:T(8,128)(2,1)S(1)} collective-permute-done((bf16[512,256]{1,0:T(8,128)(2,1)S(1)}, bf16[512,256]{1,0:T(8,128)(2,1)S(1)}, u32[]{:S(2)}, u32[]{:S(2)}) %collective-permute-start.6) | collective-permute-done | bytes 262176 | tf_op jit(solution)/shard_map/ppermute | solution.py:316
  30.2 4.0 %collective-permute-start.9 = (bf16[88,1024]{1,0:T(8,128)(2,1)S(1)}, bf16[88,1024]{1,0:T(8,128)(2,1)S(1)}, u32[]{:S(2)}, u32[]{:S(2)}) collective-permute-start(bf16[88,1024]{1,0:T(8,128)(2,1)S(1)} %get-tuple-element.44), channel_id=1, source_target_pairs={{0,16},{1,19},{2,18},{3,17},{4,20},{5,23},{6,22},{7,21},{8,24},{9,... | collective-permute-start | bytes 540680 | tf_op jit(solution)/shard_map/ppermute | solution.py:316
  35.2 10.8 %collective-permute-done.9.r_0_ = bf16[88,1024]{1,0:T(8,128)(2,1)S(1)} collective-permute-done((bf16[88,1024]{1,0:T(8,128)(2,1)S(1)}, bf16[88,1024]{1,0:T(8,128)(2,1)S(1)}, u32[]{:S(2)}, u32[]{:S(2)}) %collective-permute-start.9) | collective-permute-done | bytes 180256 | tf_op jit(solution)/shard_map/ppermute | solution.py:316
  47.1 2.6 %collective-permute-done.10.r_1_ = bf16[88,1024]{1,0:T(8,128)(2,1)S(1)} collective-permute-done((bf16[88,1024]{1,0:T(8,128)(2,1)S(1)}, bf16[88,1024]{1,0:T(8,128)(2,1)S(1)}, u32[]{:S(2)}, u32[]{:S(2)}) %collective-permute-start.10) | collective-permute-done | bytes 180256 | tf_op jit(solution)/shard_map/ppermute | solution.py:316
  49.8 3.1 %collective-permute-start.17 = (bf16[88,1024]{1,0:T(8,128)(2,1)S(1)}, bf16[88,1024]{1,0:T(8,128)(2,1)S(1)}, u32[]{:S(2)}, u32[]{:S(2)}) collective-permute-start(bf16[88,1024]{1,0:T(8,128)(2,1)S(1)} %get-tuple-element.52), channel_id=1, source_target_pairs={{0,8},{1,11},{2,10},{3,9},{4,12},{5,15},{6,14},{7,13},{8,0},{9,3},... | collective-permute-start | bytes 540680 | tf_op jit(solution)/shard_map/ppermute | solution.py:316
  52.9 1.3 %collective-permute-start.18 = (bf16[88,1024]{1,0:T(8,128)(2,1)S(1)}, bf16[88,1024]{1,0:T(8,128)(2,1)S(1)}, u32[]{:S(2)}, u32[]{:S(2)}) collective-permute-start(bf16[88,1024]{1,0:T(8,128)(2,1)S(1)} %get-tuple-element.53), channel_id=1, source_target_pairs={{0,12},{1,15},{2,14},{3,13},{4,8},{5,11},{6,10},{7,9},{8,4},{9,7},... | collective-permute-start | bytes 540680 | tf_op jit(solution)/shard_map/ppermute | solution.py:316
  54.2 2.2 %collective-permute-start.19 = (bf16[88,1024]{1,0:T(8,128)(2,1)S(1)}, bf16[88,1024]{1,0:T(8,128)(2,1)S(1)}, u32[]{:S(2)}, u32[]{:S(2)}) collective-permute-start(bf16[88,1024]{1,0:T(8,128)(2,1)S(1)} %get-tuple-element.54), channel_id=1, source_target_pairs={{0,0},{1,3},{2,2},{3,1},{4,4},{5,7},{6,6},{7,5},{8,8},{9,11},{10,1... | collective-permute-start | bytes 540680 | tf_op jit(solution)/shard_map/ppermute | solution.py:316
  57.7 2.9 %shard_map.106 = (bf16[2048,512]{1,0:T(8,128)(2,1)S(1)}, bf16[2048,512]{1,0:T(8,128)(2,1)S(1)}, bf16[512,2048]{1,0:T(8,128)(2,1)S(1)}) custom-call(bf16[1,2048,512]{2,1,0:T(8,128)(2,1)} %refs_0_.1, bf16[1,2048,512]{2,1,0:T(8,128)(2,1)} %refs_1_.1, bf16[1,512,2048]{2,1,0:T(8,128)(2,1)} %refs_2_.1), custom_call_target="tpu_custom_call" | custom-call | tf_op jit(solution)/shard_map/pallas_call | solution.py:303
  60.6 2.4 %shard_map.107 = (bf16[88,1024]{1,0:T(8,128)(2,1)S(1)}, bf16[88,1024]{1,0:T(8,128)(2,1)S(1)}) custom-call(bf16[88,1024]{1,0:T(8,128)(2,1)S(1)} %collective-permute-done.9.r_0_, bf16[88,1024]{1,0:T(8,128)(2,1)S(1)} %collective-permute-done.10.r_1_, bf16[2048,512]{1,0:T(8,128)(2,1)S(1)} %get-tuple-element.46.r_2_.r_4_, ...), custom_call_target="tpu_custom_call" | custom-call | tf_op jit(solution)/shard_map/pallas_call | solution.py:303
  62.9 3.1 %collective-permute-start.24 = (bf16[88,1024]{1,0:T(8,128)(2,1)S(1)}, bf16[88,1024]{1,0:T(8,128)(2,1)S(1)}, u32[]{:S(2)}, u32[]{:S(2)}) collective-permute-start(bf16[88,1024]{1,0:T(8,128)(2,1)S(1)} %get-tuple-element.61), channel_id=1, source_target_pairs={{0,24},{1,27},{2,26},{3,25},{4,28},{5,31},{6,30},{7,29},{8,16},{9,... | collective-permute-start | bytes 540680 | tf_op jit(solution)/shard_map/ppermute | solution.py:316
  67.1 3.6 %collective-permute-start.14 = (bf16[88,1024]{1,0:T(8,128)(2,1)S(1)}, bf16[88,1024]{1,0:T(8,128)(2,1)S(1)}, u32[]{:S(2)}, u32[]{:S(2)}) collective-permute-start(bf16[88,1024]{1,0:T(8,128)(2,1)S(1)} %get-tuple-element.49), channel_id=1, source_target_pairs={{0,16},{1,19},{2,18},{3,17},{4,20},{5,23},{6,22},{7,21},{8,24},{9,... | collective-permute-start | bytes 540680 | tf_op jit(solution)/shard_map/ppermute | solution.py:316
  70.8 2.9 %shard_map.108 = (bf16[88,1024]{1,0:T(8,128)(2,1)S(1)}, bf16[88,1024]{1,0:T(8,128)(2,1)S(1)}, bf16[88,1024]{1,0:T(8,128)(2,1)S(1)}, bf16[88,1024]{1,0:T(8,128)(2,1)S(1)}) custom-call(bf16[88,1024]{1,0:T(8,128)(2,1)S(1)} %collective-permute-done.16.r_0_, bf16[88,1024]{1,0:T(8,128)(2,1)S(1)} %collective-permute-done.17.r_1_, ...), custom_call_target="tpu_custom_call" | custom-call | tf_op jit(solution)/shard_map/pallas_call | solution.py:303
  73.8 1.7 %collective-permute-start.20 = (bf16[88,1024]{1,0:T(8,128)(2,1)S(1)}, bf16[88,1024]{1,0:T(8,128)(2,1)S(1)}, u32[]{:S(2)}, u32[]{:S(2)}) collective-permute-start(bf16[88,1024]{1,0:T(8,128)(2,1)S(1)} %get-tuple-element.55), channel_id=1, source_target_pairs={{0,4},{1,7},{2,6},{3,5},{4,0},{5,3},{6,2},{7,1},{8,12},{9,15},{10,... | collective-permute-start | bytes 540680 | tf_op jit(solution)/shard_map/ppermute | solution.py:316
  75.4 10.5 %collective-permute-done.24.r_0_ = bf16[88,1024]{1,0:T(8,128)(2,1)S(1)} collective-permute-done((bf16[88,1024]{1,0:T(8,128)(2,1)S(1)}, bf16[88,1024]{1,0:T(8,128)(2,1)S(1)}, u32[]{:S(2)}, u32[]{:S(2)}) %collective-permute-start.24) | collective-permute-done | bytes 180256 | tf_op jit(solution)/shard_map/ppermute | solution.py:316
  85.9 5.1 %collective-permute-done.25.r_1_ = bf16[88,1024]{1,0:T(8,128)(2,1)S(1)} collective-permute-done((bf16[88,1024]{1,0:T(8,128)(2,1)S(1)}, bf16[88,1024]{1,0:T(8,128)(2,1)S(1)}, u32[]{:S(2)}, u32[]{:S(2)}) %collective-permute-start.25) | collective-permute-done | bytes 180256 | tf_op jit(solution)/shard_map/ppermute | solution.py:316
  91.1 2.2 %collective-permute-done.14.r_8_ = bf16[88,1024]{1,0:T(8,128)(2,1)S(1)} collective-permute-done((bf16[88,1024]{1,0:T(8,128)(2,1)S(1)}, bf16[88,1024]{1,0:T(8,128)(2,1)S(1)}, u32[]{:S(2)}, u32[]{:S(2)}) %collective-permute-start.14) | collective-permute-done | bytes 180256 | tf_op jit(solution)/shard_map/ppermute | solution.py:316
  93.3 2.7 %collective-permute-start.23 = (bf16[88,1024]{1,0:T(8,128)(2,1)S(1)}, bf16[88,1024]{1,0:T(8,128)(2,1)S(1)}, u32[]{:S(2)}, u32[]{:S(2)}) collective-permute-start(bf16[88,1024]{1,0:T(8,128)(2,1)S(1)} %get-tuple-element.58), channel_id=1, source_target_pairs={{0,0},{1,3},{2,2},{3,1},{4,4},{5,7},{6,6},{7,5},{8,8},{9,11},{10,1... | collective-permute-start | bytes 540680 | tf_op jit(solution)/shard_map/ppermute | solution.py:316
  96.0 2.4 %shard_map.110 = (bf16[88,1024]{1,0:T(8,128)(2,1)S(1)}, bf16[88,1024]{1,0:T(8,128)(2,1)S(1)}) custom-call(bf16[88,1024]{1,0:T(8,128)(2,1)S(1)} %collective-permute-done.24.r_0_, bf16[88,1024]{1,0:T(8,128)(2,1)S(1)} %collective-permute-done.25.r_1_, bf16[2048,512]{1,0:T(8,128)(2,1)S(1)} %get-tuple-element.46.r_2_.r_4_, ...), custom_call_target="tpu_custom_call" | custom-call | tf_op jit(solution)/shard_map/pallas_call | solution.py:303
  98.6 3.1 %collective-permute-start.27 = (bf16[88,1024]{1,0:T(8,128)(2,1)S(1)}, bf16[88,1024]{1,0:T(8,128)(2,1)S(1)}, u32[]{:S(2)}, u32[]{:S(2)}) collective-permute-start(bf16[88,1024]{1,0:T(8,128)(2,1)S(1)} %get-tuple-element.64), channel_id=1, source_target_pairs={{0,28},{1,31},{2,30},{3,29},{4,24},{5,27},{6,26},{7,25},{8,20},{9,... | collective-permute-start | bytes 540680 | tf_op jit(solution)/shard_map/ppermute | solution.py:316
  102.5 2.7 %shard_map.109.early_ref = f32[256,2048]{1,0:T(8,128)S(1)} custom-call(bf16[512,528]{1,0:T(8,128)(2,1)S(1)} %get-tuple-element.38.r_0_, bf16[512,528]{1,0:T(8,128)(2,1)S(1)} %get-tuple-element.39.r_1_, bf16[256,256]{1,0:T(8,128)(2,1)S(1)} %collective-permute-done.8.r_2_, f32[1,2048]{1,0:T(1,128)S(1)} %bitcast.7, bf16[512,256]{1,0:T(8,128)(2,1)S(1)} %shard_map.104.r_1_.r_4_, ...), custom_call_target="tpu_custom_call" | custom-call | tf_op jit(solution)/shard_map/pallas_call | solution.py:303
  105.2 8.4 %collective-permute-done.26.refs_0_ = bf16[88,1024]{1,0:T(8,128)(2,1)S(1)} collective-permute-done((bf16[88,1024]{1,0:T(8,128)(2,1)S(1)}, bf16[88,1024]{1,0:T(8,128)(2,1)S(1)}, u32[]{:S(2)}, u32[]{:S(2)}) %collective-permute-start.26) | collective-permute-done | bytes 180256 | tf_op jit(solution)/shard_map/ppermute | solution.py:316
  113.6 4.0 %collective-permute-done.27.refs_1_ = bf16[88,1024]{1,0:T(8,128)(2,1)S(1)} collective-permute-done((bf16[88,1024]{1,0:T(8,128)(2,1)S(1)}, bf16[88,1024]{1,0:T(8,128)(2,1)S(1)}, u32[]{:S(2)}, u32[]{:S(2)}) %collective-permute-start.27) | collective-permute-done | bytes 180256 | tf_op jit(solution)/shard_map/ppermute | solution.py:316
  118.4 1.9 %collective-permute-done.28 = bf16[128,2048]{1,0:T(8,128)(2,1)S(1)} collective-permute-done((bf16[128,2048]{1,0:T(8,128)(2,1)S(1)}, bf16[128,2048]{1,0:T(8,128)(2,1)S(1)}, u32[]{:S(2)}, u32[]{:S(2)}) %collective-permute-start.28) | collective-permute-done | bytes 524320 | tf_op jit(solution)/shard_map/ppermute | solution.py:320
  (43 shorter events, 12.4 us)
Async XLA Ops:
  0.0 54.2 %collective-permute-start.13 = (bf16[512,2048]{1,0:T(8,128)(2,1)}, bf16[512,2048]{1,0:T(8,128)(2,1)S(1)}, u32[]{:S(2)}, u32[]{:S(2)}) collective-permute-start(bf16[512,2048]{1,0:T(8,128)(2,1)} %bitcast.10), channel_id=1, source_target_pairs={{0,1},{1,0},{2,3},{3,2},{4,5},{5,4},{6,7},{7,6},{8,9},{9,8},{10,11... | collective-permute-start | bytes 6291464 | tf_op jit(solution)/shard_map/ppermute | solution.py:320
  0.7 55.7 %collective-permute-start.12 = (bf16[2048,512]{1,0:T(8,128)(2,1)}, bf16[2048,512]{1,0:T(8,128)(2,1)S(1)}, u32[]{:S(2)}, u32[]{:S(2)}) collective-permute-start(bf16[2048,512]{1,0:T(8,128)(2,1)} %bitcast.9), channel_id=1, source_target_pairs={{0,1},{1,0},{2,3},{3,2},{4,5},{5,4},{6,7},{7,6},{8,9},{9,8},{10,11... | collective-permute-start | bytes 6291464 | tf_op jit(solution)/shard_map/ppermute | solution.py:320
  0.7 56.9 %collective-permute-start.11 = (bf16[2048,512]{1,0:T(8,128)(2,1)}, bf16[2048,512]{1,0:T(8,128)(2,1)S(1)}, u32[]{:S(2)}, u32[]{:S(2)}) collective-permute-start(bf16[2048,512]{1,0:T(8,128)(2,1)} %bitcast.8), channel_id=1, source_target_pairs={{0,1},{1,0},{2,3},{3,2},{4,5},{5,4},{6,7},{7,6},{8,9},{9,8},{10,11... | collective-permute-start | bytes 6291464 | tf_op jit(solution)/shard_map/ppermute | solution.py:320
  2.5 55.1 %copy-start.1 = (f32[128,2]{0,1:T(2,128)S(1)}, f32[128,2]{0,1:T(2,128)}, u32[]{:S(2)}) copy-start(f32[128,2]{0,1:T(2,128)} %param.13) | copy-start | bytes 3076
  2.5 5.5 %collective-permute-start.3 = (bf16[128,256]{1,0:T(8,128)(2,1)S(1)}, bf16[128,256]{1,0:T(8,128)(2,1)S(1)}, u32[]{:S(2)}, u32[]{:S(2)}) collective-permute-start(bf16[128,256]{1,0:T(8,128)(2,1)S(1)} %get-tuple-element.43.refs_0_), channel_id=1, source_target_pairs={{0,16},{1,17},{2,18},{3,19},{4,20},{5,21},{6,22},{7,23},{8,24},{9,... | collective-permute-start | bytes 196616 | tf_op jit(solution)/shard_map/ppermute | solution.py:316
  8.1 4.7 %collective-permute-start.4 = (bf16[256,256]{1,0:T(8,128)(2,1)S(1)}, bf16[256,256]{1,0:T(8,128)(2,1)S(1)}, u32[]{:S(2)}, u32[]{:S(2)}) collective-permute-start(bf16[256,256]{1,0:T(8,128)(2,1)S(1)} %shard_map.103.refs_0_), channel_id=1, source_target_pairs={{0,8},{1,9},{2,10},{3,11},{4,12},{5,13},{6,14},{7,15},{8,0},{9,1},... | collective-permute-start | bytes 393224 | tf_op jit(solution)/shard_map/ppermute | solution.py:316
  9.0 15.7 %collective-permute-start.2 = (bf16[128,2048]{1,0:T(8,128)(2,1)}, bf16[128,2048]{1,0:T(8,128)(2,1)S(1)}, u32[]{:S(2)}, u32[]{:S(2)}) collective-permute-start(bf16[128,2048]{1,0:T(8,128)(2,1)} %tok_ref.1), channel_id=1, source_target_pairs={{0,1},{1,0},{2,3},{3,2},{4,5},{5,4},{6,7},{7,6},{8,9},{9,8},{10,11... | collective-permute-start | bytes 1572872 | tf_op jit(solution)/shard_map/ppermute | solution.py:320
  12.7 2.4 %collective-permute-start = (s32[2,128]{1,0:T(2,128)}, s32[2,128]{1,0:T(2,128)S(1)}, u32[]{:S(2)}, u32[]{:S(2)}) collective-permute-start(s32[2,128]{1,0:T(2,128)} %bitcast.13), channel_id=1, source_target_pairs={{0,1},{1,0},{2,3},{3,2},{4,5},{5,4},{6,7},{7,6},{8,9},{9,8},{10,11... | collective-permute-start | bytes 3080 | tf_op jit(solution)/shard_map/ppermute | solution.py:320
  15.1 8.4 %collective-permute-start.7 = (bf16[512,256]{1,0:T(8,128)(2,1)S(1)}, bf16[512,256]{1,0:T(8,128)(2,1)S(1)}, u32[]{:S(2)}, u32[]{:S(2)}) collective-permute-start(bf16[512,256]{1,0:T(8,128)(2,1)S(1)} %shard_map.104.r_1_.r_4_), channel_id=1, source_target_pairs={{0,6},{1,7},{2,4},{3,5},{4,2},{5,3},{6,0},{7,1},{8,14},{9,15},{10,... | collective-permute-start | bytes 786440 | tf_op jit(solution)/shard_map/ppermute | solution.py:316
  23.5 6.7 %collective-permute-start.6 = (bf16[512,256]{1,0:T(8,128)(2,1)S(1)}, bf16[512,256]{1,0:T(8,128)(2,1)S(1)}, u32[]{:S(2)}, u32[]{:S(2)}) collective-permute-start(bf16[512,256]{1,0:T(8,128)(2,1)S(1)} %shard_map.104.r_1_.r_4_), channel_id=1, source_target_pairs={{0,4},{1,5},{2,6},{3,7},{4,0},{5,1},{6,2},{7,3},{8,12},{9,13},{10,... | collective-permute-start | bytes 786440 | tf_op jit(solution)/shard_map/ppermute | solution.py:316
  24.7 9.5 %collective-permute-start.5 = (bf16[512,256]{1,0:T(8,128)(2,1)S(1)}, bf16[512,256]{1,0:T(8,128)(2,1)S(1)}, u32[]{:S(2)}, u32[]{:S(2)}) collective-permute-start(bf16[512,256]{1,0:T(8,128)(2,1)S(1)} %shard_map.104.r_1_.r_4_), channel_id=1, source_target_pairs={{0,2},{1,3},{2,0},{3,1},{4,6},{5,7},{6,4},{7,5},{8,10},{9,11},{10,... | collective-permute-start | bytes 786440 | tf_op jit(solution)/shard_map/ppermute | solution.py:316
  30.2 15.7 %collective-permute-start.9 = (bf16[88,1024]{1,0:T(8,128)(2,1)S(1)}, bf16[88,1024]{1,0:T(8,128)(2,1)S(1)}, u32[]{:S(2)}, u32[]{:S(2)}) collective-permute-start(bf16[88,1024]{1,0:T(8,128)(2,1)S(1)} %get-tuple-element.44), channel_id=1, source_target_pairs={{0,16},{1,19},{2,18},{3,17},{4,20},{5,23},{6,22},{7,21},{8,24},{9,... | collective-permute-start | bytes 540680 | tf_op jit(solution)/shard_map/ppermute | solution.py:316
  34.2 15.6 %collective-permute-start.10 = (bf16[88,1024]{1,0:T(8,128)(2,1)S(1)}, bf16[88,1024]{1,0:T(8,128)(2,1)S(1)}, u32[]{:S(2)}, u32[]{:S(2)}) collective-permute-start(bf16[88,1024]{1,0:T(8,128)(2,1)S(1)} %get-tuple-element.45), channel_id=1, source_target_pairs={{0,20},{1,23},{2,22},{3,21},{4,16},{5,19},{6,18},{7,17},{8,28},{9,... | collective-permute-start | bytes 540680 | tf_op jit(solution)/shard_map/ppermute | solution.py:316
  45.9 7.0 %collective-permute-start.16 = (bf16[88,1024]{1,0:T(8,128)(2,1)S(1)}, bf16[88,1024]{1,0:T(8,128)(2,1)S(1)}, u32[]{:S(2)}, u32[]{:S(2)}) collective-permute-start(bf16[88,1024]{1,0:T(8,128)(2,1)S(1)} %get-tuple-element.51), channel_id=1, source_target_pairs={{0,4},{1,7},{2,6},{3,5},{4,0},{5,3},{6,2},{7,1},{8,12},{9,15},{10,... | collective-permute-start | bytes 540680 | tf_op jit(solution)/shard_map/ppermute | solution.py:316
  49.8 13.2 %collective-permute-start.17 = (bf16[88,1024]{1,0:T(8,128)(2,1)S(1)}, bf16[88,1024]{1,0:T(8,128)(2,1)S(1)}, u32[]{:S(2)}, u32[]{:S(2)}) collective-permute-start(bf16[88,1024]{1,0:T(8,128)(2,1)S(1)} %get-tuple-element.52), channel_id=1, source_target_pairs={{0,8},{1,11},{2,10},{3,9},{4,12},{5,15},{6,14},{7,13},{8,0},{9,3},... | collective-permute-start | bytes 540680 | tf_op jit(solution)/shard_map/ppermute | solution.py:316
  52.9 13.2 %collective-permute-start.18 = (bf16[88,1024]{1,0:T(8,128)(2,1)S(1)}, bf16[88,1024]{1,0:T(8,128)(2,1)S(1)}, u32[]{:S(2)}, u32[]{:S(2)}) collective-permute-start(bf16[88,1024]{1,0:T(8,128)(2,1)S(1)} %get-tuple-element.53), channel_id=1, source_target_pairs={{0,12},{1,15},{2,14},{3,13},{4,8},{5,11},{6,10},{7,9},{8,4},{9,7},... | collective-permute-start | bytes 540680 | tf_op jit(solution)/shard_map/ppermute | solution.py:316
  54.2 12.9 %collective-permute-start.19 = (bf16[88,1024]{1,0:T(8,128)(2,1)S(1)}, bf16[88,1024]{1,0:T(8,128)(2,1)S(1)}, u32[]{:S(2)}, u32[]{:S(2)}) collective-permute-start(bf16[88,1024]{1,0:T(8,128)(2,1)S(1)} %get-tuple-element.54), channel_id=1, source_target_pairs={{0,0},{1,3},{2,2},{3,1},{4,4},{5,7},{6,6},{7,5},{8,8},{9,11},{10,1... | collective-permute-start | bytes 540680 | tf_op jit(solution)/shard_map/ppermute | solution.py:316
  56.4 17.4 %collective-permute-start.8 = (bf16[256,256]{1,0:T(8,128)(2,1)S(1)}, bf16[256,256]{1,0:T(8,128)(2,1)S(1)}, u32[]{:S(2)}, u32[]{:S(2)}) collective-permute-start(bf16[256,256]{1,0:T(8,128)(2,1)S(1)} %shard_map.105), channel_id=1, source_target_pairs={{0,1},{1,0},{2,3},{3,2},{4,5},{5,4},{6,7},{7,6},{8,9},{9,8},{10,11... | collective-permute-start | bytes 393224 | tf_op jit(solution)/shard_map/ppermute | solution.py:320
  57.6 16.1 %collective-permute-start.1 = (f32[2,128]{1,0:T(2,128)S(1)}, f32[2,128]{1,0:T(2,128)S(1)}, u32[]{:S(2)}, u32[]{:S(2)}) collective-permute-start(f32[2,128]{1,0:T(2,128)S(1)} %bitcast.15), channel_id=1, source_target_pairs={{0,1},{1,0},{2,3},{3,2},{4,5},{5,4},{6,7},{7,6},{8,9},{9,8},{10,11... | collective-permute-start | bytes 3080 | tf_op jit(solution)/shard_map/ppermute | solution.py:320
  62.9 23.0 %collective-permute-start.24 = (bf16[88,1024]{1,0:T(8,128)(2,1)S(1)}, bf16[88,1024]{1,0:T(8,128)(2,1)S(1)}, u32[]{:S(2)}, u32[]{:S(2)}) collective-permute-start(bf16[88,1024]{1,0:T(8,128)(2,1)S(1)} %get-tuple-element.61), channel_id=1, source_target_pairs={{0,24},{1,27},{2,26},{3,25},{4,28},{5,31},{6,30},{7,29},{8,16},{9,... | collective-permute-start | bytes 540680 | tf_op jit(solution)/shard_map/ppermute | solution.py:316
  66.1 25.0 %collective-permute-start.25 = (bf16[88,1024]{1,0:T(8,128)(2,1)S(1)}, bf16[88,1024]{1,0:T(8,128)(2,1)S(1)}, u32[]{:S(2)}, u32[]{:S(2)}) collective-permute-start(bf16[88,1024]{1,0:T(8,128)(2,1)S(1)} %get-tuple-element.62), channel_id=1, source_target_pairs={{0,28},{1,31},{2,30},{3,29},{4,24},{5,27},{6,26},{7,25},{8,20},{9,... | collective-permute-start | bytes 540680 | tf_op jit(solution)/shard_map/ppermute | solution.py:316
  67.1 26.1 %collective-permute-start.14 = (bf16[88,1024]{1,0:T(8,128)(2,1)S(1)}, bf16[88,1024]{1,0:T(8,128)(2,1)S(1)}, u32[]{:S(2)}, u32[]{:S(2)}) collective-permute-start(bf16[88,1024]{1,0:T(8,128)(2,1)S(1)} %get-tuple-element.49), channel_id=1, source_target_pairs={{0,16},{1,19},{2,18},{3,17},{4,20},{5,23},{6,22},{7,21},{8,24},{9,... | collective-permute-start | bytes 540680 | tf_op jit(solution)/shard_map/ppermute | solution.py:316
  73.7 24.7 %collective-permute-start.15 = (bf16[88,1024]{1,0:T(8,128)(2,1)S(1)}, bf16[88,1024]{1,0:T(8,128)(2,1)S(1)}, u32[]{:S(2)}, u32[]{:S(2)}) collective-permute-start(bf16[88,1024]{1,0:T(8,128)(2,1)S(1)} %get-tuple-element.50), channel_id=1, source_target_pairs={{0,20},{1,23},{2,22},{3,21},{4,16},{5,19},{6,18},{7,17},{8,28},{9,... | collective-permute-start | bytes 540680 | tf_op jit(solution)/shard_map/ppermute | solution.py:316
  73.8 24.9 %collective-permute-start.20 = (bf16[88,1024]{1,0:T(8,128)(2,1)S(1)}, bf16[88,1024]{1,0:T(8,128)(2,1)S(1)}, u32[]{:S(2)}, u32[]{:S(2)}) collective-permute-start(bf16[88,1024]{1,0:T(8,128)(2,1)S(1)} %get-tuple-element.55), channel_id=1, source_target_pairs={{0,4},{1,7},{2,6},{3,5},{4,0},{5,3},{6,2},{7,1},{8,12},{9,15},{10,... | collective-permute-start | bytes 540680 | tf_op jit(solution)/shard_map/ppermute | solution.py:316
  85.9 16.5 %collective-permute-start.21 = (bf16[88,1024]{1,0:T(8,128)(2,1)S(1)}, bf16[88,1024]{1,0:T(8,128)(2,1)S(1)}, u32[]{:S(2)}, u32[]{:S(2)}) collective-permute-start(bf16[88,1024]{1,0:T(8,128)(2,1)S(1)} %get-tuple-element.56), channel_id=1, source_target_pairs={{0,8},{1,11},{2,10},{3,9},{4,12},{5,15},{6,14},{7,13},{8,0},{9,3},... | collective-permute-start | bytes 540680 | tf_op jit(solution)/shard_map/ppermute | solution.py:316
  91.1 11.4 %collective-permute-start.22 = (bf16[88,1024]{1,0:T(8,128)(2,1)S(1)}, bf16[88,1024]{1,0:T(8,128)(2,1)S(1)}, u32[]{:S(2)}, u32[]{:S(2)}) collective-permute-start(bf16[88,1024]{1,0:T(8,128)(2,1)S(1)} %get-tuple-element.57), channel_id=1, source_target_pairs={{0,12},{1,15},{2,14},{3,13},{4,8},{5,11},{6,10},{7,9},{8,4},{9,7},... | collective-permute-start | bytes 540680 | tf_op jit(solution)/shard_map/ppermute | solution.py:316
  93.3 9.2 %copy-start = (f32[2048]{0:T(1024)S(1)}, f32[2048]{0:T(1024)}, u32[]{:S(2)}) copy-start(f32[2048]{0:T(1024)} %param.19) | copy-start | bytes 24580
  93.3 9.2 %collective-permute-start.23 = (bf16[88,1024]{1,0:T(8,128)(2,1)S(1)}, bf16[88,1024]{1,0:T(8,128)(2,1)S(1)}, u32[]{:S(2)}, u32[]{:S(2)}) collective-permute-start(bf16[88,1024]{1,0:T(8,128)(2,1)S(1)} %get-tuple-element.58), channel_id=1, source_target_pairs={{0,0},{1,3},{2,2},{3,1},{4,4},{5,7},{6,6},{7,5},{8,8},{9,11},{10,1... | collective-permute-start | bytes 540680 | tf_op jit(solution)/shard_map/ppermute | solution.py:316
  98.4 15.3 %collective-permute-start.26 = (bf16[88,1024]{1,0:T(8,128)(2,1)S(1)}, bf16[88,1024]{1,0:T(8,128)(2,1)S(1)}, u32[]{:S(2)}, u32[]{:S(2)}) collective-permute-start(bf16[88,1024]{1,0:T(8,128)(2,1)S(1)} %get-tuple-element.63), channel_id=1, source_target_pairs={{0,24},{1,27},{2,26},{3,25},{4,28},{5,31},{6,30},{7,29},{8,16},{9,... | collective-permute-start | bytes 540680 | tf_op jit(solution)/shard_map/ppermute | solution.py:316
  98.6 19.0 %collective-permute-start.27 = (bf16[88,1024]{1,0:T(8,128)(2,1)S(1)}, bf16[88,1024]{1,0:T(8,128)(2,1)S(1)}, u32[]{:S(2)}, u32[]{:S(2)}) collective-permute-start(bf16[88,1024]{1,0:T(8,128)(2,1)S(1)} %get-tuple-element.64), channel_id=1, source_target_pairs={{0,28},{1,31},{2,30},{3,29},{4,24},{5,27},{6,26},{7,25},{8,20},{9,... | collective-permute-start | bytes 540680 | tf_op jit(solution)/shard_map/ppermute | solution.py:316
  118.3 2.0 %collective-permute-start.28 = (bf16[128,2048]{1,0:T(8,128)(2,1)S(1)}, bf16[128,2048]{1,0:T(8,128)(2,1)S(1)}, u32[]{:S(2)}, u32[]{:S(2)}) collective-permute-start(bf16[128,2048]{1,0:T(8,128)(2,1)S(1)} %get-tuple-element.66), channel_id=1, source_target_pairs={{0,1},{1,0},{2,3},{3,2},{4,5},{5,4},{6,7},{7,6},{8,9},{9,8},{10,11... | collective-permute-start | bytes 1572872 | tf_op jit(solution)/shard_map/ppermute | solution.py:320

commit v3 on v2

--- a/solution.py
+++ b/solution.py
@@ -65,17 +65,20 @@
     return [routes[c : c + 1, :] == expert for c in range(routes.shape[0])]
 
 
-def slot_ranks(routes, expert):
+def slot_ranks(routes, expert, capacity):
     tokens = routes.shape[1]
     chosen = sum(jnp.where(mask, 1.0, 0.0) for mask in choice_masks(routes, expert))
-    earlier = lax.broadcasted_iota(jnp.int32, (tokens, tokens), 0) < lax.broadcasted_iota(
-        jnp.int32, (tokens, tokens), 1
-    )
+    half = tokens // 2 if capacity else tokens
+    row = lax.broadcasted_iota(jnp.int32, (tokens, tokens), 0)
+    column = lax.broadcasted_iota(jnp.int32, (tokens, tokens), 1)
+    earlier = (row < column) & ((row >= half) == (column >= half))
     counted = jnp.dot(
         chosen.astype(jnp.bfloat16),
         jnp.where(earlier, 1.0, 0.0).astype(jnp.bfloat16),
         preferred_element_type=jnp.float32,
     )
+    second = lax.broadcasted_iota(jnp.int32, (1, tokens), 1) >= half
+    counted = counted + jnp.where(second, float(capacity), 0.0)
     return jnp.where(chosen > 0.0, counted, -1.0)
 
 
@@ -116,7 +119,7 @@
     norm_ref[:half, :] = own_ref[...]
     norm_ref[half:, :] = rms_normed(tok2_ref[...], gain_ref[...])
     routes = jnp.concatenate([route_ref[...], route2_ref[...]], axis=1)
-    ranks = slot_ranks(routes, expert_column(plan))
+    ranks = slot_ranks(routes, expert_column(plan), capacity // 2)
     piece, slot = block_rows(capacity, pieces)
     packed = None
     for h in range(pieces):
@@ -161,10 +164,9 @@
     return block
 
 
-def expert_kernel(count, capacity, *refs):
+def expert_kernel(count, capacity, halves, *refs):
     row_refs, refs = refs[:count], refs[count:]
     (gate0, up0, down0, gate1, up1, down1), out_refs = refs[:6], refs[6:]
-    pieces = row_refs[0].shape[0] // capacity
     padded = -(-capacity // 8) * 8
     flat = jnp.concatenate([whole_rows(r[...], capacity, padded) for r in row_refs], axis=0)
     total = None
@@ -178,15 +180,21 @@
         total = part if total is None else total + part
     for k in range(count):
         values = total[k * padded : (k + 1) * padded, :]
-        out_refs[k][...] = split_rows(values, capacity, pieces).astype(jnp.bfloat16)
-
-
-def weigh_kernel(capacity, pieces, plan, early, route_ref, route2_ref, rate_ref, rate2_ref,
-                 *out_refs):
-    routes = jnp.concatenate([route_ref[...], route2_ref[...]], axis=1)
-    weights = jnp.concatenate([rate_ref[...], rate2_ref[...]], axis=1)
+        share = capacity // halves
+        for j in range(halves):
+            out_ref = out_refs[k * halves + j]
+            part = values if j == 0 else pltpu.roll(values, padded - j * share, 0)
+            part = part[: -(-share // 8) * 8]
+            out_ref[...] = split_rows(part, share, out_ref.shape[0] // share).astype(jnp.bfloat16)
+
+
+def weigh_kernel(capacity, pieces, plan, *refs):
+    count = (len(refs) - 2) // 2
+    high_ref, low_ref = refs[-2:]
+    routes = jnp.concatenate([r[...] for r in refs[:count]], axis=1)
+    weights = jnp.concatenate([r[...] for r in refs[count : 2 * count]], axis=1)
     expert = expert_column(plan)
-    ranks = slot_ranks(routes, expert)
+    ranks = slot_ranks(routes, expert, capacity // 2 if count == 2 else 0)
     scale = sum(
         jnp.where(mask, weights[c : c + 1, :], 0.0)
         for c, mask in enumerate(choice_masks(routes, expert))
@@ -196,16 +204,13 @@
     tables = [
         jnp.where(ranks[m : m + 1, :] == slot, scale[m : m + 1, :], 0.0) for m in range(len(plan))
     ]
-    for group, (high_ref, low_ref) in zip(
-        (tables[:early], tables[early:]), (out_refs[:2], out_refs[2:])
-    ):
-        for h in range(pieces):
-            table = jnp.concatenate([jnp.where(piece == h, t, 0.0) for t in group], axis=0).T
-            high = table.astype(jnp.bfloat16)
-            high_ref[h * tokens : (h + 1) * tokens, :] = high
-            low_ref[h * tokens : (h + 1) * tokens, :] = (
-                table - high.astype(jnp.float32)
-            ).astype(jnp.bfloat16)
+    for h in range(pieces):
+        table = jnp.concatenate([jnp.where(piece == h, t, 0.0) for t in tables], axis=0).T
+        high = table.astype(jnp.bfloat16)
+        high_ref[h * tokens : (h + 1) * tokens, :] = high
+        low_ref[h * tokens : (h + 1) * tokens, :] = (
+            table - high.astype(jnp.float32)
+        ).astype(jnp.bfloat16)
 
 
 def fetch_kernel(*refs):
@@ -258,25 +263,26 @@
         out_ref[...] = jnp.zeros_like(out_ref)
 
 
-def gather_into(out_ref, start_ref, row_refs, high_ref, low_ref):
+def gathered(row_refs, high_ref, low_ref, tokens):
     flat = jnp.concatenate([r[...] for r in row_refs], axis=0)
-    tokens, part = out_ref.shape[0], flat.shape[1]
-    for h in range(out_ref.shape[1] // part):
+    part = flat.shape[1]
+    for h in range(high_ref.shape[0] // tokens):
         at = slice(h * tokens, (h + 1) * tokens)
         value = jnp.dot(high_ref[at, :], flat, preferred_element_type=jnp.float32)
         value = value + jnp.dot(low_ref[at, :], flat, preferred_element_type=jnp.float32)
-        lanes = slice(h * part, (h + 1) * part)
-        out_ref[:, lanes] = value if start_ref is None else value + start_ref[:, lanes]
+        yield slice(h * part, (h + 1) * part), value
 
 
 def early_kernel(order, held_count, high_ref, low_ref, hid_ref, dgate_ref, *refs):
-    held_refs, row_refs, out_ref = refs[:held_count], refs[held_count:-1], refs[-1]
+    held_refs, row_refs = refs[:held_count], refs[held_count:-3]
+    own_ref, other_ref, sum_ref = refs[-3:]
     me, core = position()
-    gather_into(out_ref, None, row_refs, high_ref, low_ref)
+    half = own_ref.shape[0]
+    for lanes, value in gathered(row_refs, high_ref, low_ref, 2 * half):
+        sum_ref[:, lanes] = value
 
     @pl.when(core != 0)
     def _():
-        half = hid_ref.shape[0] // 2
         hid = jnp.concatenate([hid_ref[half:, :], hid_ref[:half, :]], axis=0)
         for shard, offset, ref, at in shards_of(order, held_refs):
             lanes = pl.ds(pl.multiple_of(jnp.bitwise_xor(me, offset) * shard, shard), shard)
@@ -286,15 +292,17 @@
                 (((1,), (1,)), ((), ())),
                 preferred_element_type=jnp.float32,
             )
-            out_ref[:, lanes] += jax.nn.sigmoid(dgate_ref[:, lanes]) * branch
-
-
-def late_kernel(early_ref, high_ref, low_ref, *refs):
-    row_refs, own_ref, other_ref, sum_ref = refs[:-3], refs[-3], refs[-2], refs[-1]
-    half = own_ref.shape[0]
-    gather_into(sum_ref, early_ref, row_refs, high_ref, low_ref)
+            sum_ref[:, lanes] += jax.nn.sigmoid(dgate_ref[:, lanes]) * branch
+
     own_ref[...] = sum_ref[:half, :]
     other_ref[...] = sum_ref[half:, :].astype(jnp.bfloat16)
+
+
+def late_kernel(own_ref, share_ref, high_ref, low_ref, *refs):
+    row_refs, out_ref = refs[:-1], refs[-1]
+    for lanes, value in gathered(row_refs, high_ref, low_ref, own_ref.shape[0]):
+        value = value + (own_ref[:, lanes] + share_ref[:, lanes].astype(jnp.float32))
+        out_ref[:, lanes] = value.astype(jnp.bfloat16)
 
 
 def call(kernel, outs, ins, scratch=(), spec=VMEM):
@@ -310,9 +318,9 @@
     )(*ins)
 
 
-def swapped(value, offsets):
+def swapped(value, offsets, cross=0):
     size = lax.axis_size("ep")
-    pairs = [(2 * i + c, 2 * (i ^ offsets[c]) + c) for i in range(size) for c in range(2)]
+    pairs = [(2 * i + c, 2 * (i ^ offsets[c]) + (c ^ cross)) for i in range(size) for c in range(2)]
     return lax.ppermute(value, ("ep", "tp"), pairs)
 
 
@@ -323,9 +331,13 @@
 def plan_of(sources):
     half = sources // 2
     far = [(k, k + 1) for k in range(half, sources, 2)]
-    near = [(k, k + 1) for k in range(0, half, 2)]
-    cut = len(far) // 2
-    return far[:cut] + near[1:] + near[:1] + far[cut:], cut, len(near)
+    parts = (far[: len(far) // 2], [(2, 3), (0, 1)], [(k, k + 1) for k in range(4, half, 2)],
+             far[len(far) // 2 :])
+    plan, groups = [], []
+    for part in parts:
+        groups.append(list(range(len(plan), len(plan) + len(part))))
+        plan += part
+    return plan, groups
 
 
 def bits_of(sources):
@@ -337,14 +349,16 @@
 ):
     tok_rows, width = tokens.shape
     sources = lax.axis_size("ep")
-    capacity = 2 * capacity_of(tok_rows, routes.shape[1], sources)
-    pieces = row_split(capacity, width)
+    own_capacity = capacity_of(tok_rows, routes.shape[1], sources)
+    capacity = 2 * own_capacity
+    pieces, own_pieces = row_split(capacity, width), row_split(own_capacity, width)
     bf16, f32 = jnp.bfloat16, jnp.float32
     shape = jax.ShapeDtypeStruct
-    plan, cut, near = plan_of(sources)
+    plan, (far, plane, near, last) = plan_of(sources)
     blocks = len(plan)
-    early = cut + near
-    groups = (range(cut, early), range(cut), range(early, blocks))
+    direct = near + last
+    homes = [offsets for m in direct for offsets in (plan[m], plan[m][::-1])]
+    early = far + plane
 
     gain = norm_gain.reshape(1, width)
     routes, rates = routes.T, route_weights.T
@@ -385,11 +399,16 @@
     helds = (held,) + tuple(swapped(held, (k, k)) for k in (1, 2, 3))
     order = [k ^ j for j in range(4) for k in order]
 
-    columns = (early * block.shape[0], (blocks - early) * block.shape[0])
-    high0, low0, high1, low1 = call(
-        lambda *r: weigh_kernel(capacity, pieces, plan, early, *r),
-        tuple(shape((2 * tok_rows * pieces, n), bf16) for n in columns for _ in range(2)),
+    high, low = call(
+        lambda *r: weigh_kernel(capacity, pieces, [plan[m] for m in early], *r),
+        (shape((2 * tok_rows * pieces, len(early) * block.shape[0]), bf16),) * 2,
         (routes, routes2, rates, rates2),
+    )
+    own_block = shape((own_capacity * own_pieces, width // own_pieces), bf16)
+    own_high, own_low = call(
+        lambda *r: weigh_kernel(own_capacity, own_pieces, homes, *r),
+        (shape((tok_rows * own_pieces, len(homes) * own_block.shape[0]), bf16),) * 2,
+        (routes, rates),
     )
     dense_hidden = call(
         lambda *r: hidden_kernel(order, *r),
@@ -398,28 +417,30 @@
     )
     dense_hidden = partners(dense_hidden)
     back = {}
-    for group in groups:
+    for group in (plane, far, near, last):
+        halves = 2 if group and group[0] in direct else 1
         outs = call(
-            lambda *r, c=len(group): expert_kernel(c, capacity, *r),
-            (block,) * len(group),
+            lambda *r, c=len(group), h=halves: expert_kernel(c, capacity, h, *r),
+            (own_block if halves == 2 else block,) * (len(group) * halves),
             tuple(got[m] for m in group) + own + other,
-        )
-        for m, value in zip(group, outs):
-            back[m] = swapped(value, plan[m])
-    sum0 = call(
+        ) if group else ()
+        for i, value in enumerate(outs):
+            m, cross = group[i // halves], i % halves
+            back[m, cross] = swapped(value, plan[m], cross)
+    total, share = call(
         lambda *r: early_kernel(order, len(helds), *r),
-        shape((2 * tok_rows, width), f32),
-        (high0, low0, dense_hidden, dense_gate.reshape(1, width))
+        (shape((tok_rows, width), f32), shape((tok_rows, width), bf16)),
+        (high, low, dense_hidden, dense_gate.reshape(1, width))
         + helds
-        + tuple(back[m] for m in range(early)),
-    )
-    total, share = call(
+        + tuple(back[m, 0] for m in early),
+        scratch=(pltpu.VMEM((2 * tok_rows, width), f32),),
+    )
+    share = partners(share)
+    return call(
         late_kernel,
-        (shape((tok_rows, width), f32), shape((tok_rows, width), bf16)),
-        (sum0, high1, low1) + tuple(back[m] for m in range(early, blocks)),
-        scratch=(pltpu.VMEM((2 * tok_rows, width), f32),),
-    )
-    return (total + partners(share).astype(f32)).astype(bf16)
+        shape((tok_rows, width), bf16),
+        (total, share, own_high, own_low) + tuple(back[m, c] for m in direct for c in range(2)),
+    )
 
 
 def rounded_term(hidden_rows, down_rows):

time: 121 us -> 117 us (0.967)
  the two profiles are of different devices: /device:TPU:9 before, /device:TPU:0 now
where the time goes in v3:
time: 117 us; the launch traced here: 116 us
  starting transfers between devices  51.8 us (44%)
  waiting for transfers between devices  44.6 us (38%)
  Pallas kernels  19.8 us (17%)
    ppermute x25, starting transfers between devices, swapped(): return lax.ppermute(value, ('ep', 'tp'), pairs)  46.4 us
    ppermute x25, waiting for transfers between devices, swapped(): return lax.ppermute(value, ('ep', 'tp'), pairs)  42.6 us
    pallas_call x14, Pallas kernels, call(): pl.pallas_call(kernel, out_shape=outs, in_specs=[spec for _ in ins], out_...  19.8 us
    ppermute x8, starting transfers between devices, partners(): return lax.ppermute(value, 'tp', [(0, 1), (1, 0)])  5.42 us
  transfers between devices with their start and end apart: 33, of which 15 were waited for; matrix products, arithmetic and copies ran while one was open for 0% of the time, Pallas kernels for 14%

profile of v3, /device:TPU:0, one launch (start us, length us, event | category | flops | bytes accessed | tf_op | source)
XLA Modules:
  0.0 116.4 jit_solution(10475009002633173943)
XLA Ops:
  2.3 4.1 %collective-permute-start.3 = (bf16[128,256]{1,0:T(8,128)(2,1)S(1)}, bf16[128,256]{1,0:T(8,128)(2,1)S(1)}, u32[]{:S(2)}, u32[]{:S(2)}) collective-permute-start(bf16[128,256]{1,0:T(8,128)(2,1)S(1)} %get-tuple-element.47.refs_0_), channel_id=1, source_target_pairs={{0,16},{1,17},{2,18},{3,19},{4,20},{5,21},{6,22},{7,23},{8,24},{9,... | collective-permute-start | bytes 196616 | tf_op jit(solution)/shard_map/ppermute | solution.py:324
  6.5 3.7 %collective-permute-done.3.refs_1_ = bf16[128,256]{1,0:T(8,128)(2,1)S(1)} collective-permute-done((bf16[128,256]{1,0:T(8,128)(2,1)S(1)}, bf16[128,256]{1,0:T(8,128)(2,1)S(1)}, u32[]{:S(2)}, u32[]{:S(2)}) %collective-permute-start.3) | collective-permute-done | bytes 65568 | tf_op jit(solution)/shard_map/ppermute | solution.py:324
  11.5 2.7 %collective-permute-start.4 = (bf16[256,256]{1,0:T(8,128)(2,1)S(1)}, bf16[256,256]{1,0:T(8,128)(2,1)S(1)}, u32[]{:S(2)}, u32[]{:S(2)}) collective-permute-start(bf16[256,256]{1,0:T(8,128)(2,1)S(1)} %shard_map.103.refs_0_), channel_id=1, source_target_pairs={{0,8},{1,9},{2,10},{3,11},{4,12},{5,13},{6,14},{7,15},{8,0},{9,1},... | collective-permute-start | bytes 393224 | tf_op jit(solution)/shard_map/ppermute | solution.py:324
  15.3 1.6 %collective-permute-start.16 = (bf16[88,1024]{1,0:T(8,128)(2,1)S(1)}, bf16[88,1024]{1,0:T(8,128)(2,1)S(1)}, u32[]{:S(2)}, u32[]{:S(2)}) collective-permute-start(bf16[88,1024]{1,0:T(8,128)(2,1)S(1)} %get-tuple-element.55), channel_id=1, source_target_pairs={{0,4},{1,7},{2,6},{3,5},{4,0},{5,3},{6,2},{7,1},{8,12},{9,15},{10,... | collective-permute-start | bytes 540680 | tf_op jit(solution)/shard_map/ppermute | solution.py:324
  18.7 4.0 %collective-permute-done.16.r_0_ = bf16[88,1024]{1,0:T(8,128)(2,1)S(1)} collective-permute-done((bf16[88,1024]{1,0:T(8,128)(2,1)S(1)}, bf16[88,1024]{1,0:T(8,128)(2,1)S(1)}, u32[]{:S(2)}, u32[]{:S(2)}) %collective-permute-start.16) | collective-permute-done | bytes 180256 | tf_op jit(solution)/shard_map/ppermute | solution.py:324
  24.1 1.5 %collective-permute-start.6 = (bf16[512,256]{1,0:T(8,128)(2,1)S(1)}, bf16[512,256]{1,0:T(8,128)(2,1)S(1)}, u32[]{:S(2)}, u32[]{:S(2)}) collective-permute-start(bf16[512,256]{1,0:T(8,128)(2,1)S(1)} %shard_map.104.r_1_.r_4_), channel_id=1, source_target_pairs={{0,4},{1,5},{2,6},{3,7},{4,0},{5,1},{6,2},{7,3},{8,12},{9,13},{10,... | collective-permute-start | bytes 786440 | tf_op jit(solution)/shard_map/ppermute | solution.py:324
  26.1 3.5 %collective-permute-start.10 = (bf16[88,1024]{1,0:T(8,128)(2,1)S(1)}, bf16[88,1024]{1,0:T(8,128)(2,1)S(1)}, u32[]{:S(2)}, u32[]{:S(2)}) collective-permute-start(bf16[88,1024]{1,0:T(8,128)(2,1)S(1)} %get-tuple-element.49), channel_id=1, source_target_pairs={{0,20},{1,23},{2,22},{3,21},{4,16},{5,19},{6,18},{7,17},{8,28},{9,... | collective-permute-start | bytes 540680 | tf_op jit(solution)/shard_map/ppermute | solution.py:324
  30.0 2.9 %shard_map.106 = (bf16[2048,512]{1,0:T(8,128)(2,1)S(1)}, bf16[2048,512]{1,0:T(8,128)(2,1)S(1)}, bf16[512,2048]{1,0:T(8,128)(2,1)S(1)}) custom-call(bf16[1,2048,512]{2,1,0:T(8,128)(2,1)} %refs_0_.1, bf16[1,2048,512]{2,1,0:T(8,128)(2,1)} %refs_1_.1, bf16[1,512,2048]{2,1,0:T(8,128)(2,1)} %refs_2_.1), custom_call_target="tpu_custom_call" | custom-call | tf_op jit(solution)/shard_map/pallas_call | solution.py:311
  32.9 2.4 %shard_map.108 = (bf16[88,1024]{1,0:T(8,128)(2,1)S(1)}, bf16[88,1024]{1,0:T(8,128)(2,1)S(1)}) custom-call(bf16[88,1024]{1,0:T(8,128)(2,1)S(1)} %collective-permute-done.16.r_0_, bf16[88,1024]{1,0:T(8,128)(2,1)S(1)} %collective-permute-done.17.r_1_, bf16[2048,512]{1,0:T(8,128)(2,1)S(1)} %get-tuple-element.50.r_2_, ...), custom_call_target="tpu_custom_call" | custom-call | tf_op jit(solution)/shard_map/pallas_call | solution.py:311
  35.3 7.5 %collective-permute-done.10.r_1_ = bf16[88,1024]{1,0:T(8,128)(2,1)S(1)} collective-permute-done((bf16[88,1024]{1,0:T(8,128)(2,1)S(1)}, bf16[88,1024]{1,0:T(8,128)(2,1)S(1)}, u32[]{:S(2)}, u32[]{:S(2)}) %collective-permute-start.10) | collective-permute-done | bytes 180256 | tf_op jit(solution)/shard_map/ppermute | solution.py:324
  42.8 1.7 %collective-permute-start.18 = (bf16[88,1024]{1,0:T(8,128)(2,1)S(1)}, bf16[88,1024]{1,0:T(8,128)(2,1)S(1)}, u32[]{:S(2)}, u32[]{:S(2)}) collective-permute-start(bf16[88,1024]{1,0:T(8,128)(2,1)S(1)} %get-tuple-element.57), channel_id=1, source_target_pairs={{0,4},{1,7},{2,6},{3,5},{4,0},{5,3},{6,2},{7,1},{8,12},{9,15},{10,... | collective-permute-start | bytes 540680 | tf_op jit(solution)/shard_map/ppermute | solution.py:324
  46.7 2.4 %shard_map.107 = (bf16[88,1024]{1,0:T(8,128)(2,1)S(1)}, bf16[88,1024]{1,0:T(8,128)(2,1)S(1)}) custom-call(bf16[88,1024]{1,0:T(8,128)(2,1)S(1)} %collective-permute-done.9.r_0_, bf16[88,1024]{1,0:T(8,128)(2,1)S(1)} %collective-permute-done.10.r_1_, bf16[2048,512]{1,0:T(8,128)(2,1)S(1)} %get-tuple-element.50.r_2_, ...), custom_call_target="tpu_custom_call" | custom-call | tf_op jit(solution)/shard_map/pallas_call | solution.py:311
  49.2 3.0 %collective-permute-start.15 = (bf16[88,1024]{1,0:T(8,128)(2,1)S(1)}, bf16[88,1024]{1,0:T(8,128)(2,1)S(1)}, u32[]{:S(2)}, u32[]{:S(2)}) collective-permute-start(bf16[88,1024]{1,0:T(8,128)(2,1)S(1)} %get-tuple-element.54), channel_id=1, source_target_pairs={{0,20},{1,23},{2,22},{3,21},{4,16},{5,19},{6,18},{7,17},{8,28},{9,... | collective-permute-start | bytes 540680 | tf_op jit(solution)/shard_map/ppermute | solution.py:324
  52.2 1.9 %collective-permute-start.1 = (f32[2,128]{1,0:T(2,128)S(1)}, f32[2,128]{1,0:T(2,128)S(1)}, u32[]{:S(2)}, u32[]{:S(2)}) collective-permute-start(f32[2,128]{1,0:T(2,128)S(1)} %bitcast.15), channel_id=1, source_target_pairs={{0,1},{1,0},{2,3},{3,2},{4,5},{5,4},{6,7},{7,6},{8,9},{9,8},{10,11... | collective-permute-start | bytes 3080 | tf_op jit(solution)/shard_map/ppermute | solution.py:328
  56.2 8.4 %collective-permute-done.14.r_8_ = bf16[88,1024]{1,0:T(8,128)(2,1)S(1)} collective-permute-done((bf16[88,1024]{1,0:T(8,128)(2,1)S(1)}, bf16[88,1024]{1,0:T(8,128)(2,1)S(1)}, u32[]{:S(2)}, u32[]{:S(2)}) %collective-permute-start.14) | collective-permute-done | bytes 180256 | tf_op jit(solution)/shard_map/ppermute | solution.py:324
  64.6 4.0 %collective-permute-done.15.r_9_ = bf16[88,1024]{1,0:T(8,128)(2,1)S(1)} collective-permute-done((bf16[88,1024]{1,0:T(8,128)(2,1)S(1)}, bf16[88,1024]{1,0:T(8,128)(2,1)S(1)}, u32[]{:S(2)}, u32[]{:S(2)}) %collective-permute-start.15) | collective-permute-done | bytes 180256 | tf_op jit(solution)/shard_map/ppermute | solution.py:324
  70.0 2.2 %collective-permute-start.20 = (bf16[128,2048]{1,0:T(8,128)(2,1)S(1)}, bf16[128,2048]{1,0:T(8,128)(2,1)S(1)}, u32[]{:S(2)}, u32[]{:S(2)}) collective-permute-start(bf16[128,2048]{1,0:T(8,128)(2,1)S(1)} %get-tuple-element.60), channel_id=1, source_target_pairs={{0,1},{1,0},{2,3},{3,2},{4,5},{5,4},{6,7},{7,6},{8,9},{9,8},{10,11... | collective-permute-start | bytes 1572872 | tf_op jit(solution)/shard_map/ppermute | solution.py:328
  73.1 3.9 %collective-permute-start.28 = (bf16[88,1024]{1,0:T(8,128)(2,1)S(1)}, bf16[88,1024]{1,0:T(8,128)(2,1)S(1)}, u32[]{:S(2)}, u32[]{:S(2)}) collective-permute-start(bf16[88,1024]{1,0:T(8,128)(2,1)S(1)} %get-tuple-element.70), channel_id=1, source_target_pairs={{0,28},{1,31},{2,30},{3,29},{4,24},{5,27},{6,26},{7,25},{8,20},{9,... | collective-permute-start | bytes 540680 | tf_op jit(solution)/shard_map/ppermute | solution.py:324
  77.0 1.9 %collective-permute-start.22 = (bf16[88,1024]{1,0:T(8,128)(2,1)S(1)}, bf16[88,1024]{1,0:T(8,128)(2,1)S(1)}, u32[]{:S(2)}, u32[]{:S(2)}) collective-permute-start(bf16[88,1024]{1,0:T(8,128)(2,1)S(1)} %get-tuple-element.64), channel_id=1, source_target_pairs={{0,12},{1,15},{2,14},{3,13},{4,8},{5,11},{6,10},{7,9},{8,4},{9,7},... | collective-permute-start | bytes 540680 | tf_op jit(solution)/shard_map/ppermute | solution.py:324
  78.9 2.7 %collective-permute-done.27.r_0_ = bf16[88,1024]{1,0:T(8,128)(2,1)S(1)} collective-permute-done((bf16[88,1024]{1,0:T(8,128)(2,1)S(1)}, bf16[88,1024]{1,0:T(8,128)(2,1)S(1)}, u32[]{:S(2)}, u32[]{:S(2)}) %collective-permute-start.27) | collective-permute-done | bytes 180256 | tf_op jit(solution)/shard_map/ppermute | solution.py:324
  81.6 4.7 %collective-permute-done.28.r_1_ = bf16[88,1024]{1,0:T(8,128)(2,1)S(1)} collective-permute-done((bf16[88,1024]{1,0:T(8,128)(2,1)S(1)}, bf16[88,1024]{1,0:T(8,128)(2,1)S(1)}, u32[]{:S(2)}, u32[]{:S(2)}) %collective-permute-start.28) | collective-permute-done | bytes 180256 | tf_op jit(solution)/shard_map/ppermute | solution.py:324
  86.3 2.4 %shard_map.112 = (bf16[88,512]{1,0:T(8,128)(2,1)S(1)}, bf16[88,512]{1,0:T(8,128)(2,1)S(1)}, bf16[88,512]{1,0:T(8,128)(2,1)S(1)}, bf16[88,512]{1,0:T(8,128)(2,1)S(1)}) custom-call(bf16[88,1024]{1,0:T(8,128)(2,1)S(1)} %collective-permute-done.27.r_0_, bf16[88,1024]{1,0:T(8,128)(2,1)S(1)} %collective-permute-done.28.r_1_, ...), custom_call_target="tpu_custom_call" | custom-call | tf_op jit(solution)/shard_map/pallas_call | solution.py:311
  89.3 2.1 %collective-permute-start.30 = (bf16[88,512]{1,0:T(8,128)(2,1)S(1)}, bf16[88,512]{1,0:T(8,128)(2,1)S(1)}, u32[]{:S(2)}, u32[]{:S(2)}) collective-permute-start(bf16[88,512]{1,0:T(8,128)(2,1)S(1)} %get-tuple-element.72), channel_id=1, source_target_pairs={{0,25},{1,26},{2,27},{3,24},{4,29},{5,30},{6,31},{7,28},{8,17},{9,... | collective-permute-start | bytes 270344 | tf_op jit(solution)/shard_map/ppermute | solution.py:324
  91.4 1.6 %collective-permute-start.31 = (bf16[88,512]{1,0:T(8,128)(2,1)S(1)}, bf16[88,512]{1,0:T(8,128)(2,1)S(1)}, u32[]{:S(2)}, u32[]{:S(2)}) collective-permute-start(bf16[88,512]{1,0:T(8,128)(2,1)S(1)} %get-tuple-element.73), channel_id=1, source_target_pairs={{0,28},{1,31},{2,30},{3,29},{4,24},{5,27},{6,26},{7,25},{8,20},{9,... | collective-permute-start | bytes 270344 | tf_op jit(solution)/shard_map/ppermute | solution.py:324
  94.1 3.6 %collective-permute-start.32 = (bf16[88,512]{1,0:T(8,128)(2,1)S(1)}, bf16[88,512]{1,0:T(8,128)(2,1)S(1)}, u32[]{:S(2)}, u32[]{:S(2)}) collective-permute-start(bf16[88,512]{1,0:T(8,128)(2,1)S(1)} %get-tuple-element.74), channel_id=1, source_target_pairs={{0,29},{1,30},{2,31},{3,28},{4,25},{5,26},{6,27},{7,24},{8,21},{9,... | collective-permute-start | bytes 270344 | tf_op jit(solution)/shard_map/ppermute | solution.py:324
  97.7 2.4 %shard_map.111 = (bf16[88,512]{1,0:T(8,128)(2,1)S(1)}, bf16[88,512]{1,0:T(8,128)(2,1)S(1)}, bf16[88,512]{1,0:T(8,128)(2,1)S(1)}, bf16[88,512]{1,0:T(8,128)(2,1)S(1)}) custom-call(bf16[88,1024]{1,0:T(8,128)(2,1)S(1)} %collective-permute-done.21.r_0_, bf16[88,1024]{1,0:T(8,128)(2,1)S(1)} %collective-permute-done.22.r_1_, ...), custom_call_target="tpu_custom_call" | custom-call | tf_op jit(solution)/shard_map/pallas_call | solution.py:311
  100.1 3.3 %collective-permute-start.23 = (bf16[88,512]{1,0:T(8,128)(2,1)S(1)}, bf16[88,512]{1,0:T(8,128)(2,1)S(1)}, u32[]{:S(2)}, u32[]{:S(2)}) collective-permute-start(bf16[88,512]{1,0:T(8,128)(2,1)S(1)} %get-tuple-element.65), channel_id=1, source_target_pairs={{0,8},{1,11},{2,10},{3,9},{4,12},{5,15},{6,14},{7,13},{8,0},{9,3},... | collective-permute-start | bytes 270344 | tf_op jit(solution)/shard_map/ppermute | solution.py:324
  103.4 1.6 %collective-permute-start.24 = (bf16[88,512]{1,0:T(8,128)(2,1)S(1)}, bf16[88,512]{1,0:T(8,128)(2,1)S(1)}, u32[]{:S(2)}, u32[]{:S(2)}) collective-permute-start(bf16[88,512]{1,0:T(8,128)(2,1)S(1)} %get-tuple-element.66), channel_id=1, source_target_pairs={{0,9},{1,10},{2,11},{3,8},{4,13},{5,14},{6,15},{7,12},{8,1},{9,2},... | collective-permute-start | bytes 270344 | tf_op jit(solution)/shard_map/ppermute | solution.py:324
  105.0 3.1 %collective-permute-start.25 = (bf16[88,512]{1,0:T(8,128)(2,1)S(1)}, bf16[88,512]{1,0:T(8,128)(2,1)S(1)}, u32[]{:S(2)}, u32[]{:S(2)}) collective-permute-start(bf16[88,512]{1,0:T(8,128)(2,1)S(1)} %get-tuple-element.67), channel_id=1, source_target_pairs={{0,12},{1,15},{2,14},{3,13},{4,8},{5,11},{6,10},{7,9},{8,4},{9,7},... | collective-permute-start | bytes 270344 | tf_op jit(solution)/shard_map/ppermute | solution.py:324
  108.1 1.6 %collective-permute-start.26 = (bf16[88,512]{1,0:T(8,128)(2,1)S(1)}, bf16[88,512]{1,0:T(8,128)(2,1)S(1)}, u32[]{:S(2)}, u32[]{:S(2)}) collective-permute-start(bf16[88,512]{1,0:T(8,128)(2,1)S(1)} %get-tuple-element.68), channel_id=1, source_target_pairs={{0,13},{1,14},{2,15},{3,12},{4,9},{5,10},{6,11},{7,8},{8,5},{9,6},... | collective-permute-start | bytes 270344 | tf_op jit(solution)/shard_map/ppermute | solution.py:324
  111.0 3.6 %collective-permute-done.26.refs_3_ = bf16[88,512]{1,0:T(8,128)(2,1)S(1)} collective-permute-done((bf16[88,512]{1,0:T(8,128)(2,1)S(1)}, bf16[88,512]{1,0:T(8,128)(2,1)S(1)}, u32[]{:S(2)}, u32[]{:S(2)}) %collective-permute-start.26) | collective-permute-done | bytes 90144 | tf_op jit(solution)/shard_map/ppermute | solution.py:324
  114.6 1.8 %shard_map.113 = bf16[128,2048]{1,0:T(8,128)(2,1)} custom-call(f32[128,2048]{1,0:T(8,128)S(1)} %get-tuple-element.59.own_ref, bf16[128,2048]{1,0:T(8,128)(2,1)S(1)} %collective-permute-done.20.share_ref, bf16[512,704]{1,0:T(8,128)(2,1)S(1)} %get-tuple-element.61.high_ref, bf16[512,704]{1,0:T(8,128)(2,1)S(1)} %get-tuple-element.62.low_ref, ...), custom_call_target="tpu_custom_call" | custom-call | tf_op jit(solution)/shard_map/pallas_call | solution.py:311
  (52 shorter events, 18.4 us)
Async XLA Ops:
  0.0 25.6 %collective-permute-start.11 = (bf16[2048,512]{1,0:T(8,128)(2,1)}, bf16[2048,512]{1,0:T(8,128)(2,1)S(1)}, u32[]{:S(2)}, u32[]{:S(2)}) collective-permute-start(bf16[2048,512]{1,0:T(8,128)(2,1)} %bitcast.8), channel_id=1, source_target_pairs={{0,1},{1,0},{2,3},{3,2},{4,5},{5,4},{6,7},{7,6},{8,9},{9,8},{10,11... | collective-permute-start | bytes 6291464 | tf_op jit(solution)/shard_map/ppermute | solution.py:328
  0.5 25.6 %collective-permute-start.12 = (bf16[2048,512]{1,0:T(8,128)(2,1)}, bf16[2048,512]{1,0:T(8,128)(2,1)S(1)}, u32[]{:S(2)}, u32[]{:S(2)}) collective-permute-start(bf16[2048,512]{1,0:T(8,128)(2,1)} %bitcast.9), channel_id=1, source_target_pairs={{0,1},{1,0},{2,3},{3,2},{4,5},{5,4},{6,7},{7,6},{8,9},{9,8},{10,11... | collective-permute-start | bytes 6291464 | tf_op jit(solution)/shard_map/ppermute | solution.py:328
  0.5 29.2 %collective-permute-start.13 = (bf16[512,2048]{1,0:T(8,128)(2,1)}, bf16[512,2048]{1,0:T(8,128)(2,1)S(1)}, u32[]{:S(2)}, u32[]{:S(2)}) collective-permute-start(bf16[512,2048]{1,0:T(8,128)(2,1)} %bitcast.10), channel_id=1, source_target_pairs={{0,1},{1,0},{2,3},{3,2},{4,5},{5,4},{6,7},{7,6},{8,9},{9,8},{10,11... | collective-permute-start | bytes 6291464 | tf_op jit(solution)/shard_map/ppermute | solution.py:328
  1.0 13.2 %collective-permute-start.2 = (bf16[128,2048]{1,0:T(8,128)(2,1)}, bf16[128,2048]{1,0:T(8,128)(2,1)S(1)}, u32[]{:S(2)}, u32[]{:S(2)}) collective-permute-start(bf16[128,2048]{1,0:T(8,128)(2,1)} %tok_ref.1), channel_id=1, source_target_pairs={{0,1},{1,0},{2,3},{3,2},{4,5},{5,4},{6,7},{7,6},{8,9},{9,8},{10,11... | collective-permute-start | bytes 1572872 | tf_op jit(solution)/shard_map/ppermute | solution.py:328
  2.3 7.8 %collective-permute-start.3 = (bf16[128,256]{1,0:T(8,128)(2,1)S(1)}, bf16[128,256]{1,0:T(8,128)(2,1)S(1)}, u32[]{:S(2)}, u32[]{:S(2)}) collective-permute-start(bf16[128,256]{1,0:T(8,128)(2,1)S(1)} %get-tuple-element.47.refs_0_), channel_id=1, source_target_pairs={{0,16},{1,17},{2,18},{3,19},{4,20},{5,21},{6,22},{7,23},{8,24},{9,... | collective-permute-start | bytes 196616 | tf_op jit(solution)/shard_map/ppermute | solution.py:324
  10.1 1.4 %collective-permute-start = (s32[2,128]{1,0:T(2,128)}, s32[2,128]{1,0:T(2,128)S(1)}, u32[]{:S(2)}, u32[]{:S(2)}) collective-permute-start(s32[2,128]{1,0:T(2,128)} %bitcast.13), channel_id=1, source_target_pairs={{0,1},{1,0},{2,3},{3,2},{4,5},{5,4},{6,7},{7,6},{8,9},{9,8},{10,11... | collective-permute-start | bytes 3080 | tf_op jit(solution)/shard_map/ppermute | solution.py:328
  11.5 6.5 %collective-permute-start.4 = (bf16[256,256]{1,0:T(8,128)(2,1)S(1)}, bf16[256,256]{1,0:T(8,128)(2,1)S(1)}, u32[]{:S(2)}, u32[]{:S(2)}) collective-permute-start(bf16[256,256]{1,0:T(8,128)(2,1)S(1)} %shard_map.103.refs_0_), channel_id=1, source_target_pairs={{0,8},{1,9},{2,10},{3,11},{4,12},{5,13},{6,14},{7,15},{8,0},{9,1},... | collective-permute-start | bytes 393224 | tf_op jit(solution)/shard_map/ppermute | solution.py:324
  15.3 7.3 %collective-permute-start.16 = (bf16[88,1024]{1,0:T(8,128)(2,1)S(1)}, bf16[88,1024]{1,0:T(8,128)(2,1)S(1)}, u32[]{:S(2)}, u32[]{:S(2)}) collective-permute-start(bf16[88,1024]{1,0:T(8,128)(2,1)S(1)} %get-tuple-element.55), channel_id=1, source_target_pairs={{0,4},{1,7},{2,6},{3,5},{4,0},{5,3},{6,2},{7,1},{8,12},{9,15},{10,... | collective-permute-start | bytes 540680 | tf_op jit(solution)/shard_map/ppermute | solution.py:324
  18.0 6.1 %collective-permute-start.17 = (bf16[88,1024]{1,0:T(8,128)(2,1)S(1)}, bf16[88,1024]{1,0:T(8,128)(2,1)S(1)}, u32[]{:S(2)}, u32[]{:S(2)}) collective-permute-start(bf16[88,1024]{1,0:T(8,128)(2,1)S(1)} %get-tuple-element.56), channel_id=1, source_target_pairs={{0,0},{1,3},{2,2},{3,1},{4,4},{5,7},{6,6},{7,5},{8,8},{9,11},{10,1... | collective-permute-start | bytes 540680 | tf_op jit(solution)/shard_map/ppermute | solution.py:324
  22.6 26.5 %collective-permute-start.5 = (bf16[512,256]{1,0:T(8,128)(2,1)S(1)}, bf16[512,256]{1,0:T(8,128)(2,1)S(1)}, u32[]{:S(2)}, u32[]{:S(2)}) collective-permute-start(bf16[512,256]{1,0:T(8,128)(2,1)S(1)} %shard_map.104.r_1_.r_4_), channel_id=1, source_target_pairs={{0,2},{1,3},{2,0},{3,1},{4,6},{5,7},{6,4},{7,5},{8,10},{9,11},{10,... | collective-permute-start | bytes 786440 | tf_op jit(solution)/shard_map/ppermute | solution.py:324
  24.1 25.1 %collective-permute-start.6 = (bf16[512,256]{1,0:T(8,128)(2,1)S(1)}, bf16[512,256]{1,0:T(8,128)(2,1)S(1)}, u32[]{:S(2)}, u32[]{:S(2)}) collective-permute-start(bf16[512,256]{1,0:T(8,128)(2,1)S(1)} %shard_map.104.r_1_.r_4_), channel_id=1, source_target_pairs={{0,4},{1,5},{2,6},{3,7},{4,0},{5,1},{6,2},{7,3},{8,12},{9,13},{10,... | collective-permute-start | bytes 786440 | tf_op jit(solution)/shard_map/ppermute | solution.py:324
  25.6 26.5 %collective-permute-start.7 = (bf16[512,256]{1,0:T(8,128)(2,1)S(1)}, bf16[512,256]{1,0:T(8,128)(2,1)S(1)}, u32[]{:S(2)}, u32[]{:S(2)}) collective-permute-start(bf16[512,256]{1,0:T(8,128)(2,1)S(1)} %shard_map.104.r_1_.r_4_), channel_id=1, source_target_pairs={{0,6},{1,7},{2,4},{3,5},{4,2},{5,3},{6,0},{7,1},{8,14},{9,15},{10,... | collective-permute-start | bytes 786440 | tf_op jit(solution)/shard_map/ppermute | solution.py:324
  26.1 16.7 %collective-permute-start.10 = (bf16[88,1024]{1,0:T(8,128)(2,1)S(1)}, bf16[88,1024]{1,0:T(8,128)(2,1)S(1)}, u32[]{:S(2)}, u32[]{:S(2)}) collective-permute-start(bf16[88,1024]{1,0:T(8,128)(2,1)S(1)} %get-tuple-element.49), channel_id=1, source_target_pairs={{0,20},{1,23},{2,22},{3,21},{4,16},{5,19},{6,18},{7,17},{8,28},{9,... | collective-permute-start | bytes 540680 | tf_op jit(solution)/shard_map/ppermute | solution.py:324
  29.7 16.2 %collective-permute-start.9 = (bf16[88,1024]{1,0:T(8,128)(2,1)S(1)}, bf16[88,1024]{1,0:T(8,128)(2,1)S(1)}, u32[]{:S(2)}, u32[]{:S(2)}) collective-permute-start(bf16[88,1024]{1,0:T(8,128)(2,1)S(1)} %get-tuple-element.48), channel_id=1, source_target_pairs={{0,16},{1,19},{2,18},{3,17},{4,20},{5,23},{6,22},{7,21},{8,24},{9,... | collective-permute-start | bytes 540680 | tf_op jit(solution)/shard_map/ppermute | solution.py:324
  42.8 13.4 %collective-permute-start.18 = (bf16[88,1024]{1,0:T(8,128)(2,1)S(1)}, bf16[88,1024]{1,0:T(8,128)(2,1)S(1)}, u32[]{:S(2)}, u32[]{:S(2)}) collective-permute-start(bf16[88,1024]{1,0:T(8,128)(2,1)S(1)} %get-tuple-element.57), channel_id=1, source_target_pairs={{0,4},{1,7},{2,6},{3,5},{4,0},{5,3},{6,2},{7,1},{8,12},{9,15},{10,... | collective-permute-start | bytes 540680 | tf_op jit(solution)/shard_map/ppermute | solution.py:324
  45.9 10.3 %collective-permute-start.19 = (bf16[88,1024]{1,0:T(8,128)(2,1)S(1)}, bf16[88,1024]{1,0:T(8,128)(2,1)S(1)}, u32[]{:S(2)}, u32[]{:S(2)}) collective-permute-start(bf16[88,1024]{1,0:T(8,128)(2,1)S(1)} %get-tuple-element.58), channel_id=1, source_target_pairs={{0,0},{1,3},{2,2},{3,1},{4,4},{5,7},{6,6},{7,5},{8,8},{9,11},{10,1... | collective-permute-start | bytes 540680 | tf_op jit(solution)/shard_map/ppermute | solution.py:324
  49.1 15.4 %collective-permute-start.14 = (bf16[88,1024]{1,0:T(8,128)(2,1)S(1)}, bf16[88,1024]{1,0:T(8,128)(2,1)S(1)}, u32[]{:S(2)}, u32[]{:S(2)}) collective-permute-start(bf16[88,1024]{1,0:T(8,128)(2,1)S(1)} %get-tuple-element.53), channel_id=1, source_target_pairs={{0,16},{1,19},{2,18},{3,17},{4,20},{5,23},{6,22},{7,21},{8,24},{9,... | collective-permute-start | bytes 540680 | tf_op jit(solution)/shard_map/ppermute | solution.py:324
  49.2 19.4 %collective-permute-start.15 = (bf16[88,1024]{1,0:T(8,128)(2,1)S(1)}, bf16[88,1024]{1,0:T(8,128)(2,1)S(1)}, u32[]{:S(2)}, u32[]{:S(2)}) collective-permute-start(bf16[88,1024]{1,0:T(8,128)(2,1)S(1)} %get-tuple-element.54), channel_id=1, source_target_pairs={{0,20},{1,23},{2,22},{3,21},{4,16},{5,19},{6,18},{7,17},{8,28},{9,... | collective-permute-start | bytes 540680 | tf_op jit(solution)/shard_map/ppermute | solution.py:324
  52.2 2.7 %collective-permute-start.1 = (f32[2,128]{1,0:T(2,128)S(1)}, f32[2,128]{1,0:T(2,128)S(1)}, u32[]{:S(2)}, u32[]{:S(2)}) collective-permute-start(f32[2,128]{1,0:T(2,128)S(1)} %bitcast.15), channel_id=1, source_target_pairs={{0,1},{1,0},{2,3},{3,2},{4,5},{5,4},{6,7},{7,6},{8,9},{9,8},{10,11... | collective-permute-start | bytes 3080 | tf_op jit(solution)/shard_map/ppermute | solution.py:328
  70.0 44.7 %collective-permute-start.20 = (bf16[128,2048]{1,0:T(8,128)(2,1)S(1)}, bf16[128,2048]{1,0:T(8,128)(2,1)S(1)}, u32[]{:S(2)}, u32[]{:S(2)}) collective-permute-start(bf16[128,2048]{1,0:T(8,128)(2,1)S(1)} %get-tuple-element.60), channel_id=1, source_target_pairs={{0,1},{1,0},{2,3},{3,2},{4,5},{5,4},{6,7},{7,6},{8,9},{9,8},{10,11... | collective-permute-start | bytes 1572872 | tf_op jit(solution)/shard_map/ppermute | solution.py:328
  72.2 9.4 %collective-permute-start.27 = (bf16[88,1024]{1,0:T(8,128)(2,1)S(1)}, bf16[88,1024]{1,0:T(8,128)(2,1)S(1)}, u32[]{:S(2)}, u32[]{:S(2)}) collective-permute-start(bf16[88,1024]{1,0:T(8,128)(2,1)S(1)} %get-tuple-element.69), channel_id=1, source_target_pairs={{0,24},{1,27},{2,26},{3,25},{4,28},{5,31},{6,30},{7,29},{8,16},{9,... | collective-permute-start | bytes 540680 | tf_op jit(solution)/shard_map/ppermute | solution.py:324
  73.1 13.2 %collective-permute-start.28 = (bf16[88,1024]{1,0:T(8,128)(2,1)S(1)}, bf16[88,1024]{1,0:T(8,128)(2,1)S(1)}, u32[]{:S(2)}, u32[]{:S(2)}) collective-permute-start(bf16[88,1024]{1,0:T(8,128)(2,1)S(1)} %get-tuple-element.70), channel_id=1, source_target_pairs={{0,28},{1,31},{2,30},{3,29},{4,24},{5,27},{6,26},{7,25},{8,20},{9,... | collective-permute-start | bytes 540680 | tf_op jit(solution)/shard_map/ppermute | solution.py:324
  77.0 14.5 %collective-permute-start.21 = (bf16[88,1024]{1,0:T(8,128)(2,1)S(1)}, bf16[88,1024]{1,0:T(8,128)(2,1)S(1)}, u32[]{:S(2)}, u32[]{:S(2)}) collective-permute-start(bf16[88,1024]{1,0:T(8,128)(2,1)S(1)} %get-tuple-element.63), channel_id=1, source_target_pairs={{0,8},{1,11},{2,10},{3,9},{4,12},{5,15},{6,14},{7,13},{8,0},{9,3},... | collective-permute-start | bytes 540680 | tf_op jit(solution)/shard_map/ppermute | solution.py:324
  77.0 17.1 %collective-permute-start.22 = (bf16[88,1024]{1,0:T(8,128)(2,1)S(1)}, bf16[88,1024]{1,0:T(8,128)(2,1)S(1)}, u32[]{:S(2)}, u32[]{:S(2)}) collective-permute-start(bf16[88,1024]{1,0:T(8,128)(2,1)S(1)} %get-tuple-element.64), channel_id=1, source_target_pairs={{0,12},{1,15},{2,14},{3,13},{4,8},{5,11},{6,10},{7,9},{8,4},{9,7},... | collective-permute-start | bytes 540680 | tf_op jit(solution)/shard_map/ppermute | solution.py:324
  88.7 11.4 %collective-permute-start.29 = (bf16[88,512]{1,0:T(8,128)(2,1)S(1)}, bf16[88,512]{1,0:T(8,128)(2,1)S(1)}, u32[]{:S(2)}, u32[]{:S(2)}) collective-permute-start(bf16[88,512]{1,0:T(8,128)(2,1)S(1)} %get-tuple-element.71), channel_id=1, source_target_pairs={{0,24},{1,27},{2,26},{3,25},{4,28},{5,31},{6,30},{7,29},{8,16},{9,... | collective-permute-start | bytes 270344 | tf_op jit(solution)/shard_map/ppermute | solution.py:324
  89.3 14.1 %collective-permute-start.30 = (bf16[88,512]{1,0:T(8,128)(2,1)S(1)}, bf16[88,512]{1,0:T(8,128)(2,1)S(1)}, u32[]{:S(2)}, u32[]{:S(2)}) collective-permute-start(bf16[88,512]{1,0:T(8,128)(2,1)S(1)} %get-tuple-element.72), channel_id=1, source_target_pairs={{0,25},{1,26},{2,27},{3,24},{4,29},{5,30},{6,31},{7,28},{8,17},{9,... | collective-permute-start | bytes 270344 | tf_op jit(solution)/shard_map/ppermute | solution.py:324
  91.4 13.6 %collective-permute-start.31 = (bf16[88,512]{1,0:T(8,128)(2,1)S(1)}, bf16[88,512]{1,0:T(8,128)(2,1)S(1)}, u32[]{:S(2)}, u32[]{:S(2)}) collective-permute-start(bf16[88,512]{1,0:T(8,128)(2,1)S(1)} %get-tuple-element.73), channel_id=1, source_target_pairs={{0,28},{1,31},{2,30},{3,29},{4,24},{5,27},{6,26},{7,25},{8,20},{9,... | collective-permute-start | bytes 270344 | tf_op jit(solution)/shard_map/ppermute | solution.py:324
  94.1 14.1 %collective-permute-start.32 = (bf16[88,512]{1,0:T(8,128)(2,1)S(1)}, bf16[88,512]{1,0:T(8,128)(2,1)S(1)}, u32[]{:S(2)}, u32[]{:S(2)}) collective-permute-start(bf16[88,512]{1,0:T(8,128)(2,1)S(1)} %get-tuple-element.74), channel_id=1, source_target_pairs={{0,29},{1,30},{2,31},{3,28},{4,25},{5,26},{6,27},{7,24},{8,21},{9,... | collective-permute-start | bytes 270344 | tf_op jit(solution)/shard_map/ppermute | solution.py:324
  100.1 10.3 %collective-permute-start.23 = (bf16[88,512]{1,0:T(8,128)(2,1)S(1)}, bf16[88,512]{1,0:T(8,128)(2,1)S(1)}, u32[]{:S(2)}, u32[]{:S(2)}) collective-permute-start(bf16[88,512]{1,0:T(8,128)(2,1)S(1)} %get-tuple-element.65), channel_id=1, source_target_pairs={{0,8},{1,11},{2,10},{3,9},{4,12},{5,15},{6,14},{7,13},{8,0},{9,3},... | collective-permute-start | bytes 270344 | tf_op jit(solution)/shard_map/ppermute | solution.py:324
  103.4 7.0 %collective-permute-start.24 = (bf16[88,512]{1,0:T(8,128)(2,1)S(1)}, bf16[88,512]{1,0:T(8,128)(2,1)S(1)}, u32[]{:S(2)}, u32[]{:S(2)}) collective-permute-start(bf16[88,512]{1,0:T(8,128)(2,1)S(1)} %get-tuple-element.66), channel_id=1, source_target_pairs={{0,9},{1,10},{2,11},{3,8},{4,13},{5,14},{6,15},{7,12},{8,1},{9,2},... | collective-permute-start | bytes 270344 | tf_op jit(solution)/shard_map/ppermute | solution.py:324
  105.0 6.0 %collective-permute-start.25 = (bf16[88,512]{1,0:T(8,128)(2,1)S(1)}, bf16[88,512]{1,0:T(8,128)(2,1)S(1)}, u32[]{:S(2)}, u32[]{:S(2)}) collective-permute-start(bf16[88,512]{1,0:T(8,128)(2,1)S(1)} %get-tuple-element.67), channel_id=1, source_target_pairs={{0,12},{1,15},{2,14},{3,13},{4,8},{5,11},{6,10},{7,9},{8,4},{9,7},... | collective-permute-start | bytes 270344 | tf_op jit(solution)/shard_map/ppermute | solution.py:324
  108.1 6.5 %collective-permute-start.26 = (bf16[88,512]{1,0:T(8,128)(2,1)S(1)}, bf16[88,512]{1,0:T(8,128)(2,1)S(1)}, u32[]{:S(2)}, u32[]{:S(2)}) collective-permute-start(bf16[88,512]{1,0:T(8,128)(2,1)S(1)} %get-tuple-element.68), channel_id=1, source_target_pairs={{0,13},{1,14},{2,15},{3,12},{4,9},{5,10},{6,11},{7,8},{8,5},{9,6},... | collective-permute-start | bytes 270344 | tf_op jit(solution)/shard_map/ppermute | solution.py:324
  (3 other events, 27.1 us)

commit v4 on v3

--- a/solution.py
+++ b/solution.py
@@ -189,8 +189,7 @@
 
 
 def weigh_kernel(capacity, pieces, plan, *refs):
-    count = (len(refs) - 2) // 2
-    high_ref, low_ref = refs[-2:]
+    count, table_ref = (len(refs) - 1) // 2, refs[-1]
     routes = jnp.concatenate([r[...] for r in refs[:count]], axis=1)
     weights = jnp.concatenate([r[...] for r in refs[count : 2 * count]], axis=1)
     expert = expert_column(plan)
@@ -207,10 +206,9 @@
     for h in range(pieces):
         table = jnp.concatenate([jnp.where(piece == h, t, 0.0) for t in tables], axis=0).T
         high = table.astype(jnp.bfloat16)
-        high_ref[h * tokens : (h + 1) * tokens, :] = high
-        low_ref[h * tokens : (h + 1) * tokens, :] = (
-            table - high.astype(jnp.float32)
-        ).astype(jnp.bfloat16)
+        low = (table - high.astype(jnp.float32)).astype(jnp.bfloat16)
+        table_ref[h * tokens : (h + 1) * tokens, :] = high
+        table_ref[(pieces + h) * tokens : (pieces + h + 1) * tokens, :] = low
 
 
 def fetch_kernel(*refs):
@@ -263,22 +261,23 @@
         out_ref[...] = jnp.zeros_like(out_ref)
 
 
-def gathered(row_refs, high_ref, low_ref, tokens):
+def gathered(row_refs, table_ref, tokens):
     flat = jnp.concatenate([r[...] for r in row_refs], axis=0)
     part = flat.shape[1]
-    for h in range(high_ref.shape[0] // tokens):
-        at = slice(h * tokens, (h + 1) * tokens)
-        value = jnp.dot(high_ref[at, :], flat, preferred_element_type=jnp.float32)
-        value = value + jnp.dot(low_ref[at, :], flat, preferred_element_type=jnp.float32)
-        yield slice(h * part, (h + 1) * part), value
-
-
-def early_kernel(order, held_count, high_ref, low_ref, hid_ref, dgate_ref, *refs):
+    sums = jnp.dot(table_ref[...], flat, preferred_element_type=jnp.float32)
+    pieces = sums.shape[0] // (2 * tokens)
+    for h in range(pieces):
+        high = sums[h * tokens : (h + 1) * tokens]
+        low = sums[(pieces + h) * tokens : (pieces + h + 1) * tokens]
+        yield slice(h * part, (h + 1) * part), high + low
+
+
+def early_kernel(order, held_count, table_ref, hid_ref, dgate_ref, *refs):
     held_refs, row_refs = refs[:held_count], refs[held_count:-3]
     own_ref, other_ref, sum_ref = refs[-3:]
     me, core = position()
     half = own_ref.shape[0]
-    for lanes, value in gathered(row_refs, high_ref, low_ref, 2 * half):
+    for lanes, value in gathered(row_refs, table_ref, 2 * half):
         sum_ref[:, lanes] = value
 
     @pl.when(core != 0)
@@ -298,9 +297,9 @@
     other_ref[...] = sum_ref[half:, :].astype(jnp.bfloat16)
 
 
-def late_kernel(own_ref, share_ref, high_ref, low_ref, *refs):
+def late_kernel(own_ref, share_ref, table_ref, *refs):
     row_refs, out_ref = refs[:-1], refs[-1]
-    for lanes, value in gathered(row_refs, high_ref, low_ref, own_ref.shape[0]):
+    for lanes, value in gathered(row_refs, table_ref, own_ref.shape[0]):
         value = value + (own_ref[:, lanes] + share_ref[:, lanes].astype(jnp.float32))
         out_ref[:, lanes] = value.astype(jnp.bfloat16)
 
@@ -331,7 +330,7 @@
 def plan_of(sources):
     half = sources // 2
     far = [(k, k + 1) for k in range(half, sources, 2)]
-    parts = (far[: len(far) // 2], [(2, 3), (0, 1)], [(k, k + 1) for k in range(4, half, 2)],
+    parts = (far[: len(far) // 2], [(2, 3), (0, 1)], [(k + 1, k) for k in range(4, half, 2)],
              far[len(far) // 2 :])
     plan, groups = [], []
     for part in parts:
@@ -399,15 +398,15 @@
     helds = (held,) + tuple(swapped(held, (k, k)) for k in (1, 2, 3))
     order = [k ^ j for j in range(4) for k in order]
 
-    high, low = call(
+    table = call(
         lambda *r: weigh_kernel(capacity, pieces, [plan[m] for m in early], *r),
-        (shape((2 * tok_rows * pieces, len(early) * block.shape[0]), bf16),) * 2,
+        shape((4 * tok_rows * pieces, len(early) * block.shape[0]), bf16),
         (routes, routes2, rates, rates2),
     )
     own_block = shape((own_capacity * own_pieces, width // own_pieces), bf16)
-    own_high, own_low = call(
+    own_table = call(
         lambda *r: weigh_kernel(own_capacity, own_pieces, homes, *r),
-        (shape((tok_rows * own_pieces, len(homes) * own_block.shape[0]), bf16),) * 2,
+        shape((2 * tok_rows * own_pieces, len(homes) * own_block.shape[0]), bf16),
         (routes, rates),
     )
     dense_hidden = call(
@@ -430,7 +429,7 @@
     total, share = call(
         lambda *r: early_kernel(order, len(helds), *r),
         (shape((tok_rows, width), f32), shape((tok_rows, width), bf16)),
-        (high, low, dense_hidden, dense_gate.reshape(1, width))
+        (table, dense_hidden, dense_gate.reshape(1, width))
         + helds
         + tuple(back[m, 0] for m in early),
         scratch=(pltpu.VMEM((2 * tok_rows, width), f32),),
@@ -439,7 +438,7 @@
     return call(
         late_kernel,
         shape((tok_rows, width), bf16),
-        (total, share, own_high, own_low) + tuple(back[m, c] for m in direct for c in range(2)),
+        (total, share, own_table) + tuple(back[m, c] for m in direct for c in range(2)),
     )
 
 

time: 117 us -> 116 us (level)
  waiting for transfers between devices: 44.6 us -> 43.2 us
  starting transfers between devices: 51.8 us -> 53 us
    ppermute x25, waiting for transfers between devices: 42.6 us -> 41.2 us  [swapped(): return lax.ppermute(value, ('ep', 'tp'), pairs)]
where the time goes in v4:
time: 116 us
  starting transfers between devices  53 us (46%)
  waiting for transfers between devices  43.2 us (37%)
  Pallas kernels  19.8 us (17%)
    ppermute x25, starting transfers between devices, swapped(): return lax.ppermute(value, ('ep', 'tp'), pairs)  47.5 us
    ppermute x25, waiting for transfers between devices, swapped(): return lax.ppermute(value, ('ep', 'tp'), pairs)  41.2 us
    pallas_call x14, Pallas kernels, call(): pl.pallas_call(kernel, out_shape=outs, in_specs=[spec for _ in ins], out_...  19.8 us
    ppermute x8, starting transfers between devices, partners(): return lax.ppermute(value, 'tp', [(0, 1), (1, 0)])  5.46 us
  transfers between devices with their start and end apart: 33, of which 15 were waited for; matrix products, arithmetic and copies ran while one was open for 0% of the time, Pallas kernels for 14%

profile of v4, /device:TPU:0, one launch (start us, length us, event | category | flops | bytes accessed | tf_op | source)
XLA Modules:
  0.0 116.2 jit_solution(2101368768043500679)
XLA Ops:
  2.3 4.1 %collective-permute-start.3 = (bf16[128,256]{1,0:T(8,128)(2,1)S(1)}, bf16[128,256]{1,0:T(8,128)(2,1)S(1)}, u32[]{:S(2)}, u32[]{:S(2)}) collective-permute-start(bf16[128,256]{1,0:T(8,128)(2,1)S(1)} %get-tuple-element.41.refs_0_), channel_id=1, source_target_pairs={{0,16},{1,17},{2,18},{3,19},{4,20},{5,21},{6,22},{7,23},{8,24},{9,... | collective-permute-start | bytes 196616 | tf_op jit(solution)/shard_map/ppermute | solution.py:323
  6.5 3.7 %collective-permute-done.3.refs_1_ = bf16[128,256]{1,0:T(8,128)(2,1)S(1)} collective-permute-done((bf16[128,256]{1,0:T(8,128)(2,1)S(1)}, bf16[128,256]{1,0:T(8,128)(2,1)S(1)}, u32[]{:S(2)}, u32[]{:S(2)}) %collective-permute-start.3) | collective-permute-done | bytes 65568 | tf_op jit(solution)/shard_map/ppermute | solution.py:323
  11.5 2.7 %collective-permute-start.4 = (bf16[256,256]{1,0:T(8,128)(2,1)S(1)}, bf16[256,256]{1,0:T(8,128)(2,1)S(1)}, u32[]{:S(2)}, u32[]{:S(2)}) collective-permute-start(bf16[256,256]{1,0:T(8,128)(2,1)S(1)} %shard_map.103.refs_0_), channel_id=1, source_target_pairs={{0,8},{1,9},{2,10},{3,11},{4,12},{5,13},{6,14},{7,15},{8,0},{9,1},... | collective-permute-start | bytes 393224 | tf_op jit(solution)/shard_map/ppermute | solution.py:323
  15.3 1.6 %collective-permute-start.16 = (bf16[88,1024]{1,0:T(8,128)(2,1)S(1)}, bf16[88,1024]{1,0:T(8,128)(2,1)S(1)}, u32[]{:S(2)}, u32[]{:S(2)}) collective-permute-start(bf16[88,1024]{1,0:T(8,128)(2,1)S(1)} %get-tuple-element.49), channel_id=1, source_target_pairs={{0,4},{1,7},{2,6},{3,5},{4,0},{5,3},{6,2},{7,1},{8,12},{9,15},{10,... | collective-permute-start | bytes 540680 | tf_op jit(solution)/shard_map/ppermute | solution.py:323
  18.7 4.0 %collective-permute-done.16.r_0_ = bf16[88,1024]{1,0:T(8,128)(2,1)S(1)} collective-permute-done((bf16[88,1024]{1,0:T(8,128)(2,1)S(1)}, bf16[88,1024]{1,0:T(8,128)(2,1)S(1)}, u32[]{:S(2)}, u32[]{:S(2)}) %collective-permute-start.16) | collective-permute-done | bytes 180256 | tf_op jit(solution)/shard_map/ppermute | solution.py:323
  22.6 1.5 %collective-permute-start.5 = (bf16[512,256]{1,0:T(8,128)(2,1)S(1)}, bf16[512,256]{1,0:T(8,128)(2,1)S(1)}, u32[]{:S(2)}, u32[]{:S(2)}) collective-permute-start(bf16[512,256]{1,0:T(8,128)(2,1)S(1)} %shard_map.104.r_1_.r_3_), channel_id=1, source_target_pairs={{0,2},{1,3},{2,0},{3,1},{4,6},{5,7},{6,4},{7,5},{8,10},{9,11},{10,... | collective-permute-start | bytes 786440 | tf_op jit(solution)/shard_map/ppermute | solution.py:323
  24.1 1.5 %collective-permute-start.6 = (bf16[512,256]{1,0:T(8,128)(2,1)S(1)}, bf16[512,256]{1,0:T(8,128)(2,1)S(1)}, u32[]{:S(2)}, u32[]{:S(2)}) collective-permute-start(bf16[512,256]{1,0:T(8,128)(2,1)S(1)} %shard_map.104.r_1_.r_3_), channel_id=1, source_target_pairs={{0,4},{1,5},{2,6},{3,7},{4,0},{5,1},{6,2},{7,3},{8,12},{9,13},{10,... | collective-permute-start | bytes 786440 | tf_op jit(solution)/shard_map/ppermute | solution.py:323
  26.1 3.5 %collective-permute-start.10 = (bf16[88,1024]{1,0:T(8,128)(2,1)S(1)}, bf16[88,1024]{1,0:T(8,128)(2,1)S(1)}, u32[]{:S(2)}, u32[]{:S(2)}) collective-permute-start(bf16[88,1024]{1,0:T(8,128)(2,1)S(1)} %get-tuple-element.43), channel_id=1, source_target_pairs={{0,20},{1,23},{2,22},{3,21},{4,16},{5,19},{6,18},{7,17},{8,28},{9,... | collective-permute-start | bytes 540680 | tf_op jit(solution)/shard_map/ppermute | solution.py:323
  30.0 2.9 %shard_map.106 = (bf16[2048,512]{1,0:T(8,128)(2,1)S(1)}, bf16[2048,512]{1,0:T(8,128)(2,1)S(1)}, bf16[512,2048]{1,0:T(8,128)(2,1)S(1)}) custom-call(bf16[1,2048,512]{2,1,0:T(8,128)(2,1)} %refs_0_.1, bf16[1,2048,512]{2,1,0:T(8,128)(2,1)} %refs_1_.1, bf16[1,512,2048]{2,1,0:T(8,128)(2,1)} %refs_2_.1), custom_call_target="tpu_custom_call" | custom-call | tf_op jit(solution)/shard_map/pallas_call | solution.py:310
  32.9 2.4 %shard_map.108 = (bf16[88,1024]{1,0:T(8,128)(2,1)S(1)}, bf16[88,1024]{1,0:T(8,128)(2,1)S(1)}) custom-call(bf16[88,1024]{1,0:T(8,128)(2,1)S(1)} %collective-permute-done.16.r_0_, bf16[88,1024]{1,0:T(8,128)(2,1)S(1)} %collective-permute-done.17.r_1_, bf16[2048,512]{1,0:T(8,128)(2,1)S(1)} %get-tuple-element.44.r_2_, ...), custom_call_target="tpu_custom_call" | custom-call | tf_op jit(solution)/shard_map/pallas_call | solution.py:310
  35.3 7.5 %collective-permute-done.10.r_1_ = bf16[88,1024]{1,0:T(8,128)(2,1)S(1)} collective-permute-done((bf16[88,1024]{1,0:T(8,128)(2,1)S(1)}, bf16[88,1024]{1,0:T(8,128)(2,1)S(1)}, u32[]{:S(2)}, u32[]{:S(2)}) %collective-permute-start.10) | collective-permute-done | bytes 180256 | tf_op jit(solution)/shard_map/ppermute | solution.py:323
  42.8 1.8 %collective-permute-start.18 = (bf16[88,1024]{1,0:T(8,128)(2,1)S(1)}, bf16[88,1024]{1,0:T(8,128)(2,1)S(1)}, u32[]{:S(2)}, u32[]{:S(2)}) collective-permute-start(bf16[88,1024]{1,0:T(8,128)(2,1)S(1)} %get-tuple-element.51), channel_id=1, source_target_pairs={{0,4},{1,7},{2,6},{3,5},{4,0},{5,3},{6,2},{7,1},{8,12},{9,15},{10,... | collective-permute-start | bytes 540680 | tf_op jit(solution)/shard_map/ppermute | solution.py:323
  46.7 2.4 %shard_map.107 = (bf16[88,1024]{1,0:T(8,128)(2,1)S(1)}, bf16[88,1024]{1,0:T(8,128)(2,1)S(1)}) custom-call(bf16[88,1024]{1,0:T(8,128)(2,1)S(1)} %collective-permute-done.9.r_0_, bf16[88,1024]{1,0:T(8,128)(2,1)S(1)} %collective-permute-done.10.r_1_, bf16[2048,512]{1,0:T(8,128)(2,1)S(1)} %get-tuple-element.44.r_2_, ...), custom_call_target="tpu_custom_call" | custom-call | tf_op jit(solution)/shard_map/pallas_call | solution.py:310
  49.2 3.0 %collective-permute-start.15 = (bf16[88,1024]{1,0:T(8,128)(2,1)S(1)}, bf16[88,1024]{1,0:T(8,128)(2,1)S(1)}, u32[]{:S(2)}, u32[]{:S(2)}) collective-permute-start(bf16[88,1024]{1,0:T(8,128)(2,1)S(1)} %get-tuple-element.48), channel_id=1, source_target_pairs={{0,20},{1,23},{2,22},{3,21},{4,16},{5,19},{6,18},{7,17},{8,28},{9,... | collective-permute-start | bytes 540680 | tf_op jit(solution)/shard_map/ppermute | solution.py:323
  52.2 1.9 %collective-permute-start.1 = (f32[2,128]{1,0:T(2,128)S(1)}, f32[2,128]{1,0:T(2,128)S(1)}, u32[]{:S(2)}, u32[]{:S(2)}) collective-permute-start(f32[2,128]{1,0:T(2,128)S(1)} %bitcast.15), channel_id=1, source_target_pairs={{0,1},{1,0},{2,3},{3,2},{4,5},{5,4},{6,7},{7,6},{8,9},{9,8},{10,11... | collective-permute-start | bytes 3080 | tf_op jit(solution)/shard_map/ppermute | solution.py:327
  56.2 8.3 %collective-permute-done.14.r_7_ = bf16[88,1024]{1,0:T(8,128)(2,1)S(1)} collective-permute-done((bf16[88,1024]{1,0:T(8,128)(2,1)S(1)}, bf16[88,1024]{1,0:T(8,128)(2,1)S(1)}, u32[]{:S(2)}, u32[]{:S(2)}) %collective-permute-start.14) | collective-permute-done | bytes 180256 | tf_op jit(solution)/shard_map/ppermute | solution.py:323
  64.6 4.0 %collective-permute-done.15.r_8_ = bf16[88,1024]{1,0:T(8,128)(2,1)S(1)} collective-permute-done((bf16[88,1024]{1,0:T(8,128)(2,1)S(1)}, bf16[88,1024]{1,0:T(8,128)(2,1)S(1)}, u32[]{:S(2)}, u32[]{:S(2)}) %collective-permute-start.15) | collective-permute-done | bytes 180256 | tf_op jit(solution)/shard_map/ppermute | solution.py:323
  70.0 2.2 %collective-permute-start.20 = (bf16[128,2048]{1,0:T(8,128)(2,1)S(1)}, bf16[128,2048]{1,0:T(8,128)(2,1)S(1)}, u32[]{:S(2)}, u32[]{:S(2)}) collective-permute-start(bf16[128,2048]{1,0:T(8,128)(2,1)S(1)} %get-tuple-element.54), channel_id=1, source_target_pairs={{0,1},{1,0},{2,3},{3,2},{4,5},{5,4},{6,7},{7,6},{8,9},{9,8},{10,11... | collective-permute-start | bytes 1572872 | tf_op jit(solution)/shard_map/ppermute | solution.py:327
  73.1 3.9 %collective-permute-start.28 = (bf16[88,1024]{1,0:T(8,128)(2,1)S(1)}, bf16[88,1024]{1,0:T(8,128)(2,1)S(1)}, u32[]{:S(2)}, u32[]{:S(2)}) collective-permute-start(bf16[88,1024]{1,0:T(8,128)(2,1)S(1)} %get-tuple-element.62), channel_id=1, source_target_pairs={{0,28},{1,31},{2,30},{3,29},{4,24},{5,27},{6,26},{7,25},{8,20},{9,... | collective-permute-start | bytes 540680 | tf_op jit(solution)/shard_map/ppermute | solution.py:323
  77.0 2.9 %collective-permute-start.22 = (bf16[88,1024]{1,0:T(8,128)(2,1)S(1)}, bf16[88,1024]{1,0:T(8,128)(2,1)S(1)}, u32[]{:S(2)}, u32[]{:S(2)}) collective-permute-start(bf16[88,1024]{1,0:T(8,128)(2,1)S(1)} %get-tuple-element.56), channel_id=1, source_target_pairs={{0,14},{1,13},{2,12},{3,15},{4,10},{5,9},{6,8},{7,11},{8,6},{9,5},... | collective-permute-start | bytes 540680 | tf_op jit(solution)/shard_map/ppermute | solution.py:323
  79.8 1.8 %collective-permute-done.27.r_0_ = bf16[88,1024]{1,0:T(8,128)(2,1)S(1)} collective-permute-done((bf16[88,1024]{1,0:T(8,128)(2,1)S(1)}, bf16[88,1024]{1,0:T(8,128)(2,1)S(1)}, u32[]{:S(2)}, u32[]{:S(2)}) %collective-permute-start.27) | collective-permute-done | bytes 180256 | tf_op jit(solution)/shard_map/ppermute | solution.py:323
  81.6 4.7 %collective-permute-done.28.r_1_ = bf16[88,1024]{1,0:T(8,128)(2,1)S(1)} collective-permute-done((bf16[88,1024]{1,0:T(8,128)(2,1)S(1)}, bf16[88,1024]{1,0:T(8,128)(2,1)S(1)}, u32[]{:S(2)}, u32[]{:S(2)}) %collective-permute-start.28) | collective-permute-done | bytes 180256 | tf_op jit(solution)/shard_map/ppermute | solution.py:323
  86.3 2.4 %shard_map.112 = (bf16[88,512]{1,0:T(8,128)(2,1)S(1)}, bf16[88,512]{1,0:T(8,128)(2,1)S(1)}, bf16[88,512]{1,0:T(8,128)(2,1)S(1)}, bf16[88,512]{1,0:T(8,128)(2,1)S(1)}) custom-call(bf16[88,1024]{1,0:T(8,128)(2,1)S(1)} %collective-permute-done.27.r_0_, bf16[88,1024]{1,0:T(8,128)(2,1)S(1)} %collective-permute-done.28.r_1_, ...), custom_call_target="tpu_custom_call" | custom-call | tf_op jit(solution)/shard_map/pallas_call | solution.py:310
  89.2 2.2 %collective-permute-start.30 = (bf16[88,512]{1,0:T(8,128)(2,1)S(1)}, bf16[88,512]{1,0:T(8,128)(2,1)S(1)}, u32[]{:S(2)}, u32[]{:S(2)}) collective-permute-start(bf16[88,512]{1,0:T(8,128)(2,1)S(1)} %get-tuple-element.64), channel_id=1, source_target_pairs={{0,25},{1,26},{2,27},{3,24},{4,29},{5,30},{6,31},{7,28},{8,17},{9,... | collective-permute-start | bytes 270344 | tf_op jit(solution)/shard_map/ppermute | solution.py:323
  91.4 1.6 %collective-permute-start.31 = (bf16[88,512]{1,0:T(8,128)(2,1)S(1)}, bf16[88,512]{1,0:T(8,128)(2,1)S(1)}, u32[]{:S(2)}, u32[]{:S(2)}) collective-permute-start(bf16[88,512]{1,0:T(8,128)(2,1)S(1)} %get-tuple-element.65), channel_id=1, source_target_pairs={{0,28},{1,31},{2,30},{3,29},{4,24},{5,27},{6,26},{7,25},{8,20},{9,... | collective-permute-start | bytes 270344 | tf_op jit(solution)/shard_map/ppermute | solution.py:323
  94.2 3.5 %collective-permute-start.32 = (bf16[88,512]{1,0:T(8,128)(2,1)S(1)}, bf16[88,512]{1,0:T(8,128)(2,1)S(1)}, u32[]{:S(2)}, u32[]{:S(2)}) collective-permute-start(bf16[88,512]{1,0:T(8,128)(2,1)S(1)} %get-tuple-element.66), channel_id=1, source_target_pairs={{0,29},{1,30},{2,31},{3,28},{4,25},{5,26},{6,27},{7,24},{8,21},{9,... | collective-permute-start | bytes 270344 | tf_op jit(solution)/shard_map/ppermute | solution.py:323
  97.7 2.4 %shard_map.111 = (bf16[88,512]{1,0:T(8,128)(2,1)S(1)}, bf16[88,512]{1,0:T(8,128)(2,1)S(1)}, bf16[88,512]{1,0:T(8,128)(2,1)S(1)}, bf16[88,512]{1,0:T(8,128)(2,1)S(1)}) custom-call(bf16[88,1024]{1,0:T(8,128)(2,1)S(1)} %collective-permute-done.21.r_0_, bf16[88,1024]{1,0:T(8,128)(2,1)S(1)} %collective-permute-done.22.r_1_, ...), custom_call_target="tpu_custom_call" | custom-call | tf_op jit(solution)/shard_map/pallas_call | solution.py:310
  100.1 4.0 %collective-permute-start.23 = (bf16[88,512]{1,0:T(8,128)(2,1)S(1)}, bf16[88,512]{1,0:T(8,128)(2,1)S(1)}, u32[]{:S(2)}, u32[]{:S(2)}) collective-permute-start(bf16[88,512]{1,0:T(8,128)(2,1)S(1)} %get-tuple-element.57), channel_id=1, source_target_pairs={{0,10},{1,9},{2,8},{3,11},{4,14},{5,13},{6,12},{7,15},{8,2},{9,1},... | collective-permute-start | bytes 270344 | tf_op jit(solution)/shard_map/ppermute | solution.py:323
  104.0 1.4 %collective-permute-start.24 = (bf16[88,512]{1,0:T(8,128)(2,1)S(1)}, bf16[88,512]{1,0:T(8,128)(2,1)S(1)}, u32[]{:S(2)}, u32[]{:S(2)}) collective-permute-start(bf16[88,512]{1,0:T(8,128)(2,1)S(1)} %get-tuple-element.58), channel_id=1, source_target_pairs={{0,11},{1,8},{2,9},{3,10},{4,15},{5,12},{6,13},{7,14},{8,3},{9,0},... | collective-permute-start | bytes 270344 | tf_op jit(solution)/shard_map/ppermute | solution.py:323
  105.5 3.3 %collective-permute-start.25 = (bf16[88,512]{1,0:T(8,128)(2,1)S(1)}, bf16[88,512]{1,0:T(8,128)(2,1)S(1)}, u32[]{:S(2)}, u32[]{:S(2)}) collective-permute-start(bf16[88,512]{1,0:T(8,128)(2,1)S(1)} %get-tuple-element.59), channel_id=1, source_target_pairs={{0,14},{1,13},{2,12},{3,15},{4,10},{5,9},{6,8},{7,11},{8,6},{9,5},... | collective-permute-start | bytes 270344 | tf_op jit(solution)/shard_map/ppermute | solution.py:323
  111.8 2.7 %collective-permute-done.26.refs_3_ = bf16[88,512]{1,0:T(8,128)(2,1)S(1)} collective-permute-done((bf16[88,512]{1,0:T(8,128)(2,1)S(1)}, bf16[88,512]{1,0:T(8,128)(2,1)S(1)}, u32[]{:S(2)}, u32[]{:S(2)}) %collective-permute-start.26) | collective-permute-done | bytes 90144 | tf_op jit(solution)/shard_map/ppermute | solution.py:323
  114.5 1.8 %shard_map.113 = bf16[128,2048]{1,0:T(8,128)(2,1)} custom-call(f32[128,2048]{1,0:T(8,128)S(1)} %get-tuple-element.53.own_ref, bf16[128,2048]{1,0:T(8,128)(2,1)S(1)} %collective-permute-done.20.share_ref, bf16[1024,704]{1,0:T(8,128)(2,1)S(1)} %shard_map.110.table_ref, bf16[88,512]{1,0:T(8,128)(2,1)S(1)} %collective-permute-done.23.refs_0_, ...), custom_call_target="tpu_custom_call" | custom-call | tf_op jit(solution)/shard_map/pallas_call | solution.py:310
  (52 shorter events, 18.7 us)
Async XLA Ops:
  0.0 25.6 %collective-permute-start.11 = (bf16[2048,512]{1,0:T(8,128)(2,1)}, bf16[2048,512]{1,0:T(8,128)(2,1)S(1)}, u32[]{:S(2)}, u32[]{:S(2)}) collective-permute-start(bf16[2048,512]{1,0:T(8,128)(2,1)} %bitcast.8), channel_id=1, source_target_pairs={{0,1},{1,0},{2,3},{3,2},{4,5},{5,4},{6,7},{7,6},{8,9},{9,8},{10,11... | collective-permute-start | bytes 6291464 | tf_op jit(solution)/shard_map/ppermute | solution.py:327
  0.5 25.6 %collective-permute-start.12 = (bf16[2048,512]{1,0:T(8,128)(2,1)}, bf16[2048,512]{1,0:T(8,128)(2,1)S(1)}, u32[]{:S(2)}, u32[]{:S(2)}) collective-permute-start(bf16[2048,512]{1,0:T(8,128)(2,1)} %bitcast.9), channel_id=1, source_target_pairs={{0,1},{1,0},{2,3},{3,2},{4,5},{5,4},{6,7},{7,6},{8,9},{9,8},{10,11... | collective-permute-start | bytes 6291464 | tf_op jit(solution)/shard_map/ppermute | solution.py:327
  0.5 29.2 %collective-permute-start.13 = (bf16[512,2048]{1,0:T(8,128)(2,1)}, bf16[512,2048]{1,0:T(8,128)(2,1)S(1)}, u32[]{:S(2)}, u32[]{:S(2)}) collective-permute-start(bf16[512,2048]{1,0:T(8,128)(2,1)} %bitcast.10), channel_id=1, source_target_pairs={{0,1},{1,0},{2,3},{3,2},{4,5},{5,4},{6,7},{7,6},{8,9},{9,8},{10,11... | collective-permute-start | bytes 6291464 | tf_op jit(solution)/shard_map/ppermute | solution.py:327
  1.0 13.2 %collective-permute-start.2 = (bf16[128,2048]{1,0:T(8,128)(2,1)}, bf16[128,2048]{1,0:T(8,128)(2,1)S(1)}, u32[]{:S(2)}, u32[]{:S(2)}) collective-permute-start(bf16[128,2048]{1,0:T(8,128)(2,1)} %tok_ref.1), channel_id=1, source_target_pairs={{0,1},{1,0},{2,3},{3,2},{4,5},{5,4},{6,7},{7,6},{8,9},{9,8},{10,11... | collective-permute-start | bytes 1572872 | tf_op jit(solution)/shard_map/ppermute | solution.py:327
  2.3 7.8 %collective-permute-start.3 = (bf16[128,256]{1,0:T(8,128)(2,1)S(1)}, bf16[128,256]{1,0:T(8,128)(2,1)S(1)}, u32[]{:S(2)}, u32[]{:S(2)}) collective-permute-start(bf16[128,256]{1,0:T(8,128)(2,1)S(1)} %get-tuple-element.41.refs_0_), channel_id=1, source_target_pairs={{0,16},{1,17},{2,18},{3,19},{4,20},{5,21},{6,22},{7,23},{8,24},{9,... | collective-permute-start | bytes 196616 | tf_op jit(solution)/shard_map/ppermute | solution.py:323
  10.1 1.4 %collective-permute-start = (s32[2,128]{1,0:T(2,128)}, s32[2,128]{1,0:T(2,128)S(1)}, u32[]{:S(2)}, u32[]{:S(2)}) collective-permute-start(s32[2,128]{1,0:T(2,128)} %bitcast.13), channel_id=1, source_target_pairs={{0,1},{1,0},{2,3},{3,2},{4,5},{5,4},{6,7},{7,6},{8,9},{9,8},{10,11... | collective-permute-start | bytes 3080 | tf_op jit(solution)/shard_map/ppermute | solution.py:327
  11.5 6.5 %collective-permute-start.4 = (bf16[256,256]{1,0:T(8,128)(2,1)S(1)}, bf16[256,256]{1,0:T(8,128)(2,1)S(1)}, u32[]{:S(2)}, u32[]{:S(2)}) collective-permute-start(bf16[256,256]{1,0:T(8,128)(2,1)S(1)} %shard_map.103.refs_0_), channel_id=1, source_target_pairs={{0,8},{1,9},{2,10},{3,11},{4,12},{5,13},{6,14},{7,15},{8,0},{9,1},... | collective-permute-start | bytes 393224 | tf_op jit(solution)/shard_map/ppermute | solution.py:323
  15.3 7.3 %collective-permute-start.16 = (bf16[88,1024]{1,0:T(8,128)(2,1)S(1)}, bf16[88,1024]{1,0:T(8,128)(2,1)S(1)}, u32[]{:S(2)}, u32[]{:S(2)}) collective-permute-start(bf16[88,1024]{1,0:T(8,128)(2,1)S(1)} %get-tuple-element.49), channel_id=1, source_target_pairs={{0,4},{1,7},{2,6},{3,5},{4,0},{5,3},{6,2},{7,1},{8,12},{9,15},{10,... | collective-permute-start | bytes 540680 | tf_op jit(solution)/shard_map/ppermute | solution.py:323
  18.0 6.2 %collective-permute-start.17 = (bf16[88,1024]{1,0:T(8,128)(2,1)S(1)}, bf16[88,1024]{1,0:T(8,128)(2,1)S(1)}, u32[]{:S(2)}, u32[]{:S(2)}) collective-permute-start(bf16[88,1024]{1,0:T(8,128)(2,1)S(1)} %get-tuple-element.50), channel_id=1, source_target_pairs={{0,0},{1,3},{2,2},{3,1},{4,4},{5,7},{6,6},{7,5},{8,8},{9,11},{10,1... | collective-permute-start | bytes 540680 | tf_op jit(solution)/shard_map/ppermute | solution.py:323
  22.6 26.5 %collective-permute-start.5 = (bf16[512,256]{1,0:T(8,128)(2,1)S(1)}, bf16[512,256]{1,0:T(8,128)(2,1)S(1)}, u32[]{:S(2)}, u32[]{:S(2)}) collective-permute-start(bf16[512,256]{1,0:T(8,128)(2,1)S(1)} %shard_map.104.r_1_.r_3_), channel_id=1, source_target_pairs={{0,2},{1,3},{2,0},{3,1},{4,6},{5,7},{6,4},{7,5},{8,10},{9,11},{10,... | collective-permute-start | bytes 786440 | tf_op jit(solution)/shard_map/ppermute | solution.py:323
  24.1 25.1 %collective-permute-start.6 = (bf16[512,256]{1,0:T(8,128)(2,1)S(1)}, bf16[512,256]{1,0:T(8,128)(2,1)S(1)}, u32[]{:S(2)}, u32[]{:S(2)}) collective-permute-start(bf16[512,256]{1,0:T(8,128)(2,1)S(1)} %shard_map.104.r_1_.r_3_), channel_id=1, source_target_pairs={{0,4},{1,5},{2,6},{3,7},{4,0},{5,1},{6,2},{7,3},{8,12},{9,13},{10,... | collective-permute-start | bytes 786440 | tf_op jit(solution)/shard_map/ppermute | solution.py:323
  25.6 26.5 %collective-permute-start.7 = (bf16[512,256]{1,0:T(8,128)(2,1)S(1)}, bf16[512,256]{1,0:T(8,128)(2,1)S(1)}, u32[]{:S(2)}, u32[]{:S(2)}) collective-permute-start(bf16[512,256]{1,0:T(8,128)(2,1)S(1)} %shard_map.104.r_1_.r_3_), channel_id=1, source_target_pairs={{0,6},{1,7},{2,4},{3,5},{4,2},{5,3},{6,0},{7,1},{8,14},{9,15},{10,... | collective-permute-start | bytes 786440 | tf_op jit(solution)/shard_map/ppermute | solution.py:323
  26.1 16.7 %collective-permute-start.10 = (bf16[88,1024]{1,0:T(8,128)(2,1)S(1)}, bf16[88,1024]{1,0:T(8,128)(2,1)S(1)}, u32[]{:S(2)}, u32[]{:S(2)}) collective-permute-start(bf16[88,1024]{1,0:T(8,128)(2,1)S(1)} %get-tuple-element.43), channel_id=1, source_target_pairs={{0,20},{1,23},{2,22},{3,21},{4,16},{5,19},{6,18},{7,17},{8,28},{9,... | collective-permute-start | bytes 540680 | tf_op jit(solution)/shard_map/ppermute | solution.py:323
  29.7 16.2 %collective-permute-start.9 = (bf16[88,1024]{1,0:T(8,128)(2,1)S(1)}, bf16[88,1024]{1,0:T(8,128)(2,1)S(1)}, u32[]{:S(2)}, u32[]{:S(2)}) collective-permute-start(bf16[88,1024]{1,0:T(8,128)(2,1)S(1)} %get-tuple-element.42), channel_id=1, source_target_pairs={{0,16},{1,19},{2,18},{3,17},{4,20},{5,23},{6,22},{7,21},{8,24},{9,... | collective-permute-start | bytes 540680 | tf_op jit(solution)/shard_map/ppermute | solution.py:323
  42.8 13.4 %collective-permute-start.18 = (bf16[88,1024]{1,0:T(8,128)(2,1)S(1)}, bf16[88,1024]{1,0:T(8,128)(2,1)S(1)}, u32[]{:S(2)}, u32[]{:S(2)}) collective-permute-start(bf16[88,1024]{1,0:T(8,128)(2,1)S(1)} %get-tuple-element.51), channel_id=1, source_target_pairs={{0,4},{1,7},{2,6},{3,5},{4,0},{5,3},{6,2},{7,1},{8,12},{9,15},{10,... | collective-permute-start | bytes 540680 | tf_op jit(solution)/shard_map/ppermute | solution.py:323
  45.9 10.3 %collective-permute-start.19 = (bf16[88,1024]{1,0:T(8,128)(2,1)S(1)}, bf16[88,1024]{1,0:T(8,128)(2,1)S(1)}, u32[]{:S(2)}, u32[]{:S(2)}) collective-permute-start(bf16[88,1024]{1,0:T(8,128)(2,1)S(1)} %get-tuple-element.52), channel_id=1, source_target_pairs={{0,0},{1,3},{2,2},{3,1},{4,4},{5,7},{6,6},{7,5},{8,8},{9,11},{10,1... | collective-permute-start | bytes 540680 | tf_op jit(solution)/shard_map/ppermute | solution.py:323
  49.1 15.4 %collective-permute-start.14 = (bf16[88,1024]{1,0:T(8,128)(2,1)S(1)}, bf16[88,1024]{1,0:T(8,128)(2,1)S(1)}, u32[]{:S(2)}, u32[]{:S(2)}) collective-permute-start(bf16[88,1024]{1,0:T(8,128)(2,1)S(1)} %get-tuple-element.47), channel_id=1, source_target_pairs={{0,16},{1,19},{2,18},{3,17},{4,20},{5,23},{6,22},{7,21},{8,24},{9,... | collective-permute-start | bytes 540680 | tf_op jit(solution)/shard_map/ppermute | solution.py:323
  49.2 19.4 %collective-permute-start.15 = (bf16[88,1024]{1,0:T(8,128)(2,1)S(1)}, bf16[88,1024]{1,0:T(8,128)(2,1)S(1)}, u32[]{:S(2)}, u32[]{:S(2)}) collective-permute-start(bf16[88,1024]{1,0:T(8,128)(2,1)S(1)} %get-tuple-element.48), channel_id=1, source_target_pairs={{0,20},{1,23},{2,22},{3,21},{4,16},{5,19},{6,18},{7,17},{8,28},{9,... | collective-permute-start | bytes 540680 | tf_op jit(solution)/shard_map/ppermute | solution.py:323
  52.2 2.7 %collective-permute-start.1 = (f32[2,128]{1,0:T(2,128)S(1)}, f32[2,128]{1,0:T(2,128)S(1)}, u32[]{:S(2)}, u32[]{:S(2)}) collective-permute-start(f32[2,128]{1,0:T(2,128)S(1)} %bitcast.15), channel_id=1, source_target_pairs={{0,1},{1,0},{2,3},{3,2},{4,5},{5,4},{6,7},{7,6},{8,9},{9,8},{10,11... | collective-permute-start | bytes 3080 | tf_op jit(solution)/shard_map/ppermute | solution.py:327
  70.0 44.5 %collective-permute-start.20 = (bf16[128,2048]{1,0:T(8,128)(2,1)S(1)}, bf16[128,2048]{1,0:T(8,128)(2,1)S(1)}, u32[]{:S(2)}, u32[]{:S(2)}) collective-permute-start(bf16[128,2048]{1,0:T(8,128)(2,1)S(1)} %get-tuple-element.54), channel_id=1, source_target_pairs={{0,1},{1,0},{2,3},{3,2},{4,5},{5,4},{6,7},{7,6},{8,9},{9,8},{10,11... | collective-permute-start | bytes 1572872 | tf_op jit(solution)/shard_map/ppermute | solution.py:327
  72.2 9.4 %collective-permute-start.27 = (bf16[88,1024]{1,0:T(8,128)(2,1)S(1)}, bf16[88,1024]{1,0:T(8,128)(2,1)S(1)}, u32[]{:S(2)}, u32[]{:S(2)}) collective-permute-start(bf16[88,1024]{1,0:T(8,128)(2,1)S(1)} %get-tuple-element.61), channel_id=1, source_target_pairs={{0,24},{1,27},{2,26},{3,25},{4,28},{5,31},{6,30},{7,29},{8,16},{9,... | collective-permute-start | bytes 540680 | tf_op jit(solution)/shard_map/ppermute | solution.py:323
  73.1 13.2 %collective-permute-start.28 = (bf16[88,1024]{1,0:T(8,128)(2,1)S(1)}, bf16[88,1024]{1,0:T(8,128)(2,1)S(1)}, u32[]{:S(2)}, u32[]{:S(2)}) collective-permute-start(bf16[88,1024]{1,0:T(8,128)(2,1)S(1)} %get-tuple-element.62), channel_id=1, source_target_pairs={{0,28},{1,31},{2,30},{3,29},{4,24},{5,27},{6,26},{7,25},{8,20},{9,... | collective-permute-start | bytes 540680 | tf_op jit(solution)/shard_map/ppermute | solution.py:323
  76.9 14.5 %collective-permute-start.21 = (bf16[88,1024]{1,0:T(8,128)(2,1)S(1)}, bf16[88,1024]{1,0:T(8,128)(2,1)S(1)}, u32[]{:S(2)}, u32[]{:S(2)}) collective-permute-start(bf16[88,1024]{1,0:T(8,128)(2,1)S(1)} %get-tuple-element.55), channel_id=1, source_target_pairs={{0,10},{1,9},{2,8},{3,11},{4,14},{5,13},{6,12},{7,15},{8,2},{9,1},... | collective-permute-start | bytes 540680 | tf_op jit(solution)/shard_map/ppermute | solution.py:323
  77.0 17.2 %collective-permute-start.22 = (bf16[88,1024]{1,0:T(8,128)(2,1)S(1)}, bf16[88,1024]{1,0:T(8,128)(2,1)S(1)}, u32[]{:S(2)}, u32[]{:S(2)}) collective-permute-start(bf16[88,1024]{1,0:T(8,128)(2,1)S(1)} %get-tuple-element.56), channel_id=1, source_target_pairs={{0,14},{1,13},{2,12},{3,15},{4,10},{5,9},{6,8},{7,11},{8,6},{9,5},... | collective-permute-start | bytes 540680 | tf_op jit(solution)/shard_map/ppermute | solution.py:323
  88.7 11.4 %collective-permute-start.29 = (bf16[88,512]{1,0:T(8,128)(2,1)S(1)}, bf16[88,512]{1,0:T(8,128)(2,1)S(1)}, u32[]{:S(2)}, u32[]{:S(2)}) collective-permute-start(bf16[88,512]{1,0:T(8,128)(2,1)S(1)} %get-tuple-element.63), channel_id=1, source_target_pairs={{0,24},{1,27},{2,26},{3,25},{4,28},{5,31},{6,30},{7,29},{8,16},{9,... | collective-permute-start | bytes 270344 | tf_op jit(solution)/shard_map/ppermute | solution.py:323
  89.2 14.8 %collective-permute-start.30 = (bf16[88,512]{1,0:T(8,128)(2,1)S(1)}, bf16[88,512]{1,0:T(8,128)(2,1)S(1)}, u32[]{:S(2)}, u32[]{:S(2)}) collective-permute-start(bf16[88,512]{1,0:T(8,128)(2,1)S(1)} %get-tuple-element.64), channel_id=1, source_target_pairs={{0,25},{1,26},{2,27},{3,24},{4,29},{5,30},{6,31},{7,28},{8,17},{9,... | collective-permute-start | bytes 270344 | tf_op jit(solution)/shard_map/ppermute | solution.py:323
  91.4 14.0 %collective-permute-start.31 = (bf16[88,512]{1,0:T(8,128)(2,1)S(1)}, bf16[88,512]{1,0:T(8,128)(2,1)S(1)}, u32[]{:S(2)}, u32[]{:S(2)}) collective-permute-start(bf16[88,512]{1,0:T(8,128)(2,1)S(1)} %get-tuple-element.65), channel_id=1, source_target_pairs={{0,28},{1,31},{2,30},{3,29},{4,24},{5,27},{6,26},{7,25},{8,20},{9,... | collective-permute-start | bytes 270344 | tf_op jit(solution)/shard_map/ppermute | solution.py:323
  94.2 14.6 %collective-permute-start.32 = (bf16[88,512]{1,0:T(8,128)(2,1)S(1)}, bf16[88,512]{1,0:T(8,128)(2,1)S(1)}, u32[]{:S(2)}, u32[]{:S(2)}) collective-permute-start(bf16[88,512]{1,0:T(8,128)(2,1)S(1)} %get-tuple-element.66), channel_id=1, source_target_pairs={{0,29},{1,30},{2,31},{3,28},{4,25},{5,26},{6,27},{7,24},{8,21},{9,... | collective-permute-start | bytes 270344 | tf_op jit(solution)/shard_map/ppermute | solution.py:323
  100.1 10.8 %collective-permute-start.23 = (bf16[88,512]{1,0:T(8,128)(2,1)S(1)}, bf16[88,512]{1,0:T(8,128)(2,1)S(1)}, u32[]{:S(2)}, u32[]{:S(2)}) collective-permute-start(bf16[88,512]{1,0:T(8,128)(2,1)S(1)} %get-tuple-element.57), channel_id=1, source_target_pairs={{0,10},{1,9},{2,8},{3,11},{4,14},{5,13},{6,12},{7,15},{8,2},{9,1},... | collective-permute-start | bytes 270344 | tf_op jit(solution)/shard_map/ppermute | solution.py:323
  104.0 6.8 %collective-permute-start.24 = (bf16[88,512]{1,0:T(8,128)(2,1)S(1)}, bf16[88,512]{1,0:T(8,128)(2,1)S(1)}, u32[]{:S(2)}, u32[]{:S(2)}) collective-permute-start(bf16[88,512]{1,0:T(8,128)(2,1)S(1)} %get-tuple-element.58), channel_id=1, source_target_pairs={{0,11},{1,8},{2,9},{3,10},{4,15},{5,12},{6,13},{7,14},{8,3},{9,0},... | collective-permute-start | bytes 270344 | tf_op jit(solution)/shard_map/ppermute | solution.py:323
  105.5 6.3 %collective-permute-start.25 = (bf16[88,512]{1,0:T(8,128)(2,1)S(1)}, bf16[88,512]{1,0:T(8,128)(2,1)S(1)}, u32[]{:S(2)}, u32[]{:S(2)}) collective-permute-start(bf16[88,512]{1,0:T(8,128)(2,1)S(1)} %get-tuple-element.59), channel_id=1, source_target_pairs={{0,14},{1,13},{2,12},{3,15},{4,10},{5,9},{6,8},{7,11},{8,6},{9,5},... | collective-permute-start | bytes 270344 | tf_op jit(solution)/shard_map/ppermute | solution.py:323
  108.8 5.7 %collective-permute-start.26 = (bf16[88,512]{1,0:T(8,128)(2,1)S(1)}, bf16[88,512]{1,0:T(8,128)(2,1)S(1)}, u32[]{:S(2)}, u32[]{:S(2)}) collective-permute-start(bf16[88,512]{1,0:T(8,128)(2,1)S(1)} %get-tuple-element.60), channel_id=1, source_target_pairs={{0,15},{1,12},{2,13},{3,14},{4,11},{5,8},{6,9},{7,10},{8,7},{9,4},... | collective-permute-start | bytes 270344 | tf_op jit(solution)/shard_map/ppermute | solution.py:323
  (3 other events, 27.1 us)
